TPU v7x, 32 devices: a whole 2x2x4 slice. The times are simulated.
32 devices in a mesh: ep: 8 (over z, x), tp: 4 (over y, core).
Axes of the slice: x: 2, y: 2, z: 4, core: 2. Of those that a mesh axis runs over, the one named last changes fastest.
Arguments:
- tokens: bfloat16 [128, 1024], P('ep'), may hold values from -6 to 6
- memory: float32 [128, 4, 128, 256], P('ep', 'tp'), may hold values from -6 to 6
- log_scale: float32 [128, 4], P('ep', 'tp'), may hold values from -1 to 130
- mix_gain_in: float32 [1024], replicated, may hold values from 0.1 to 1.9
- w_query: bfloat16 [1024, 512], P(None, 'tp'), may hold values from -0.1875 to 0.1875
- w_key: bfloat16 [1024, 512], P(None, 'tp'), may hold values from -0.1875 to 0.1875
- w_value: bfloat16 [1024, 1024], P(None, 'tp'), may hold values from -0.1875 to 0.1875
- w_igate: bfloat16 [1024, 4], P(None, 'tp'), may hold values from -0.1875 to 0.1875
- w_fgate: bfloat16 [1024, 4], P(None, 'tp'), may hold values from -0.1875 to 0.1875
- igate_bias: float32 [4], P('tp'), may hold values from -1 to 1
- fgate_bias: float32 [4], P('tp'), may hold values from 0 to 4
- head_gain: float32 [1024], P('tp'), may hold values from 0.1 to 1.9
- w_output: bfloat16 [1024, 1024], P('tp'), may hold values from -0.1875 to 0.1875
- mix_gain_out: float32 [1024], replicated, may hold values from 0.1 to 1.9
- ffn_gain_in: float32 [1024], replicated, may hold values from 0.1 to 1.9
- routes: int32 [128, 6], P('ep'), may hold values from 0 to 7, all different within a row; in each aligned block of 16 rows (0 to 15, 16 to 31, ...) at most 16 rows name the same one
- route_weights: float32 [128, 6], P('ep'), may hold values from 0.1 to 1
- expert_gate: bfloat16 [8, 1024, 1024], P('ep', None, 'tp'), may hold values from -0.1875 to 0.1875
- expert_up: bfloat16 [8, 1024, 1024], P('ep', None, 'tp'), may hold values from -0.1875 to 0.1875
- expert_down: bfloat16 [8, 1024, 1024], P('ep', 'tp'), may hold values from -0.9375 to 0.9375
- ffn_gain_out: float32 [1024], P('tp'), may hold values from 0.1 to 1.9
Outputs:
- output: bfloat16 [128, 1024], P('ep', 'tp')
Inputs may be any that keep to these rules, and one draw needn't show every extreme that they name: `routes`: among the 16 tokens of one index of ep no expert is named by more than 16 tokens, and in every draw some expert is named by exactly 16 of them.
All inputs are finite; a program needn't handle non-finite values.
Results may differ from a plain program's by a relative error of at most 0.02.
Values may be sent and summed in bfloat16 or wider, within the bound.
No kernel may reach another device: no remote copies, remote signals or barrier semaphores. Data moves between devices by JAX's collectives and lax.ppermute only.
A program may use at most 64 MiB of HBM per device.

v0:
```python
import jax
import jax.numpy as jnp
from jax import lax
from jax.sharding import PartitionSpec as P

EPS = 1e-06


def rms_scale(values):
    return lax.rsqrt(jnp.mean(values * values, axis=-1, keepdims=True) + EPS)


def per_device(
    tokens,
    memory,
    log_scale,
    mix_gain_in,
    w_query,
    w_key,
    w_value,
    w_igate,
    w_fgate,
    igate_bias,
    fgate_bias,
    head_gain,
    w_output,
    mix_gain_out,
    ffn_gain_in,
    routes,
    route_weights,
    expert_gate,
    expert_up,
    expert_down,
    ffn_gain_out,
):
    f32 = jnp.float32
    bf16 = jnp.bfloat16
    seqs, width = tokens.shape
    heads = log_scale.shape[1]
    key_dim = memory.shape[2]
    value_dim = memory.shape[3]
    xf = tokens.astype(f32)
    normed = (xf * rms_scale(xf) * mix_gain_in).astype(bf16)
    query = jnp.dot(normed, w_query, preferred_element_type=f32).reshape(
        seqs, heads, key_dim
    ) * key_dim ** (-0.5)
    keys = jnp.dot(normed, w_key, preferred_element_type=f32).reshape(seqs, heads, key_dim)
    values = jnp.dot(normed, w_value, preferred_element_type=f32).reshape(seqs, heads, value_dim)
    in_pre = jnp.dot(normed, w_igate, preferred_element_type=f32) + igate_bias
    forget_log = jax.nn.log_sigmoid(
        jnp.dot(normed, w_fgate, preferred_element_type=f32) + fgate_bias
    )
    carried = forget_log + log_scale
    new_max = jnp.maximum(carried, in_pre)
    carry_weight = jnp.exp(carried - new_max)
    fresh_weight = jnp.exp(in_pre - new_max)
    recall = jnp.einsum("shk,shkv->shv", query, memory, precision=lax.Precision.HIGHEST)
    match = jnp.sum(query * keys, axis=-1)
    read = carry_weight[..., None] * recall + (fresh_weight * match)[..., None] * values
    headout = (
        (read * rms_scale(read) * head_gain.reshape(heads, value_dim))
        .astype(bf16)
        .reshape(seqs, heads * value_dim)
    )
    partial_value = jnp.dot(headout, w_output, preferred_element_type=f32)
    mixed = lax.psum(partial_value.astype(jnp.bfloat16), "tp").astype(jnp.float32)
    resid = (xf + mixed * rms_scale(mixed) * mix_gain_out).astype(bf16)
    rf = resid.astype(f32)
    ffn_in = (rf * rms_scale(rf) * ffn_gain_in).astype(bf16)
    lanes = lax.axis_size("tp")
    quarter = width // lanes
    own = lax.axis_index("tp") * quarter
    local_experts = expert_gate.shape[0]
    experts_all = local_experts * lax.axis_size("ep")
    top = routes.shape[1]
    cap = min(seqs, max(2, 3 * seqs * top // (2 * experts_all)))
    flat = routes.reshape(-1)
    hits = (flat[:, None] == jnp.arange(experts_all, dtype=jnp.int32)[None, :]).astype(jnp.int32)
    earlier = jnp.cumsum(hits, axis=0) - hits
    slot = jnp.sum(earlier * hits, axis=1)
    place = (flat * cap + slot).reshape(seqs, top)
    picker = jnp.any(
        jnp.arange(experts_all * cap, dtype=jnp.int32)[:, None, None] == place[None, :, :], axis=2
    ).astype(bf16)
    outbound = (
        jnp.dot(picker, ffn_in, preferred_element_type=f32)
        .astype(bf16)
        .reshape(experts_all, cap, width)
    )
    arrived = lax.all_to_all(outbound, "ep", split_axis=0, concat_axis=0, tiled=True)
    items = arrived.shape[1]
    rows = arrived.reshape(-1, local_experts, items, width)
    gate = jnp.einsum("secd,edf->secf", rows, expert_gate, preferred_element_type=f32)
    up = jnp.einsum("secd,edf->secf", rows, expert_up, preferred_element_type=f32)
    act = (jax.nn.silu(gate) * up).astype(bf16)
    part = jnp.einsum("secf,efd->secd", act, expert_down, preferred_element_type=f32).reshape(
        -1, items, width
    )
    summed = lax.psum_scatter(
        part.astype(jnp.bfloat16), "tp", scatter_dimension=2, tiled=True
    ).astype(jnp.float32)
    done = summed.astype(bf16)
    returned = lax.all_to_all(done, "ep", split_axis=0, concat_axis=0, tiled=True)
    columns = returned.shape[2]
    chosen = jnp.take(returned.reshape(-1, columns), place.reshape(-1), axis=0).reshape(
        seqs, top, columns
    )
    routed = jnp.sum(route_weights[:, :, None] * chosen.astype(f32), axis=1)
    resid_part = lax.dynamic_slice_in_dim(rf, own, quarter, 1)
    total = lax.psum(jnp.sum(routed * routed, axis=1), "tp")
    scaled = routed * lax.rsqrt(total / width + EPS)[:, None]
    return (resid_part + scaled * ffn_gain_out).astype(bf16)


def solution(mesh):
    return jax.shard_map(
        per_device,
        mesh=mesh,
        in_specs=(
            P("ep", None),
            P("ep", "tp", None, None),
            P("ep", "tp"),
            P(),
            P(None, "tp"),
            P(None, "tp"),
            P(None, "tp"),
            P(None, "tp"),
            P(None, "tp"),
            P("tp"),
            P("tp"),
            P("tp"),
            P("tp", None),
            P(),
            P(),
            P("ep", None),
            P("ep", None),
            P("ep", None, "tp"),
            P("ep", None, "tp"),
            P("ep", "tp", None),
            P("tp"),
        ),
        out_specs=P("ep", "tp"),
        check_vma=False,
    )
```

profile of v0, /device:TPU:0, one launch (start us, length us, event | category | flops | bytes accessed | tf_op | source)
XLA Modules:
  0.0 91.5 jit_solution(16629815895781907717)
XLA Ops:
  6.5 0.0 copy-start
  6.5 0.0 copy-start.8
  6.6 0.0 copy-start.2
  6.6 0.0 reduce-scatter.2.cloned.1.call-start
  6.6 0.0 copy-start.10
  6.6 1.0 %fusion.22 = f32[16]{0:T(128)S(1)} fusion(bf16[16,1024]{1,0:T(8,128)(2,1)} %param.21), kind=kLoop, calls=%fused_computation.38 | loop fusion | flops 49136 | bytes 32832 | tf_op jit(solution)/shard_map/reduce_sum | solution.py:10
  9.0 0.0 copy-start.4
  9.0 1.2 %convolution_multiply_fusion.2 = f32[16,128]{1,0:T(8,128)S(1)} fusion(bf16[1024,128]{1,0:T(8,128)(2,1)} %param.25, bf16[16,1024]{1,0:T(8,128)(2,1)} %param.21, f32[1024]{0:T(1024)} %param.24, f32[16]{0:T(128)S(1)} %add_rsqrt_fusion.4), kind=kOutput, calls=%fused_computation.14 | convolution fusion | flops 4261888 | bytes 307264 | tf_op jit(solution)/shard_map/dot_general | solution.py:44
  10.2 1.3 %fusion.6 = f32[16]{0:T(128)S(1)} fusion(f32[16,128]{1,0:T(8,128)S(1)} %convolution_multiply_fusion.2, bf16[1024,128]{1,0:T(8,128)(2,1)} %param.26, bf16[16,1024]{1,0:T(8,128)(2,1)} %param.21, f32[1024]{0:T(1024)} %param.24, f32[16]{0:T(128)S(1)} %add_rsqrt_fusion.4), kind=kOutput, calls=%fused_computation.15 | convolution fusion | flops 4263920 | bytes 307328 | tf_op jit(solution)/shard_map/dot_general | solution.py:47
  11.5 0.0 copy-start.7
  11.5 1.0 %fusion.8 = f32[16,1]{0,1:T(1,128)S(1)} fusion(bf16[1024,1]{0,1:T(2,128)(2,1)} %param.28, f32[]{:T(128)} %bitcast.97, bf16[16,1024]{1,0:T(8,128)(2,1)} %param.21, f32[1024]{0:T(1024)} %param.24, f32[16]{0:T(128)S(1)} %add_rsqrt_fusion.4), kind=kOutput, calls=%fused_computation.18 | convolution fusion | flops 98320 | bytes 39044 | tf_op jit(solution)/shard_map/dot_general | solution.py:49
  12.5 0.0 copy-done
  12.5 1.1 %fusion = f32[16,1,256]{2,1,0:T(1,128)S(1)} fusion(f32[16,128,1]{1,2,0:T(1,128)S(1)} %bitcast.101, f32[16,1,128,256]{3,2,1,0:T(8,128)S(1)} %copy-done), kind=kOutput, calls=%fused_computation.1 | convolution fusion | flops 6291456 | bytes 2121728 | tf_op jit(solution)/shard_map/shk,shkv->shv/dot_general | solution.py:57
  13.6 0.0 copy-done.3
  13.6 0.0 copy-done.12
  13.6 0.2 fusion.39
  13.9 0.3 multiply_reduce_fusion.3
  14.2 0.2 convolution_convert_fusion.2
  14.5 12.9 %psum.14 = bf16[16,1024]{1,0:T(8,128)(2,1)S(1)} all-reduce(bf16[16,1024]{1,0:T(8,128)(2,1)S(1)} %convolution_convert_fusion.2), channel_id=1, replica_groups=mesh['ep'=8,'tp'=4] {'tp'}, use_global_device_ids=true, to_apply=%region_3.4 | all-reduce | flops 16384 | bytes 65536 | tf_op jit(solution)/shard_map/psum | solution.py:66
  27.4 0.1 fusion.20
  27.5 0.0 copy-done.4
  27.5 0.2 multiply_reduce_fusion.1
  27.8 0.0 copy-done.5
  27.8 0.1 copy.29
  27.8 0.1 reshape.181
  27.9 0.1 fusion.27
  28.0 0.1 reduce_window_sum.11
  28.2 0.2 select_reduce_fusion
  28.3 0.1 reduce_sum.84
  28.5 0.1 copy.31
  28.5 0.1 fusion.28
  28.6 0.3 convolution_convert_fusion.1
  28.9 0.0 copy-start.9
  28.9 13.8 %all_to_all.10 = bf16[8,16,1024]{2,1,0:T(8,128)(2,1)S(1)} all-to-all(bf16[8,16,1024]{2,1,0:T(8,128)(2,1)S(1)} %bitcast.100), channel_id=1, replica_groups=mesh['ep'=8,'tp'=4] {'ep'}, dimensions={0} | all-to-all | bytes 524288 | tf_op jit(solution)/shard_map/all_to_all | solution.py:90
  42.8 0.2 convolution_bitcast_fusion.1
  43.0 2.4 %convolution_convert_fusion = bf16[8,16,1024]{2,1,0:T(8,128)(2,1)} fusion(bf16[8,16,1024]{2,1,0:T(8,128)(2,1)S(1)} %all_to_all.10, bf16[1,256,1024]{2,1,0:T(8,128)(2,1)} %param.40, bf16[1,1024,256]{2,1,0:T(8,128)(2,1)} %param.39, f32[8,1,16,256]{3,2,0,1:T(8,128)S(1)} %convolution_bitcast_fusion.1), kind=kOutput, calls=%fused_computation.3 | convolution fusion | flops 134545408 | bytes 1703936 | tf_op jit(solution)/shard_map/secf,efd->secd/dot_general | solution.py:96
  45.4 0.0 reduce-scatter.2.cloned.1.call-update
  45.4 0.1 mul.213
  45.5 19.0 %reduce-scatter.2.cloned.1.call-done = bf16[8,16,256]{2,1,0:T(8,128)(2,1)} async-done(((bf16[8,16,1024]{2,1,0:T(8,128)(2,1)}), bf16[8,16,256]{2,1,0:T(8,128)(2,1)}) %reduce-scatter.2.cloned.1.call-update) | async-done | bytes 65552 | tf_op jit(solution)/shard_map/reduce_scatter | solution.py:99
  64.5 5.5 %all-to-all-start.1 = ((bf16[8,16,256]{2,1,0:T(8,128)(2,1)}), bf16[8,16,256]{2,1,0:T(8,128)(2,1)S(1)}, u32[]{:S(2)}, u32[]{:S(2)}) async-start(bf16[8,16,256]{2,1,0:T(8,128)(2,1)} %reduce-scatter.2.cloned.1.call-done), calls=%async_computation.2 | async-start | bytes 131072 | tf_op jit(solution)/shard_map/all_to_all | solution.py:103
  70.1 0.1 copy.28
  70.2 6.8 %all-to-all-done.1 = bf16[8,16,256]{2,1,0:T(8,128)(2,1)S(1)} async-done(((bf16[8,16,256]{2,1,0:T(8,128)(2,1)}), bf16[8,16,256]{2,1,0:T(8,128)(2,1)S(1)}, u32[]{:S(2)}, u32[]{:S(2)}) %all-to-all-start.1) | async-done | bytes 65568 | tf_op jit(solution)/shard_map/all_to_all | solution.py:103
  77.0 0.8 gather_fusion
  77.8 0.1 multiply_reduce_fusion
  77.9 0.1 multiply_reduce_fusion.2
  78.0 5.9 %psum.15 = f32[16]{0:T(128)S(1)} all-reduce(f32[16]{0:T(128)S(1)} %multiply_reduce_fusion.2), channel_id=1, replica_groups=mesh['ep'=8,'tp'=4] {'tp'}, use_global_device_ids=true, to_apply=%region_12.13 | all-reduce | flops 16 | bytes 128 | tf_op jit(solution)/shard_map/psum | solution.py:110
  84.0 0.0 copy-done.9
  84.0 0.7 add_convert_fusion
  (25 shorter events, 0.1 us)
Async XLA Ops:
  6.5 6.0 %copy-start = (f32[16,1,128,256]{3,2,1,0:T(8,128)S(1)}, f32[16,1,128,256]{3,2,1,0:T(8,128)}, u32[]{:S(2)}) copy-start(f32[16,1,128,256]{3,2,1,0:T(8,128)} %param.22) | copy-start | bytes 6291460
  6.5 7.1 %copy-start.3 = (bf16[16,1024]{1,0:T(8,128)(2,1)S(1)}, bf16[16,1024]{1,0:T(8,128)(2,1)}, u32[]{:S(2)}) copy-start(bf16[16,1024]{1,0:T(8,128)(2,1)} %param.21) | copy-start | bytes 98308
  6.5 7.1 %copy-start.12 = (f32[1024]{0:T(1024)S(1)}, f32[1024]{0:T(1024)}, u32[]{:S(2)}) copy-start(f32[1024]{0:T(1024)} %param.24) | copy-start | bytes 12292
  6.5 7.1 %copy-start.13 = (f32[16,1]{0,1:T(1,128)S(1)}, f32[16,1]{0,1:T(1,128)}, u32[]{:S(2)}) copy-start(f32[16,1]{0,1:T(1,128)} %param.23) | copy-start | bytes 196
  6.5 7.1 %copy-start.11 = (bf16[1024,1]{0,1:T(2,128)(2,1)S(1)}, bf16[1024,1]{0,1:T(2,128)(2,1)}, u32[]{:S(2)}) copy-start(bf16[1024,1]{0,1:T(2,128)(2,1)} %param.29) | copy-start | bytes 6148
  6.5 7.7 %copy-start.8 = (f32[256]{0:T(256)S(1)}, f32[256]{0:T(256)}, u32[]{:S(2)}) copy-start(f32[256]{0:T(256)} %param.32) | copy-start | bytes 3076
  6.6 7.7 %copy-start.2 = (bf16[256,1024]{1,0:T(8,128)(2,1)S(1)}, bf16[256,1024]{1,0:T(8,128)(2,1)}, u32[]{:S(2)}) copy-start(bf16[256,1024]{1,0:T(8,128)(2,1)} %param.33) | copy-start | bytes 1572868
  6.6 58.0 %reduce-scatter.2.cloned.1.call-start = ((), (), s32[]{:S(2)}) async-start(), calls=%async_computation.3 | async-start | bytes 327680 | tf_op jit(solution)/shard_map/reduce_scatter | solution.py:99
  6.6 7.3 %copy-start.10 = (bf16[1024,256]{1,0:T(8,128)(2,1)S(1)}, bf16[1024,256]{1,0:T(8,128)(2,1)}, u32[]{:S(2)}) copy-start(bf16[1024,256]{1,0:T(8,128)(2,1)} %param.27) | copy-start | bytes 1572868
  9.0 18.5 %copy-start.4 = (f32[1024]{0:T(1024)S(1)}, f32[1024]{0:T(1024)}, u32[]{:S(2)}) copy-start(f32[1024]{0:T(1024)} %param.34) | copy-start | bytes 12292
  10.2 17.6 %copy-start.5 = (s32[16,6]{0,1:T(8,128)S(1)}, s32[16,6]{0,1:T(8,128)}, u32[]{:S(2)}) copy-start(s32[16,6]{0,1:T(8,128)} %param.36) | copy-start | bytes 1156
  11.5 17.1 %copy-start.7 = (f32[1024]{0:T(1024)S(1)}, f32[1024]{0:T(1024)}, u32[]{:S(2)}) copy-start(f32[1024]{0:T(1024)} %param.35) | copy-start | bytes 12292
  12.5 30.2 %copy-start.1 = (bf16[1,1024,256]{2,1,0:T(8,128)(2,1)S(1)}, bf16[1,1024,256]{2,1,0:T(8,128)(2,1)}, u32[]{:S(2)}) copy-start(bf16[1,1024,256]{2,1,0:T(8,128)(2,1)} %param.38) | copy-start | bytes 1572868
  27.7 42.3 %copy-start.6 = (f32[16,6]{0,1:T(8,128)S(1)}, f32[16,6]{0,1:T(8,128)}, u32[]{:S(2)}) copy-start(f32[16,6]{0,1:T(8,128)} %param.37) | copy-start | bytes 1156
  28.9 55.0 %copy-start.9 = (f32[256]{0:T(256)S(1)}, f32[256]{0:T(256)}, u32[]{:S(2)}) copy-start(f32[256]{0:T(256)} %param.41) | copy-start | bytes 3076
  64.5 12.4 %all-to-all-start.1 = ((bf16[8,16,256]{2,1,0:T(8,128)(2,1)}), bf16[8,16,256]{2,1,0:T(8,128)(2,1)S(1)}, u32[]{:S(2)}, u32[]{:S(2)}) async-start(bf16[8,16,256]{2,1,0:T(8,128)(2,1)} %reduce-scatter.2.cloned.1.call-done), calls=%async_computation.2 | async-start | bytes 131072 | tf_op jit(solution)/shard_map/all_to_all | solution.py:103
Sparse Core Ops, SparseCore 0:
  45.5 18.9 reduce-scatter.1
where the time goes:
time: 91.9 us; the launch traced here: 91.5 us
  blocking collectives  32.7 us (36%)
  waiting for transfers between devices  25.8 us (28%)
  between operations  15 us (16%)
  matrix products  8.26 us (9%)
  starting transfers between devices  5.57 us (6%)
  other arithmetic  2.83 us (3%)
  local copies, waits for them, and re-layouts  1.35 us (1%)
    reduce_scatter x1, waiting for transfers between devices, per_device(): lax.psum_scatter(part.astype(jnp.bfloat16), 'tp', scatter_dimension=2, ti...  19 us
    all_to_all x1, blocking collectives, per_device(): lax.all_to_all(outbound, 'ep', split_axis=0, concat_axis=0, tiled=True)  13.8 us
    psum x1, blocking collectives, per_device(): lax.psum(partial_value.astype(jnp.bfloat16), 'tp').astype(jnp.float32)  12.9 us
    all_to_all x1, waiting for transfers between devices, per_device(): lax.all_to_all(done, 'ep', split_axis=0, concat_axis=0, tiled=True)  6.79 us
    psum x1, blocking collectives, per_device(): total = lax.psum(jnp.sum(routed * routed, axis=1), 'tp')  5.95 us
    all_to_all x1, starting transfers between devices, per_device(): lax.all_to_all(done, 'ep', split_axis=0, concat_axis=0, tiled=True)  5.53 us
    dot_general x1, matrix products, per_device(): jnp.einsum('secf,efd->secd', act, expert_down, preferred_element_type=f32)  2.4 us
  transfers between devices with their start and end apart: 2, of which 2 were waited for; matrix products, arithmetic and copies ran while one was open for 0% of the time, Pallas kernels for 0%

commit v1 on v0

--- a/solution.py
+++ b/solution.py
@@ -63,17 +63,71 @@
         .reshape(seqs, heads * value_dim)
     )
     partial_value = jnp.dot(headout, w_output, preferred_element_type=f32)
-    mixed = lax.psum(partial_value.astype(jnp.bfloat16), "tp").astype(jnp.float32)
+    mixed = sum_over(partial_value.astype(bf16), "tp")
     resid = (xf + mixed * rms_scale(mixed) * mix_gain_out).astype(bf16)
     rf = resid.astype(f32)
     ffn_in = (rf * rms_scale(rf) * ffn_gain_in).astype(bf16)
     lanes = lax.axis_size("tp")
+    groups = lax.axis_size("ep")
     quarter = width // lanes
     own = lax.axis_index("tp") * quarter
     local_experts = expert_gate.shape[0]
-    experts_all = local_experts * lax.axis_size("ep")
+    experts_all = local_experts * groups
     top = routes.shape[1]
     cap = min(seqs, max(2, 3 * seqs * top // (2 * experts_all)))
+    if cap == seqs and local_experts == 1:
+        routed = every_token(ffn_in, routes, route_weights, expert_gate, expert_up, expert_down)
+    else:
+        routed = slotted(ffn_in, routes, route_weights, expert_gate, expert_up, expert_down, cap)
+    resid_part = lax.dynamic_slice_in_dim(rf, own, quarter, 1)
+    total = sum_over(jnp.sum(routed * routed, axis=1), "tp")
+    scaled = routed * lax.rsqrt(total / width + EPS)[:, None]
+    return (resid_part + scaled * ffn_gain_out).astype(bf16)
+
+
+def sum_over(value, axis):
+    size = lax.axis_size(axis)
+    total = value.astype(jnp.float32)
+    for step in range(1, size):
+        if size & (size - 1) == 0:
+            pairs = [(i, i ^ step) for i in range(size)]
+        else:
+            pairs = [(i, (i + step) % size) for i in range(size)]
+        total = total + lax.ppermute(value, axis, pairs).astype(jnp.float32)
+    return total
+
+
+def every_token(ffn_in, routes, route_weights, expert_gate, expert_up, expert_down):
+    f32 = jnp.float32
+    bf16 = jnp.bfloat16
+    seqs, width = ffn_in.shape
+    lanes = lax.axis_size("tp")
+    groups = lax.axis_size("ep")
+    quarter = width // lanes
+    spread = jnp.broadcast_to(ffn_in[None], (groups, seqs, width))
+    rows = lax.all_to_all(spread, "ep", split_axis=0, concat_axis=0, tiled=True)
+    rows = rows.reshape(groups * seqs, width)
+    gate = jnp.dot(rows, expert_gate[0], preferred_element_type=f32)
+    up = jnp.dot(rows, expert_up[0], preferred_element_type=f32)
+    act = (jax.nn.silu(gate) * up).astype(bf16)
+    part = jnp.dot(act, expert_down[0], preferred_element_type=f32).astype(bf16)
+    blocks = part.reshape(groups, seqs, lanes, quarter).transpose(0, 2, 1, 3)
+    blocks = blocks.reshape(groups * lanes, seqs, quarter)
+    back = lax.all_to_all(blocks, ("ep", "tp"), split_axis=0, concat_axis=0, tiled=True)
+    back = back.reshape(groups, lanes, seqs, quarter).astype(f32)
+    done = jnp.sum(back, axis=1).astype(bf16).astype(f32)
+    named = routes[:, :, None] == jnp.arange(groups, dtype=jnp.int32)[None, None, :]
+    weights = jnp.sum(jnp.where(named, route_weights[:, :, None], 0.0), axis=1)
+    return jnp.sum(weights.T[:, :, None] * done, axis=0)
+
+
+def slotted(ffn_in, routes, route_weights, expert_gate, expert_up, expert_down, cap):
+    f32 = jnp.float32
+    bf16 = jnp.bfloat16
+    seqs, width = ffn_in.shape
+    top = routes.shape[1]
+    local_experts = expert_gate.shape[0]
+    experts_all = local_experts * lax.axis_size("ep")
     flat = routes.reshape(-1)
     hits = (flat[:, None] == jnp.arange(experts_all, dtype=jnp.int32)[None, :]).astype(jnp.int32)
     earlier = jnp.cumsum(hits, axis=0) - hits
@@ -105,11 +159,7 @@
     chosen = jnp.take(returned.reshape(-1, columns), place.reshape(-1), axis=0).reshape(
         seqs, top, columns
     )
-    routed = jnp.sum(route_weights[:, :, None] * chosen.astype(f32), axis=1)
-    resid_part = lax.dynamic_slice_in_dim(rf, own, quarter, 1)
-    total = lax.psum(jnp.sum(routed * routed, axis=1), "tp")
-    scaled = routed * lax.rsqrt(total / width + EPS)[:, None]
-    return (resid_part + scaled * ffn_gain_out).astype(bf16)
+    return jnp.sum(route_weights[:, :, None] * chosen.astype(f32), axis=1)
 
 
 def solution(mesh):

time: 91.9 us -> 51 us (0.55)
  blocking collectives: 32.7 us -> 14.9 us
  between operations: 15 us -> 1.55 us
  waiting for transfers between devices: 25.8 us -> 15.7 us
  starting transfers between devices: 5.57 us -> 7.99 us
  matrix products: 8.26 us -> 7.14 us
    reduce_scatter x1 -> x0, waiting for transfers between devices: 19 us -> none  [per_device(): lax.psum_scatter(part.astype(jnp.bfloat16), 'tp', scatter_dimension=2, ti...]
    psum x2 -> x0, blocking collectives: 18.9 us -> none  [the longest x1 12.9 us: per_device(): lax.psum(partial_value.astype(jnp.bfloat16), 'tp').astype(jnp.float32)]
    ppermute x0 -> x6, waiting for transfers between devices: none -> 5.21 us  [sum_over(): total = total + lax.ppermute(value, axis, pairs).astype(jnp.float32)]
    ppermute x0 -> x6, starting transfers between devices: none -> 5.05 us  [sum_over(): total = total + lax.ppermute(value, axis, pairs).astype(jnp.float32)]
    all_to_all x1, waiting for transfers between devices: 6.79 us -> 10.5 us  [every_token(): lax.all_to_all(blocks, ('ep', 'tp'), split_axis=0, concat_axis=0, tiled=T...]
    all_to_all x1, starting transfers between devices: 5.53 us -> 2.94 us  [every_token(): lax.all_to_all(blocks, ('ep', 'tp'), split_axis=0, concat_axis=0, tiled=T...]
    dot_general x3 -> x2, matrix products: 2.9 us -> 1.78 us  [the longest x1 1.55 us: every_token(): part = jnp.dot(act, expert_down[0], preferred_element_type=f32).astype(bf16)]
    all_to_all x1, blocking collectives: 13.8 us -> 14.9 us  [every_token(): rows = lax.all_to_all(spread, 'ep', split_axis=0, concat_axis=0, tiled=True)]
  transfers between devices with their start and end apart: 2 -> 7, of which waited for: 2 -> 5; matrix products, arithmetic and copies ran while one was open for 0% -> 0% of each run, Pallas kernels for 0% -> 0%
where the time goes in v1:
time: 51 us; the launch traced here: 50.7 us
  waiting for transfers between devices  15.7 us (31%)
  blocking collectives  14.9 us (29%)
  starting transfers between devices  7.99 us (16%)
  matrix products  7.14 us (14%)
  other arithmetic  2.4 us (5%)
  between operations  1.55 us (3%)
  local copies, waits for them, and re-layouts  0.99 us (2%)
    all_to_all x1, blocking collectives, every_token(): rows = lax.all_to_all(spread, 'ep', split_axis=0, concat_axis=0, tiled=True)  14.9 us
    all_to_all x1, waiting for transfers between devices, every_token(): lax.all_to_all(blocks, ('ep', 'tp'), split_axis=0, concat_axis=0, tiled=T...  10.5 us
    ppermute x6, waiting for transfers between devices, sum_over(): total = total + lax.ppermute(value, axis, pairs).astype(jnp.float32)  5.21 us
    ppermute x6, starting transfers between devices, sum_over(): total = total + lax.ppermute(value, axis, pairs).astype(jnp.float32)  5.05 us
    all_to_all x1, starting transfers between devices, every_token(): lax.all_to_all(blocks, ('ep', 'tp'), split_axis=0, concat_axis=0, tiled=T...  2.94 us
    dot_general x1, matrix products, every_token(): part = jnp.dot(act, expert_down[0], preferred_element_type=f32).astype(bf16)  1.55 us
    reduce_sum x3, other arithmetic, rms_scale(): return lax.rsqrt(jnp.mean(values * values, axis=-1, keepdims=True) + EPS)  1.36 us
    dot_general x1, matrix products, per_device(): jnp.dot(normed, w_key, preferred_element_type=f32)  1.32 us
  transfers between devices with their start and end apart: 7, of which 5 were waited for; matrix products, arithmetic and copies ran while one was open for 0% of the time, Pallas kernels for 0%

profile of v1, /device:TPU:0, one launch (start us, length us, event | category | flops | bytes accessed | tf_op | source)
XLA Modules:
  0.0 50.7 jit_solution(12915245315478170360)
XLA Ops:
  0.0 0.0 copy-start
  0.0 0.0 copy-start.12
  0.0 0.0 copy-start.11
  0.0 0.0 copy-start.9
  0.0 0.0 copy-start.2
  0.1 1.0 %fusion.19 = f32[16]{0:T(128)S(1)} fusion(bf16[16,1024]{1,0:T(8,128)(2,1)} %param.21), kind=kLoop, calls=%fused_computation.31 | loop fusion | flops 49136 | bytes 32832 | tf_op jit(solution)/shard_map/reduce_sum | solution.py:10
  2.4 0.0 copy-start.5
  2.4 1.2 %convolution_multiply_fusion.3 = f32[16,128]{1,0:T(8,128)S(1)} fusion(bf16[1024,128]{1,0:T(8,128)(2,1)} %param.25, bf16[16,1024]{1,0:T(8,128)(2,1)} %param.21, f32[1024]{0:T(1024)} %param.24, f32[16]{0:T(128)S(1)} %add_rsqrt_fusion.4), kind=kOutput, calls=%fused_computation.9 | convolution fusion | flops 4261888 | bytes 307264 | tf_op jit(solution)/shard_map/dot_general | solution.py:44
  3.6 1.3 %fusion.4 = f32[16]{0:T(128)S(1)} fusion(f32[16,128]{1,0:T(8,128)S(1)} %convolution_multiply_fusion.3, bf16[1024,128]{1,0:T(8,128)(2,1)} %param.26, bf16[16,1024]{1,0:T(8,128)(2,1)} %param.21, f32[1024]{0:T(1024)} %param.24, f32[16]{0:T(128)S(1)} %add_rsqrt_fusion.4), kind=kOutput, calls=%fused_computation.10 | convolution fusion | flops 4263920 | bytes 307328 | tf_op jit(solution)/shard_map/dot_general | solution.py:47
  4.9 1.0 %fusion.6 = f32[16,1]{0,1:T(1,128)S(1)} fusion(bf16[1024,1]{0,1:T(2,128)(2,1)} %param.28, f32[]{:T(128)} %bitcast.68, bf16[16,1024]{1,0:T(8,128)(2,1)} %param.21, f32[1024]{0:T(1024)} %param.24, f32[16]{0:T(128)S(1)} %add_rsqrt_fusion.4), kind=kOutput, calls=%fused_computation.13 | convolution fusion | flops 98320 | bytes 39044 | tf_op jit(solution)/shard_map/dot_general | solution.py:49
  5.9 0.0 copy-done
  5.9 1.1 %fusion = f32[16,1,256]{2,1,0:T(1,128)S(1)} fusion(f32[16,128,1]{1,2,0:T(1,128)S(1)} %bitcast.73, f32[16,1,128,256]{3,2,1,0:T(8,128)S(1)} %copy-done), kind=kOutput, calls=%fused_computation | convolution fusion | flops 6291456 | bytes 2121728 | tf_op jit(solution)/shard_map/shk,shkv->shv/dot_general | solution.py:57
  7.0 0.0 copy-done.4
  7.0 0.0 copy-done.13
  7.1 0.2 fusion.31
  7.3 0.0 copy-done.11
  7.3 0.3 multiply_reduce_fusion.4
  7.7 0.2 convolution_convert_fusion.1
  7.9 0.5 %collective-permute-start = (bf16[16,1024]{1,0:T(8,128)(2,1)S(1)}, bf16[16,1024]{1,0:T(8,128)(2,1)S(1)}, u32[]{:S(2)}, u32[]{:S(2)}) collective-permute-start(bf16[16,1024]{1,0:T(8,128)(2,1)S(1)} %convolution_convert_fusion.1), channel_id=1, source_target_pairs={{0,1},{1,0},{2,3},{3,2},{4,5},{5,4},{6,7},{7,6},{8,9},{9,8},{10,11... | collective-permute-start | bytes 98312 | tf_op jit(solution)/shard_map/ppermute | solution.py:96
  8.4 2.5 %collective-permute-start.1 = (bf16[16,1024]{1,0:T(8,128)(2,1)S(1)}, bf16[16,1024]{1,0:T(8,128)(2,1)S(1)}, u32[]{:S(2)}, u32[]{:S(2)}) collective-permute-start(bf16[16,1024]{1,0:T(8,128)(2,1)S(1)} %convolution_convert_fusion.1), channel_id=1, source_target_pairs={{0,2},{1,3},{2,0},{3,1},{4,6},{5,7},{6,4},{7,5},{8,10},{9,11},{10,... | collective-permute-start | bytes 98312 | tf_op jit(solution)/shard_map/ppermute | solution.py:96
  10.9 0.1 collective-permute-start.2
  11.0 0.0 collective-permute-done
  11.0 1.9 %collective-permute-done.1 = bf16[16,1024]{1,0:T(8,128)(2,1)S(1)} collective-permute-done((bf16[16,1024]{1,0:T(8,128)(2,1)S(1)}, bf16[16,1024]{1,0:T(8,128)(2,1)S(1)}, u32[]{:S(2)}, u32[]{:S(2)}) %collective-permute-start.1) | collective-permute-done | bytes 32800 | tf_op jit(solution)/shard_map/ppermute | solution.py:96
  13.0 1.3 %collective-permute-done.2 = bf16[16,1024]{1,0:T(8,128)(2,1)S(1)} collective-permute-done((bf16[16,1024]{1,0:T(8,128)(2,1)S(1)}, bf16[16,1024]{1,0:T(8,128)(2,1)S(1)}, u32[]{:S(2)}, u32[]{:S(2)}) %collective-permute-start.2) | collective-permute-done | bytes 32800 | tf_op jit(solution)/shard_map/ppermute | solution.py:96
  14.3 0.1 multiply_reduce_fusion.2
  14.4 0.2 multiply_reduce_fusion.1
  14.6 0.0 copy-done.6
  14.6 0.1 multiply_convert_fusion
  14.7 14.9 %all_to_all.10 = bf16[8,16,1024]{2,1,0:T(8,128)(2,1)S(1)} all-to-all(bf16[8,16,1024]{2,1,0:T(8,128)(2,1)S(1)} %broadcast_in_dim.12), channel_id=1, replica_groups=mesh['ep'=8,'tp'=4] {'ep'}, dimensions={0} | all-to-all | bytes 524288 | tf_op jit(solution)/shard_map/all_to_all | solution.py:108
  29.6 0.2 fusion.12
  29.9 0.0 copy-done.3
  29.9 0.0 copy-start.10
  29.9 1.5 %convolution_convert_fusion = bf16[128,1024]{1,0:T(8,128)(2,1)S(1)} fusion(bf16[128,1024]{1,0:T(8,128)(2,1)S(1)} %bitcast.71, bf16[1,256,1024]{2,1,0:T(8,128)(2,1)S(1)} %copy-done.3, bf16[1,1024,256]{2,1,0:T(8,128)(2,1)} %param.39, f32[128,256]{1,0:T(8,128)S(1)} %fusion.12), kind=kOutput, calls=%fused_computation.2 | convolution fusion | flops 134545408 | bytes 1703936 | tf_op jit(solution)/shard_map/dot_general | solution.py:113
  31.4 0.2 reshape.118
  31.6 0.7 %copy.29 = bf16[8,16,4,256]{3,1,2,0:T(8,128)(2,1)} copy(bf16[8,16,4,256]{3,2,1,0:T(4,128)(2,1)S(1)} %reshape.118) | data formatting | bytes 524288 | tf_op jit(solution)/shard_map/reshape | solution.py:114
  32.3 2.9 %all-to-all-start.1 = ((bf16[32,16,256]{2,1,0:T(8,128)(2,1)}), bf16[32,16,256]{2,1,0:T(8,128)(2,1)S(1)}, u32[]{:S(2)}, u32[]{:S(2)}) async-start(bf16[32,16,256]{2,1,0:T(8,128)(2,1)} %bitcast.19), calls=%async_computation.1 | async-start | bytes 524288 | tf_op jit(solution)/shard_map/all_to_all | solution.py:116
  35.3 0.0 copy-done.7
  35.3 0.0 copy-done.8
  35.3 10.5 %all-to-all-done.1 = bf16[32,16,256]{2,1,0:T(8,128)(2,1)S(1)} async-done(((bf16[32,16,256]{2,1,0:T(8,128)(2,1)}), bf16[32,16,256]{2,1,0:T(8,128)(2,1)S(1)}, u32[]{:S(2)}, u32[]{:S(2)}) %all-to-all-start.1) | async-done | bytes 262176 | tf_op jit(solution)/shard_map/all_to_all | solution.py:116
  45.9 0.1 multiply_reduce_fusion
  46.0 0.1 multiply_reduce_fusion.3
  46.1 0.1 collective-permute-start.3
  46.2 0.8 %collective-permute-start.4 = (f32[16]{0:T(128)S(1)}, f32[16]{0:T(128)S(1)}, u32[]{:S(2)}, u32[]{:S(2)}) collective-permute-start(f32[16]{0:T(128)S(1)} %multiply_reduce_fusion.3), channel_id=1, source_target_pairs={{0,2},{1,3},{2,0},{3,1},{4,6},{5,7},{6,4},{7,5},{8,10},{9,11},{10,... | collective-permute-start | bytes 200 | tf_op jit(solution)/shard_map/ppermute | solution.py:96
  47.0 1.0 %collective-permute-start.5 = (f32[16]{0:T(128)S(1)}, f32[16]{0:T(128)S(1)}, u32[]{:S(2)}, u32[]{:S(2)}) collective-permute-start(f32[16]{0:T(128)S(1)} %multiply_reduce_fusion.3), channel_id=1, source_target_pairs={{0,3},{1,2},{2,1},{3,0},{4,7},{5,6},{6,5},{7,4},{8,11},{9,10},{10,... | collective-permute-start | bytes 200 | tf_op jit(solution)/shard_map/ppermute | solution.py:96
  48.0 0.0 collective-permute-done.3
  48.0 1.8 %collective-permute-done.4 = f32[16]{0:T(128)S(1)} collective-permute-done((f32[16]{0:T(128)S(1)}, f32[16]{0:T(128)S(1)}, u32[]{:S(2)}, u32[]{:S(2)}) %collective-permute-start.4) | collective-permute-done | bytes 96 | tf_op jit(solution)/shard_map/ppermute | solution.py:96
  49.8 0.2 collective-permute-done.5
  50.0 0.7 %add_convert_fusion = bf16[16,256]{1,0:T(8,128)(2,1)} fusion(f32[16,256]{1,0:T(8,128)S(1)} %multiply_reduce_fusion, f32[16,1024]{1,0:T(8,128)S(1)} %get-tuple-element.6, s32[]{:T(128)S(6)} %select_n.14, f32[256]{0:T(256)S(1)} %copy-done.10, f32[16]{0:T(128)S(1)} %add_rsqrt_fusion), kind=kLoop, calls=%fused_computation.44 | loop fusion | flops 16384 | bytes 42052 | tf_op jit(solution)/shard_map/convert_element_type | solution.py:85
  (23 shorter events, 0.1 us)
Async XLA Ops:
  0.0 5.9 %copy-start = (f32[16,1,128,256]{3,2,1,0:T(8,128)S(1)}, f32[16,1,128,256]{3,2,1,0:T(8,128)}, u32[]{:S(2)}) copy-start(f32[16,1,128,256]{3,2,1,0:T(8,128)} %param.22) | copy-start | bytes 6291460
  0.0 7.0 %copy-start.4 = (bf16[16,1024]{1,0:T(8,128)(2,1)S(1)}, bf16[16,1024]{1,0:T(8,128)(2,1)}, u32[]{:S(2)}) copy-start(bf16[16,1024]{1,0:T(8,128)(2,1)} %param.21) | copy-start | bytes 98308
  0.0 7.0 %copy-start.13 = (f32[1024]{0:T(1024)S(1)}, f32[1024]{0:T(1024)}, u32[]{:S(2)}) copy-start(f32[1024]{0:T(1024)} %param.24) | copy-start | bytes 12292
  0.0 7.0 %copy-start.14 = (f32[16,1]{0,1:T(1,128)S(1)}, f32[16,1]{0,1:T(1,128)}, u32[]{:S(2)}) copy-start(f32[16,1]{0,1:T(1,128)} %param.23) | copy-start | bytes 196
  0.0 7.0 %copy-start.12 = (bf16[1024,1]{0,1:T(2,128)(2,1)S(1)}, bf16[1024,1]{0,1:T(2,128)(2,1)}, u32[]{:S(2)}) copy-start(bf16[1024,1]{0,1:T(2,128)(2,1)} %param.29) | copy-start | bytes 6148
  0.0 7.3 %copy-start.11 = (bf16[1024,256]{1,0:T(8,128)(2,1)S(1)}, bf16[1024,256]{1,0:T(8,128)(2,1)}, u32[]{:S(2)}) copy-start(bf16[1024,256]{1,0:T(8,128)(2,1)} %param.27) | copy-start | bytes 1572868
  0.0 7.6 %copy-start.9 = (f32[256]{0:T(256)S(1)}, f32[256]{0:T(256)}, u32[]{:S(2)}) copy-start(f32[256]{0:T(256)} %param.32) | copy-start | bytes 3076
  0.0 7.6 %copy-start.2 = (bf16[256,1024]{1,0:T(8,128)(2,1)S(1)}, bf16[256,1024]{1,0:T(8,128)(2,1)}, u32[]{:S(2)}) copy-start(bf16[256,1024]{1,0:T(8,128)(2,1)} %param.33) | copy-start | bytes 1572868
  2.4 12.0 %copy-start.5 = (f32[1024]{0:T(1024)S(1)}, f32[1024]{0:T(1024)}, u32[]{:S(2)}) copy-start(f32[1024]{0:T(1024)} %param.34) | copy-start | bytes 12292
  3.6 11.0 %copy-start.6 = (f32[1024]{0:T(1024)S(1)}, f32[1024]{0:T(1024)}, u32[]{:S(2)}) copy-start(f32[1024]{0:T(1024)} %param.35) | copy-start | bytes 12292
  5.9 23.7 %copy-start.1 = (bf16[1,1024,256]{2,1,0:T(8,128)(2,1)S(1)}, bf16[1,1024,256]{2,1,0:T(8,128)(2,1)}, u32[]{:S(2)}) copy-start(bf16[1,1024,256]{2,1,0:T(8,128)(2,1)} %param.38) | copy-start | bytes 1572868
  7.0 22.8 %copy-start.3 = (bf16[1,256,1024]{2,1,0:T(8,128)(2,1)S(1)}, bf16[1,256,1024]{2,1,0:T(8,128)(2,1)}, u32[]{:S(2)}) copy-start(bf16[1,256,1024]{2,1,0:T(8,128)(2,1)} %param.40) | copy-start | bytes 1572868
  7.9 3.1 %collective-permute-start = (bf16[16,1024]{1,0:T(8,128)(2,1)S(1)}, bf16[16,1024]{1,0:T(8,128)(2,1)S(1)}, u32[]{:S(2)}, u32[]{:S(2)}) collective-permute-start(bf16[16,1024]{1,0:T(8,128)(2,1)S(1)} %convolution_convert_fusion.1), channel_id=1, source_target_pairs={{0,1},{1,0},{2,3},{3,2},{4,5},{5,4},{6,7},{7,6},{8,9},{9,8},{10,11... | collective-permute-start | bytes 98312 | tf_op jit(solution)/shard_map/ppermute | solution.py:96
  8.4 4.6 %collective-permute-start.1 = (bf16[16,1024]{1,0:T(8,128)(2,1)S(1)}, bf16[16,1024]{1,0:T(8,128)(2,1)S(1)}, u32[]{:S(2)}, u32[]{:S(2)}) collective-permute-start(bf16[16,1024]{1,0:T(8,128)(2,1)S(1)} %convolution_convert_fusion.1), channel_id=1, source_target_pairs={{0,2},{1,3},{2,0},{3,1},{4,6},{5,7},{6,4},{7,5},{8,10},{9,11},{10,... | collective-permute-start | bytes 98312 | tf_op jit(solution)/shard_map/ppermute | solution.py:96
  10.9 3.3 %collective-permute-start.2 = (bf16[16,1024]{1,0:T(8,128)(2,1)S(1)}, bf16[16,1024]{1,0:T(8,128)(2,1)S(1)}, u32[]{:S(2)}, u32[]{:S(2)}) collective-permute-start(bf16[16,1024]{1,0:T(8,128)(2,1)S(1)} %convolution_convert_fusion.1), channel_id=1, source_target_pairs={{0,3},{1,2},{2,1},{3,0},{4,7},{5,6},{6,5},{7,4},{8,11},{9,10},{10,... | collective-permute-start | bytes 98312 | tf_op jit(solution)/shard_map/ppermute | solution.py:96
  29.6 5.7 %copy-start.7 = (f32[16,6]{0,1:T(8,128)S(1)}, f32[16,6]{0,1:T(8,128)}, u32[]{:S(2)}) copy-start(f32[16,6]{0,1:T(8,128)} %param.37) | copy-start | bytes 1156
  29.6 5.7 %copy-start.8 = (s32[16,6]{0,1:T(8,128)S(1)}, s32[16,6]{0,1:T(8,128)}, u32[]{:S(2)}) copy-start(s32[16,6]{0,1:T(8,128)} %param.36) | copy-start | bytes 1156
  29.9 20.1 %copy-start.10 = (f32[256]{0:T(256)S(1)}, f32[256]{0:T(256)}, u32[]{:S(2)}) copy-start(f32[256]{0:T(256)} %param.41) | copy-start | bytes 3076
  32.3 13.5 %all-to-all-start.1 = ((bf16[32,16,256]{2,1,0:T(8,128)(2,1)}), bf16[32,16,256]{2,1,0:T(8,128)(2,1)S(1)}, u32[]{:S(2)}, u32[]{:S(2)}) async-start(bf16[32,16,256]{2,1,0:T(8,128)(2,1)} %bitcast.19), calls=%async_computation.1 | async-start | bytes 524288 | tf_op jit(solution)/shard_map/all_to_all | solution.py:116
  46.1 1.9 %collective-permute-start.3 = (f32[16]{0:T(128)S(1)}, f32[16]{0:T(128)S(1)}, u32[]{:S(2)}, u32[]{:S(2)}) collective-permute-start(f32[16]{0:T(128)S(1)} %multiply_reduce_fusion.3), channel_id=1, source_target_pairs={{0,1},{1,0},{2,3},{3,2},{4,5},{5,4},{6,7},{7,6},{8,9},{9,8},{10,11... | collective-permute-start | bytes 200 | tf_op jit(solution)/shard_map/ppermute | solution.py:96
  46.2 3.6 %collective-permute-start.4 = (f32[16]{0:T(128)S(1)}, f32[16]{0:T(128)S(1)}, u32[]{:S(2)}, u32[]{:S(2)}) collective-permute-start(f32[16]{0:T(128)S(1)} %multiply_reduce_fusion.3), channel_id=1, source_target_pairs={{0,2},{1,3},{2,0},{3,1},{4,6},{5,7},{6,4},{7,5},{8,10},{9,11},{10,... | collective-permute-start | bytes 200 | tf_op jit(solution)/shard_map/ppermute | solution.py:96
  47.0 3.0 %collective-permute-start.5 = (f32[16]{0:T(128)S(1)}, f32[16]{0:T(128)S(1)}, u32[]{:S(2)}, u32[]{:S(2)}) collective-permute-start(f32[16]{0:T(128)S(1)} %multiply_reduce_fusion.3), channel_id=1, source_target_pairs={{0,3},{1,2},{2,1},{3,0},{4,7},{5,6},{6,5},{7,4},{8,11},{9,10},{10,... | collective-permute-start | bytes 200 | tf_op jit(solution)/shard_map/ppermute | solution.py:96

commit v2 on v1

--- a/solution.py
+++ b/solution.py
@@ -1,6 +1,8 @@
 import jax
 import jax.numpy as jnp
 from jax import lax
+from jax.experimental import pallas as pl
+from jax.experimental.pallas import tpu as pltpu
 from jax.sharding import PartitionSpec as P
 
 EPS = 1e-06
@@ -36,37 +38,24 @@
     f32 = jnp.float32
     bf16 = jnp.bfloat16
     seqs, width = tokens.shape
-    heads = log_scale.shape[1]
-    key_dim = memory.shape[2]
-    value_dim = memory.shape[3]
-    xf = tokens.astype(f32)
-    normed = (xf * rms_scale(xf) * mix_gain_in).astype(bf16)
-    query = jnp.dot(normed, w_query, preferred_element_type=f32).reshape(
-        seqs, heads, key_dim
-    ) * key_dim ** (-0.5)
-    keys = jnp.dot(normed, w_key, preferred_element_type=f32).reshape(seqs, heads, key_dim)
-    values = jnp.dot(normed, w_value, preferred_element_type=f32).reshape(seqs, heads, value_dim)
-    in_pre = jnp.dot(normed, w_igate, preferred_element_type=f32) + igate_bias
-    forget_log = jax.nn.log_sigmoid(
-        jnp.dot(normed, w_fgate, preferred_element_type=f32) + fgate_bias
-    )
-    carried = forget_log + log_scale
-    new_max = jnp.maximum(carried, in_pre)
-    carry_weight = jnp.exp(carried - new_max)
-    fresh_weight = jnp.exp(in_pre - new_max)
-    recall = jnp.einsum("shk,shkv->shv", query, memory, precision=lax.Precision.HIGHEST)
-    match = jnp.sum(query * keys, axis=-1)
-    read = carry_weight[..., None] * recall + (fresh_weight * match)[..., None] * values
-    headout = (
-        (read * rms_scale(read) * head_gain.reshape(heads, value_dim))
-        .astype(bf16)
-        .reshape(seqs, heads * value_dim)
-    )
-    partial_value = jnp.dot(headout, w_output, preferred_element_type=f32)
-    mixed = sum_over(partial_value.astype(bf16), "tp")
-    resid = (xf + mixed * rms_scale(mixed) * mix_gain_out).astype(bf16)
+    partial_value = cell(
+        tokens,
+        memory,
+        log_scale,
+        mix_gain_in,
+        w_query,
+        w_key,
+        w_value,
+        w_igate,
+        w_fgate,
+        igate_bias,
+        fgate_bias,
+        head_gain,
+        w_output,
+    )
+    others = from_others(partial_value, "tp")
+    resid, ffn_in = after_mix([partial_value] + others, tokens, mix_gain_out, ffn_gain_in)
     rf = resid.astype(f32)
-    ffn_in = (rf * rms_scale(rf) * ffn_gain_in).astype(bf16)
     lanes = lax.axis_size("tp")
     groups = lax.axis_size("ep")
     quarter = width // lanes
@@ -85,16 +74,196 @@
     return (resid_part + scaled * ffn_gain_out).astype(bf16)
 
 
-def sum_over(value, axis):
+def from_others(value, axis):
     size = lax.axis_size(axis)
-    total = value.astype(jnp.float32)
+    received = []
     for step in range(1, size):
         if size & (size - 1) == 0:
             pairs = [(i, i ^ step) for i in range(size)]
         else:
             pairs = [(i, (i + step) % size) for i in range(size)]
-        total = total + lax.ppermute(value, axis, pairs).astype(jnp.float32)
-    return total
+        received.append(lax.ppermute(value, axis, pairs))
+    return received
+
+
+def sum_over(value, axis):
+    return sum(from_others(value, axis), value)
+
+
+def whole():
+    return pl.BlockSpec(memory_space=pltpu.VMEM)
+
+
+def cell_body(heads, key_dim, value_dim, chunk, *refs):
+    f32 = jnp.float32
+    bf16 = jnp.bfloat16
+    (tokens_h, gain_h, wi_h, wf_h, scale_h, wq_h, wk_h, wv_h, mem_h, hg_h, wo_h, ib, fb) = refs[:13]
+    out = refs[13]
+    (tokens, gain, wi, wf, scale, wq, wk, wv, mem, hg, wo, recall, sems) = refs[14:]
+    seqs = tokens.shape[0]
+    count = seqs // chunk
+    pieces = [
+        (tokens_h, tokens),
+        (gain_h, gain),
+        (wq_h, wq),
+        (wi_h, wi),
+        (wf_h, wf),
+        (scale_h, scale),
+        (wk_h, wk),
+    ]
+    for c in range(count):
+        rows = pl.ds(c * chunk, chunk)
+        pieces.append((mem_h.at[rows], mem.at[rows]))
+    pieces += [(wv_h, wv), (hg_h, hg), (wo_h, wo)]
+    copies = [pltpu.make_async_copy(src, dst, sems.at[i]) for i, (src, dst) in enumerate(pieces)]
+    for copy in copies:
+        copy.start()
+    copies[0].wait()
+    copies[1].wait()
+    xf = tokens[...].astype(f32)
+    inv = lax.rsqrt(jnp.mean(xf * xf, axis=1, keepdims=True) + EPS)
+    normed = (xf * inv * gain[...]).astype(bf16)
+    copies[2].wait()
+    query = jnp.dot(normed, wq[...], preferred_element_type=f32) * key_dim ** (-0.5)
+    for i in (3, 4, 5):
+        copies[i].wait()
+    wide = normed.astype(f32)
+    diagonal = lax.broadcasted_iota(jnp.int32, (seqs, seqs), 0) == lax.broadcasted_iota(
+        jnp.int32, (seqs, seqs), 1
+    )
+    carries, fresh = [], []
+    for h in range(heads):
+        in_pre = jnp.sum(wide * wi[h : h + 1, :].astype(f32), axis=1, keepdims=True) + ib[h]
+        forget = jnp.sum(wide * wf[h : h + 1, :].astype(f32), axis=1, keepdims=True) + fb[h]
+        forget_log = jnp.minimum(forget, 0.0) - jnp.log1p(jnp.exp(-jnp.abs(forget)))
+        column = jnp.sum(jnp.where(diagonal, scale[h : h + 1, :], 0.0), axis=1, keepdims=True)
+        carried = forget_log + column
+        new_max = jnp.maximum(carried, in_pre)
+        carries.append(jnp.exp(carried - new_max))
+        fresh.append(jnp.exp(in_pre - new_max))
+    copies[6].wait()
+    keys = jnp.dot(normed, wk[...], preferred_element_type=f32)
+    turned = [query[:, h * key_dim : (h + 1) * key_dim].T for h in range(heads)]
+    for c in range(count):
+        copies[7 + c].wait()
+        for b in range(c * chunk, (c + 1) * chunk):
+            for h in range(heads):
+                product = turned[h][:, b : b + 1] * mem[b, h]
+                recall[h, b : b + 1, :] = jnp.sum(product, axis=0, keepdims=True)
+    copies[7 + count].wait()
+    values = jnp.dot(normed, wv[...], preferred_element_type=f32)
+    copies[8 + count].wait()
+    parts = []
+    for h in range(heads):
+        ks = slice(h * key_dim, (h + 1) * key_dim)
+        vs = slice(h * value_dim, (h + 1) * value_dim)
+        match = jnp.sum(query[:, ks] * keys[:, ks], axis=1, keepdims=True)
+        read = carries[h] * recall[h] + (fresh[h] * match) * values[:, vs]
+        inv = lax.rsqrt(jnp.mean(read * read, axis=1, keepdims=True) + EPS)
+        parts.append((read * inv * hg[:, vs]).astype(bf16))
+    copies[9 + count].wait()
+    headout = parts[0] if heads == 1 else jnp.concatenate(parts, axis=1)
+    out[...] = jnp.dot(headout, wo[...], preferred_element_type=f32).astype(bf16)
+
+
+def cell(
+    tokens,
+    memory,
+    log_scale,
+    mix_gain_in,
+    w_query,
+    w_key,
+    w_value,
+    w_igate,
+    w_fgate,
+    igate_bias,
+    fgate_bias,
+    head_gain,
+    w_output,
+):
+    f32 = jnp.float32
+    bf16 = jnp.bfloat16
+    seqs, width = tokens.shape
+    heads, key_dim, value_dim = memory.shape[1:]
+    chunk = 4 if seqs % 4 == 0 else 1
+    body = lambda *refs: cell_body(heads, key_dim, value_dim, chunk, *refs)
+    operands = [
+        tokens,
+        mix_gain_in.reshape(1, width),
+        w_igate.T,
+        w_fgate.T,
+        log_scale.T,
+        w_query,
+        w_key,
+        w_value,
+        memory,
+        head_gain.reshape(1, heads * value_dim),
+        w_output,
+    ]
+    return pl.pallas_call(
+        body,
+        out_shape=jax.ShapeDtypeStruct((seqs, w_output.shape[1]), bf16),
+        in_specs=[pl.BlockSpec(memory_space=pltpu.HBM)] * len(operands)
+        + [pl.BlockSpec(memory_space=pltpu.SMEM)] * 2,
+        out_specs=whole(),
+        scratch_shapes=[pltpu.VMEM(o.shape, o.dtype) for o in operands]
+        + [
+            pltpu.VMEM((heads, seqs, value_dim), f32),
+            pltpu.SemaphoreType.DMA((10 + seqs // chunk,)),
+        ],
+        name="cell",
+    )(*operands, igate_bias, fgate_bias)
+
+
+def after_mix_body(count, *refs):
+    f32 = jnp.float32
+    bf16 = jnp.bfloat16
+    parts = refs[:count]
+    tokens, gain_out, gain_in, resid, ffn_in = refs[count:]
+    mixed = parts[0][...].astype(f32)
+    for part in parts[1:]:
+        mixed = mixed + part[...].astype(f32)
+    kept = (tokens[...].astype(f32) + mixed * rms_scale(mixed) * gain_out[...]).astype(bf16)
+    resid[...] = kept
+    rf = kept.astype(f32)
+    ffn_in[...] = (rf * rms_scale(rf) * gain_in[...]).astype(bf16)
+
+
+def after_mix(parts, tokens, gain_out, gain_in):
+    width = tokens.shape[1]
+    shape = jax.ShapeDtypeStruct(tokens.shape, jnp.bfloat16)
+    return pl.pallas_call(
+        lambda *refs: after_mix_body(len(parts), *refs),
+        out_shape=(shape, shape),
+        in_specs=[whole()] * (len(parts) + 3),
+        out_specs=(whole(), whole()),
+        name="after_mix",
+    )(*parts, tokens, gain_out.reshape(1, width), gain_in.reshape(1, width))
+
+
+def expert_body(groups, seqs, lanes, quarter, rows, gate_w, up_w, down_w, out):
+    f32 = jnp.float32
+    bf16 = jnp.bfloat16
+    gate = jnp.dot(rows[...], gate_w[...], preferred_element_type=f32)
+    up = jnp.dot(rows[...], up_w[...], preferred_element_type=f32)
+    act = (gate * jax.nn.sigmoid(gate) * up).astype(bf16)
+    for q in range(lanes):
+        columns = slice(q * quarter, (q + 1) * quarter)
+        part = jnp.dot(act, down_w[:, columns], preferred_element_type=f32).astype(bf16)
+        for g in range(groups):
+            out[g * lanes + q] = part[g * seqs : (g + 1) * seqs]
+
+
+def expert(rows, gate_w, up_w, down_w, groups, lanes):
+    seqs = rows.shape[0] // groups
+    quarter = rows.shape[1] // lanes
+    return pl.pallas_call(
+        lambda *refs: expert_body(groups, seqs, lanes, quarter, *refs),
+        out_shape=jax.ShapeDtypeStruct((groups * lanes, seqs, quarter), jnp.bfloat16),
+        in_specs=[whole()] * 4,
+        out_specs=whole(),
+        name="expert",
+    )(rows, gate_w, up_w, down_w)
 
 
 def every_token(ffn_in, routes, route_weights, expert_gate, expert_up, expert_down):
@@ -107,12 +276,7 @@
     spread = jnp.broadcast_to(ffn_in[None], (groups, seqs, width))
     rows = lax.all_to_all(spread, "ep", split_axis=0, concat_axis=0, tiled=True)
     rows = rows.reshape(groups * seqs, width)
-    gate = jnp.dot(rows, expert_gate[0], preferred_element_type=f32)
-    up = jnp.dot(rows, expert_up[0], preferred_element_type=f32)
-    act = (jax.nn.silu(gate) * up).astype(bf16)
-    part = jnp.dot(act, expert_down[0], preferred_element_type=f32).astype(bf16)
-    blocks = part.reshape(groups, seqs, lanes, quarter).transpose(0, 2, 1, 3)
-    blocks = blocks.reshape(groups * lanes, seqs, quarter)
+    blocks = expert(rows, expert_gate[0], expert_up[0], expert_down[0], groups, lanes)
     back = lax.all_to_all(blocks, ("ep", "tp"), split_axis=0, concat_axis=0, tiled=True)
     back = back.reshape(groups, lanes, seqs, quarter).astype(f32)
     done = jnp.sum(back, axis=1).astype(bf16).astype(f32)

time: 51 us -> 51.6 us (1.012)
  Pallas kernels: 0 us -> 7.69 us
  matrix products: 7.14 us -> 0 us
  other arithmetic: 2.4 us -> 1.63 us
    pallas_call x0 -> x3, Pallas kernels: none -> 7.69 us  [the longest x1 3.42 us: cell(): pl.pallas_call(body, out_shape=jax.ShapeDtypeStruct((seqs, w_output.shape...]
    dot_general x9 -> x0, matrix products: 7.14 us -> none  [the longest x1 1.55 us: every_token(): part = jnp.dot(act, expert_down[0], preferred_element_type=f32).astype(bf16)]
    reduce_sum x3 -> x0, other arithmetic: 1.36 us -> none  [rms_scale(): return lax.rsqrt(jnp.mean(values * values, axis=-1, keepdims=True) + EPS)]
    reshape x2 -> x0, local copies, waits for them, and re-layouts: 0.9 us -> none  [every_token(): blocks = part.reshape(groups, seqs, lanes, quarter).transpose(0, 2, 1, 3)]
    broadcast_in_dim x1, local copies, waits for them, and re-layouts: 0.02 us -> 0.77 us  [every_token(): spread = jnp.broadcast_to(ffn_in[None], (groups, seqs, width))]
    convert_element_type x1, other arithmetic: 0.68 us -> 1.38 us  [per_device(): return (resid_part + scaled * ffn_gain_out).astype(bf16)]
    unnamed x30 -> x12, local copies, waits for them, and re-layouts: 0.06 us -> 0.63 us
where the time goes in v2:
time: 51.6 us; the launch traced here: 51.1 us
  waiting for transfers between devices  16 us (31%)
  blocking collectives  14.9 us (29%)
  starting transfers between devices  8.06 us (16%)
  Pallas kernels  7.69 us (15%)
  other arithmetic  1.63 us (3%)
  local copies, waits for them, and re-layouts  1.4 us (3%)
  between operations  1.4 us (3%)
    all_to_all x1, blocking collectives, every_token(): rows = lax.all_to_all(spread, 'ep', split_axis=0, concat_axis=0, tiled=True)  14.9 us
    all_to_all x1, waiting for transfers between devices, every_token(): lax.all_to_all(blocks, ('ep', 'tp'), split_axis=0, concat_axis=0, tiled=T...  10.5 us
    ppermute x6, waiting for transfers between devices, from_others(): received.append(lax.ppermute(value, axis, pairs))  5.48 us
    ppermute x6, starting transfers between devices, from_others(): received.append(lax.ppermute(value, axis, pairs))  5.09 us
    pallas_call x1, Pallas kernels, cell(): pl.pallas_call(body, out_shape=jax.ShapeDtypeStruct((seqs, w_output.shape...  3.42 us
    all_to_all x1, starting transfers between devices, every_token(): lax.all_to_all(blocks, ('ep', 'tp'), split_axis=0, concat_axis=0, tiled=T...  2.97 us
    pallas_call x1, Pallas kernels, expert(): pl.pallas_call(lambda *refs: expert_body(groups, seqs, lanes, quarter, *r...  2.62 us
    pallas_call x1, Pallas kernels, after_mix(): pl.pallas_call(lambda *refs: after_mix_body(len(parts), *refs), out_shape...  1.65 us
  transfers between devices with their start and end apart: 7, of which 5 were waited for; matrix products, arithmetic and copies ran while one was open for 0% of the time, Pallas kernels for 0%

profile of v2, /device:TPU:0, one launch (start us, length us, event | category | flops | bytes accessed | tf_op | source)
XLA Modules:
  0.0 51.1 jit_solution(16271884522070890049)
XLA Ops:
  1.3 3.4 %cell.1.refs_0_ = bf16[16,1024]{1,0:T(8,128)(2,1)} custom-call(bf16[16,1024]{1,0:T(8,128)(2,1)} %refs_4_.1, f32[1,1024]{1,0:T(1,128)} %bitcast.21, bf16[1,1024]{1,0:T(2,128)(2,1)} %bitcast.22, bf16[1,1024]{1,0:T(2,128)(2,1)} %bitcast.23, f32[1,16]{1,0:T(1,128)} %bitcast.25, bf16[1024,128]{1,0:T(8,128)(2,1)} %refs_5_.1, bf16[1024,128]{1,0:T(8,128)(2,1)} %refs_6_.1, ...), custom_call_target="tpu_custom_call" | custom-call | tf_op jit(solution)/shard_map/cell/pallas_call | solution.py:203
  4.7 0.0 copy-start.3
  4.7 0.0 copy-start.4
  4.7 0.0 copy-start.5
  4.8 0.6 %collective-permute-start = (bf16[16,1024]{1,0:T(8,128)(2,1)}, bf16[16,1024]{1,0:T(8,128)(2,1)S(1)}, u32[]{:S(2)}, u32[]{:S(2)}) collective-permute-start(bf16[16,1024]{1,0:T(8,128)(2,1)} %cell.1.refs_0_), channel_id=1, source_target_pairs={{0,1},{1,0},{2,3},{3,2},{4,5},{5,4},{6,7},{7,6},{8,9},{9,8},{10,11... | collective-permute-start | bytes 98312 | tf_op jit(solution)/shard_map/ppermute | solution.py:85
  5.3 2.6 %collective-permute-start.1 = (bf16[16,1024]{1,0:T(8,128)(2,1)}, bf16[16,1024]{1,0:T(8,128)(2,1)S(1)}, u32[]{:S(2)}, u32[]{:S(2)}) collective-permute-start(bf16[16,1024]{1,0:T(8,128)(2,1)} %cell.1.refs_0_), channel_id=1, source_target_pairs={{0,2},{1,3},{2,0},{3,1},{4,6},{5,7},{6,4},{7,5},{8,10},{9,11},{10,... | collective-permute-start | bytes 98312 | tf_op jit(solution)/shard_map/ppermute | solution.py:85
  7.9 0.0 collective-permute-start.2
  7.9 0.0 collective-permute-done.refs_1_
  7.9 0.0 copy-start
  7.9 2.1 %collective-permute-done.1.refs_2_ = bf16[16,1024]{1,0:T(8,128)(2,1)S(1)} collective-permute-done((bf16[16,1024]{1,0:T(8,128)(2,1)}, bf16[16,1024]{1,0:T(8,128)(2,1)S(1)}, u32[]{:S(2)}, u32[]{:S(2)}) %collective-permute-start.1) | collective-permute-done | bytes 32800 | tf_op jit(solution)/shard_map/ppermute | solution.py:85
  10.1 0.0 copy-start.1
  10.1 1.4 %collective-permute-done.2.refs_3_ = bf16[16,1024]{1,0:T(8,128)(2,1)S(1)} collective-permute-done((bf16[16,1024]{1,0:T(8,128)(2,1)}, bf16[16,1024]{1,0:T(8,128)(2,1)S(1)}, u32[]{:S(2)}, u32[]{:S(2)}) %collective-permute-start.2) | collective-permute-done | bytes 32800 | tf_op jit(solution)/shard_map/ppermute | solution.py:85
  11.5 0.0 copy-start.2
  11.5 0.0 copy-done
  11.5 0.0 copy-done.1
  11.5 0.6 %copy-done.2 = bf16[16,1024]{1,0:T(8,128)(2,1)} copy-done((bf16[16,1024]{1,0:T(8,128)(2,1)}, bf16[16,1024]{1,0:T(8,128)(2,1)S(1)}, u32[]{:S(2)}) %copy-start.2) | copy-done | bytes 32792
  12.1 1.7 %after_mix.1 = (bf16[16,1024]{1,0:T(8,128)(2,1)}, bf16[16,1024]{1,0:T(8,128)(2,1)}) custom-call(bf16[16,1024]{1,0:T(8,128)(2,1)} %cell.1.refs_0_, bf16[16,1024]{1,0:T(8,128)(2,1)} %copy-done, bf16[16,1024]{1,0:T(8,128)(2,1)} %copy-done.1, bf16[16,1024]{1,0:T(8,128)(2,1)} %copy-done.2, bf16[16,1024]{1,0:T(8,128)(2,1)} %refs_4_.1, f32[1,1024]{1,0:T(1,128)} %bitcast.19, ...), custom_call_target="tpu_custom_call" | custom-call | tf_op jit(solution)/shard_map/after_mix/pallas_call | solution.py:235
  13.7 0.8 %broadcast_in_dim.16 = bf16[8,16,1024]{2,1,0:T(8,128)(2,1)S(1)} broadcast(bf16[16,1024]{1,0:T(8,128)(2,1)} %get-tuple-element.8), dimensions={1,2} | broadcast | bytes 294912 | tf_op jit(solution)/shard_map/broadcast_in_dim | solution.py:276
  14.5 14.9 %all_to_all.10 = bf16[8,16,1024]{2,1,0:T(8,128)(2,1)} all-to-all(bf16[8,16,1024]{2,1,0:T(8,128)(2,1)S(1)} %broadcast_in_dim.16), channel_id=1, replica_groups=mesh['ep'=8,'tp'=4] {'ep'}, dimensions={0} | all-to-all | bytes 524288 | tf_op jit(solution)/shard_map/all_to_all | solution.py:277
  29.5 2.6 %expert.1 = bf16[32,16,256]{2,1,0:T(8,128)(2,1)} custom-call(bf16[128,1024]{1,0:T(8,128)(2,1)} %bitcast.14, bf16[1024,256]{1,0:T(8,128)(2,1)} %bitcast.15, bf16[1024,256]{1,0:T(8,128)(2,1)} %bitcast.16, bf16[256,1024]{1,0:T(8,128)(2,1)} %bitcast.17), custom_call_target="tpu_custom_call" | custom-call | tf_op jit(solution)/shard_map/expert/pallas_call | solution.py:260
  32.1 3.0 %all-to-all-start.1 = ((bf16[32,16,256]{2,1,0:T(8,128)(2,1)}), bf16[32,16,256]{2,1,0:T(8,128)(2,1)S(1)}, u32[]{:S(2)}, u32[]{:S(2)}) async-start(bf16[32,16,256]{2,1,0:T(8,128)(2,1)} %expert.1), calls=%async_computation.1 | async-start | bytes 524288 | tf_op jit(solution)/shard_map/all_to_all | solution.py:280
  35.1 0.0 copy-done.3
  35.1 0.0 copy-done.4
  35.1 10.5 %all-to-all-done.1 = bf16[32,16,256]{2,1,0:T(8,128)(2,1)S(1)} async-done(((bf16[32,16,256]{2,1,0:T(8,128)(2,1)}), bf16[32,16,256]{2,1,0:T(8,128)(2,1)S(1)}, u32[]{:S(2)}, u32[]{:S(2)}) %all-to-all-start.1) | async-done | bytes 262176 | tf_op jit(solution)/shard_map/all_to_all | solution.py:280
  45.7 0.1 multiply_reduce_fusion
  45.8 0.1 multiply_reduce_fusion.1
  45.9 0.1 collective-permute-start.3
  45.9 0.8 %collective-permute-start.4 = (f32[16]{0:T(128)S(1)}, f32[16]{0:T(128)S(1)}, u32[]{:S(2)}, u32[]{:S(2)}) collective-permute-start(f32[16]{0:T(128)S(1)} %multiply_reduce_fusion.1), channel_id=1, source_target_pairs={{0,2},{1,3},{2,0},{3,1},{4,6},{5,7},{6,4},{7,5},{8,10},{9,11},{10,... | collective-permute-start | bytes 200 | tf_op jit(solution)/shard_map/ppermute | solution.py:85
  46.8 1.0 %collective-permute-start.5 = (f32[16]{0:T(128)S(1)}, f32[16]{0:T(128)S(1)}, u32[]{:S(2)}, u32[]{:S(2)}) collective-permute-start(f32[16]{0:T(128)S(1)} %multiply_reduce_fusion.1), channel_id=1, source_target_pairs={{0,3},{1,2},{2,1},{3,0},{4,7},{5,6},{6,5},{7,4},{8,11},{9,10},{10,... | collective-permute-start | bytes 200 | tf_op jit(solution)/shard_map/ppermute | solution.py:85
  47.8 0.0 collective-permute-done.3
  47.8 1.8 %collective-permute-done.4 = f32[16]{0:T(128)S(1)} collective-permute-done((f32[16]{0:T(128)S(1)}, f32[16]{0:T(128)S(1)}, u32[]{:S(2)}, u32[]{:S(2)}) %collective-permute-start.4) | collective-permute-done | bytes 96 | tf_op jit(solution)/shard_map/ppermute | solution.py:85
  49.6 0.2 collective-permute-done.5
  49.8 0.0 copy-done.5
  49.8 1.4 %add_convert_fusion = bf16[16,256]{1,0:T(8,128)(2,1)} fusion(f32[16,256]{1,0:T(8,128)S(1)} %multiply_reduce_fusion, bf16[16,1024]{1,0:T(8,128)(2,1)} %get-tuple-element.7, s32[]{:T(128)S(6)} %select_n.7, f32[256]{0:T(256)S(1)} %copy-done.5, f32[16]{0:T(128)S(1)} %add_rsqrt_fusion), kind=kLoop, calls=%fused_computation.4 | loop fusion | flops 20480 | bytes 33860 | tf_op jit(solution)/shard_map/convert_element_type | solution.py:74
  (3 shorter events, 0.1 us)
Async XLA Ops:
  4.7 30.3 %copy-start.3 = (f32[16,6]{0,1:T(8,128)S(1)}, f32[16,6]{0,1:T(8,128)}, u32[]{:S(2)}) copy-start(f32[16,6]{0,1:T(8,128)} %param.37) | copy-start | bytes 1156
  4.7 30.3 %copy-start.4 = (s32[16,6]{0,1:T(8,128)S(1)}, s32[16,6]{0,1:T(8,128)}, u32[]{:S(2)}) copy-start(s32[16,6]{0,1:T(8,128)} %param.36) | copy-start | bytes 1156
  4.7 45.0 %copy-start.5 = (f32[256]{0:T(256)S(1)}, f32[256]{0:T(256)}, u32[]{:S(2)}) copy-start(f32[256]{0:T(256)} %param.41) | copy-start | bytes 3076
  4.8 3.2 %collective-permute-start = (bf16[16,1024]{1,0:T(8,128)(2,1)}, bf16[16,1024]{1,0:T(8,128)(2,1)S(1)}, u32[]{:S(2)}, u32[]{:S(2)}) collective-permute-start(bf16[16,1024]{1,0:T(8,128)(2,1)} %cell.1.refs_0_), channel_id=1, source_target_pairs={{0,1},{1,0},{2,3},{3,2},{4,5},{5,4},{6,7},{7,6},{8,9},{9,8},{10,11... | collective-permute-start | bytes 98312 | tf_op jit(solution)/shard_map/ppermute | solution.py:85
  5.3 4.8 %collective-permute-start.1 = (bf16[16,1024]{1,0:T(8,128)(2,1)}, bf16[16,1024]{1,0:T(8,128)(2,1)S(1)}, u32[]{:S(2)}, u32[]{:S(2)}) collective-permute-start(bf16[16,1024]{1,0:T(8,128)(2,1)} %cell.1.refs_0_), channel_id=1, source_target_pairs={{0,2},{1,3},{2,0},{3,1},{4,6},{5,7},{6,4},{7,5},{8,10},{9,11},{10,... | collective-permute-start | bytes 98312 | tf_op jit(solution)/shard_map/ppermute | solution.py:85
  7.9 3.6 %collective-permute-start.2 = (bf16[16,1024]{1,0:T(8,128)(2,1)}, bf16[16,1024]{1,0:T(8,128)(2,1)S(1)}, u32[]{:S(2)}, u32[]{:S(2)}) collective-permute-start(bf16[16,1024]{1,0:T(8,128)(2,1)} %cell.1.refs_0_), channel_id=1, source_target_pairs={{0,3},{1,2},{2,1},{3,0},{4,7},{5,6},{6,5},{7,4},{8,11},{9,10},{10,... | collective-permute-start | bytes 98312 | tf_op jit(solution)/shard_map/ppermute | solution.py:85
  7.9 3.5 %copy-start = (bf16[16,1024]{1,0:T(8,128)(2,1)}, bf16[16,1024]{1,0:T(8,128)(2,1)S(1)}, u32[]{:S(2)}) copy-start(bf16[16,1024]{1,0:T(8,128)(2,1)S(1)} %collective-permute-done.refs_1_) | copy-start | bytes 98308
  10.1 1.4 %copy-start.1 = (bf16[16,1024]{1,0:T(8,128)(2,1)}, bf16[16,1024]{1,0:T(8,128)(2,1)S(1)}, u32[]{:S(2)}) copy-start(bf16[16,1024]{1,0:T(8,128)(2,1)S(1)} %collective-permute-done.1.refs_2_) | copy-start | bytes 98308
  11.5 0.6 %copy-start.2 = (bf16[16,1024]{1,0:T(8,128)(2,1)}, bf16[16,1024]{1,0:T(8,128)(2,1)S(1)}, u32[]{:S(2)}) copy-start(bf16[16,1024]{1,0:T(8,128)(2,1)S(1)} %collective-permute-done.2.refs_3_) | copy-start | bytes 98308
  32.1 13.5 %all-to-all-start.1 = ((bf16[32,16,256]{2,1,0:T(8,128)(2,1)}), bf16[32,16,256]{2,1,0:T(8,128)(2,1)S(1)}, u32[]{:S(2)}, u32[]{:S(2)}) async-start(bf16[32,16,256]{2,1,0:T(8,128)(2,1)} %expert.1), calls=%async_computation.1 | async-start | bytes 524288 | tf_op jit(solution)/shard_map/all_to_all | solution.py:280
  45.9 1.9 %collective-permute-start.3 = (f32[16]{0:T(128)S(1)}, f32[16]{0:T(128)S(1)}, u32[]{:S(2)}, u32[]{:S(2)}) collective-permute-start(f32[16]{0:T(128)S(1)} %multiply_reduce_fusion.1), channel_id=1, source_target_pairs={{0,1},{1,0},{2,3},{3,2},{4,5},{5,4},{6,7},{7,6},{8,9},{9,8},{10,11... | collective-permute-start | bytes 200 | tf_op jit(solution)/shard_map/ppermute | solution.py:85
  45.9 3.6 %collective-permute-start.4 = (f32[16]{0:T(128)S(1)}, f32[16]{0:T(128)S(1)}, u32[]{:S(2)}, u32[]{:S(2)}) collective-permute-start(f32[16]{0:T(128)S(1)} %multiply_reduce_fusion.1), channel_id=1, source_target_pairs={{0,2},{1,3},{2,0},{3,1},{4,6},{5,7},{6,4},{7,5},{8,10},{9,11},{10,... | collective-permute-start | bytes 200 | tf_op jit(solution)/shard_map/ppermute | solution.py:85
  46.8 3.0 %collective-permute-start.5 = (f32[16]{0:T(128)S(1)}, f32[16]{0:T(128)S(1)}, u32[]{:S(2)}, u32[]{:S(2)}) collective-permute-start(f32[16]{0:T(128)S(1)} %multiply_reduce_fusion.1), channel_id=1, source_target_pairs={{0,3},{1,2},{2,1},{3,0},{4,7},{5,6},{6,5},{7,4},{8,11},{9,10},{10,... | collective-permute-start | bytes 200 | tf_op jit(solution)/shard_map/ppermute | solution.py:85

commit v3 on v2

--- a/solution.py
+++ b/solution.py
@@ -54,12 +54,12 @@
         w_output,
     )
     others = from_others(partial_value, "tp")
-    resid, ffn_in = after_mix([partial_value] + others, tokens, mix_gain_out, ffn_gain_in)
-    rf = resid.astype(f32)
     lanes = lax.axis_size("tp")
     groups = lax.axis_size("ep")
-    quarter = width // lanes
-    own = lax.axis_index("tp") * quarter
+    own = lax.axis_index("tp").astype(jnp.int32).reshape(1)
+    resid_part, ffn_in = after_mix(
+        own, [partial_value] + others, tokens, mix_gain_out, ffn_gain_in, lanes
+    )
     local_experts = expert_gate.shape[0]
     experts_all = local_experts * groups
     top = routes.shape[1]
@@ -68,10 +68,9 @@
         routed = every_token(ffn_in, routes, route_weights, expert_gate, expert_up, expert_down)
     else:
         routed = slotted(ffn_in, routes, route_weights, expert_gate, expert_up, expert_down, cap)
-    resid_part = lax.dynamic_slice_in_dim(rf, own, quarter, 1)
     total = sum_over(jnp.sum(routed * routed, axis=1), "tp")
     scaled = routed * lax.rsqrt(total / width + EPS)[:, None]
-    return (resid_part + scaled * ffn_gain_out).astype(bf16)
+    return (resid_part.astype(f32) + scaled * ffn_gain_out).astype(bf16)
 
 
 def from_others(value, axis):
@@ -211,15 +210,16 @@
             pltpu.VMEM((heads, seqs, value_dim), f32),
             pltpu.SemaphoreType.DMA((10 + seqs // chunk,)),
         ],
+        compiler_params=pltpu.CompilerParams(vmem_limit_bytes=12 << 20),
         name="cell",
-    )(*operands, igate_bias, fgate_bias)
-
-
-def after_mix_body(count, *refs):
+    )(*[pltpu.with_memory_space_constraint(o, pltpu.HBM) for o in operands], igate_bias, fgate_bias)
+
+
+def after_mix_body(count, quarter, own, *refs):
     f32 = jnp.float32
     bf16 = jnp.bfloat16
     parts = refs[:count]
-    tokens, gain_out, gain_in, resid, ffn_in = refs[count:]
+    tokens, gain_out, gain_in, resid_part, ffn_in, resid = refs[count:]
     mixed = parts[0][...].astype(f32)
     for part in parts[1:]:
         mixed = mixed + part[...].astype(f32)
@@ -227,18 +227,25 @@
     resid[...] = kept
     rf = kept.astype(f32)
     ffn_in[...] = (rf * rms_scale(rf) * gain_in[...]).astype(bf16)
-
-
-def after_mix(parts, tokens, gain_out, gain_in):
-    width = tokens.shape[1]
-    shape = jax.ShapeDtypeStruct(tokens.shape, jnp.bfloat16)
+    resid_part[...] = resid[:, pl.ds(pl.multiple_of(own[0] * quarter, quarter), quarter)]
+
+
+def after_mix(own, parts, tokens, gain_out, gain_in, lanes):
+    bf16 = jnp.bfloat16
+    seqs, width = tokens.shape
+    quarter = width // lanes
     return pl.pallas_call(
-        lambda *refs: after_mix_body(len(parts), *refs),
-        out_shape=(shape, shape),
-        in_specs=[whole()] * (len(parts) + 3),
+        lambda *refs: after_mix_body(len(parts), quarter, *refs),
+        out_shape=(
+            jax.ShapeDtypeStruct((seqs, quarter), bf16),
+            jax.ShapeDtypeStruct((seqs, width), bf16),
+        ),
+        in_specs=[pl.BlockSpec(memory_space=pltpu.SMEM)] + [whole()] * (len(parts) + 3),
         out_specs=(whole(), whole()),
+        scratch_shapes=[pltpu.VMEM((seqs, width), bf16)],
+        compiler_params=pltpu.CompilerParams(vmem_limit_bytes=8 << 20),
         name="after_mix",
-    )(*parts, tokens, gain_out.reshape(1, width), gain_in.reshape(1, width))
+    )(own, *parts, tokens, gain_out.reshape(1, width), gain_in.reshape(1, width))
 
 
 def expert_body(groups, seqs, lanes, quarter, rows, gate_w, up_w, down_w, out):
@@ -262,6 +269,7 @@
         out_shape=jax.ShapeDtypeStruct((groups * lanes, seqs, quarter), jnp.bfloat16),
         in_specs=[whole()] * 4,
         out_specs=whole(),
+        compiler_params=pltpu.CompilerParams(vmem_limit_bytes=12 << 20),
         name="expert",
     )(rows, gate_w, up_w, down_w)
 
@@ -273,16 +281,19 @@
     lanes = lax.axis_size("tp")
     groups = lax.axis_size("ep")
     quarter = width // lanes
+    named = routes[:, :, None] == jnp.arange(groups, dtype=jnp.int32)[None, None, :]
+    weights = jnp.sum(jnp.where(named, route_weights[:, :, None], 0.0), axis=1)
     spread = jnp.broadcast_to(ffn_in[None], (groups, seqs, width))
+    spread, weights, gate_w, up_w, down_w = lax.optimization_barrier(
+        (spread, weights.T, expert_gate[0], expert_up[0], expert_down[0])
+    )
     rows = lax.all_to_all(spread, "ep", split_axis=0, concat_axis=0, tiled=True)
     rows = rows.reshape(groups * seqs, width)
-    blocks = expert(rows, expert_gate[0], expert_up[0], expert_down[0], groups, lanes)
+    blocks = expert(rows, gate_w, up_w, down_w, groups, lanes)
     back = lax.all_to_all(blocks, ("ep", "tp"), split_axis=0, concat_axis=0, tiled=True)
     back = back.reshape(groups, lanes, seqs, quarter).astype(f32)
     done = jnp.sum(back, axis=1).astype(bf16).astype(f32)
-    named = routes[:, :, None] == jnp.arange(groups, dtype=jnp.int32)[None, None, :]
-    weights = jnp.sum(jnp.where(named, route_weights[:, :, None], 0.0), axis=1)
-    return jnp.sum(weights.T[:, :, None] * done, axis=0)
+    return jnp.sum(weights[:, :, None] * done, axis=0)
 
 
 def slotted(ffn_in, routes, route_weights, expert_gate, expert_up, expert_down, cap):

time: 51.6 us -> 45.1 us (0.87)
  blocking collectives: 14.9 us -> 28.3 us
  waiting for transfers between devices: 16 us -> 5.41 us
  Pallas kernels: 7.69 us -> 3.63 us
  starting transfers between devices: 8.06 us -> 5.1 us
  local copies, waits for them, and re-layouts: 1.4 us -> 0.06 us
  other arithmetic: 1.63 us -> 0.92 us
    all_to_all x0 -> x1, blocking collectives: none -> 13.8 us  [every_token(): lax.all_to_all(blocks, ('ep', 'tp'), split_axis=0, concat_axis=0, tiled=T...]
    all_to_all x1 -> x0, waiting for transfers between devices: 10.5 us -> none  [every_token(): lax.all_to_all(blocks, ('ep', 'tp'), split_axis=0, concat_axis=0, tiled=T...]
    all_to_all x1 -> x0, starting transfers between devices: 2.97 us -> none  [every_token(): lax.all_to_all(blocks, ('ep', 'tp'), split_axis=0, concat_axis=0, tiled=T...]
    pallas_call x1, Pallas kernels: 2.62 us -> 0.49 us  [expert(): pl.pallas_call(lambda *refs: expert_body(groups, seqs, lanes, quarter, *r...]
    pallas_call x1, Pallas kernels: 1.65 us -> 0.21 us  [after_mix(): pl.pallas_call(lambda *refs: after_mix_body(len(parts), quarter, *refs),...]
    broadcast_in_dim x1, local copies, waits for them, and re-layouts: 0.77 us -> 0.02 us  [every_token(): spread = jnp.broadcast_to(ffn_in[None], (groups, seqs, width))]
    convert_element_type x1, other arithmetic: 1.38 us -> 0.67 us  [per_device(): return (resid_part.astype(f32) + scaled * ffn_gain_out).astype(bf16)]
    unnamed x12 -> x18, local copies, waits for them, and re-layouts: 0.63 us -> 0.04 us
  transfers between devices with their start and end apart: 7 -> 6, of which waited for: 5 -> 4; matrix products, arithmetic and copies ran while one was open for 0% -> 0% of each run, Pallas kernels for 0% -> 0%
where the time goes in v3:
time: 45.1 us; the launch traced here: 44.9 us
  blocking collectives  28.3 us (63%)
  waiting for transfers between devices  5.41 us (12%)
  starting transfers between devices  5.1 us (11%)
  Pallas kernels  3.63 us (8%)
  between operations  1.48 us (3%)
  other arithmetic  0.92 us (2%)
    all_to_all x1, blocking collectives, every_token(): rows = lax.all_to_all(spread, 'ep', split_axis=0, concat_axis=0, tiled=True)  14.5 us
    all_to_all x1, blocking collectives, every_token(): lax.all_to_all(blocks, ('ep', 'tp'), split_axis=0, concat_axis=0, tiled=T...  13.8 us
    ppermute x6, waiting for transfers between devices, from_others(): received.append(lax.ppermute(value, axis, pairs))  5.41 us
    ppermute x6, starting transfers between devices, from_others(): received.append(lax.ppermute(value, axis, pairs))  5.1 us
    pallas_call x1, Pallas kernels, cell(): pl.pallas_call(body, out_shape=jax.ShapeDtypeStruct((seqs, w_output.shape...  2.93 us
  transfers between devices with their start and end apart: 6, of which 4 were waited for; matrix products, arithmetic and copies ran while one was open for 0% of the time, Pallas kernels for 0%

profile of v3, /device:TPU:0, one launch (start us, length us, event | category | flops | bytes accessed | tf_op | source)
XLA Modules:
  0.0 44.9 jit_solution(3076987457020470661)
XLA Ops:
  0.0 0.0 copy-start.3
  0.0 0.0 copy-start.6
  0.0 0.0 copy-start.7
  0.0 0.0 copy-start.5
  0.0 0.0 copy-start.4
  1.4 0.0 copy-start
  1.4 0.0 copy-start.1
  1.4 0.0 copy-start.2
  1.4 2.9 %cell.1.refs_1_ = bf16[16,1024]{1,0:T(8,128)(2,1)S(1)} custom-call(bf16[16,1024]{1,0:T(8,128)(2,1)} %refs_5_.3, f32[1,1024]{1,0:T(1,128)} %bitcast.22, bf16[1,1024]{1,0:T(2,128)(2,1)} %bitcast.23, bf16[1,1024]{1,0:T(2,128)(2,1)} %bitcast.24, f32[1,16]{1,0:T(1,128)} %bitcast.26, bf16[1024,128]{1,0:T(8,128)(2,1)} %refs_5_.2, bf16[1024,128]{1,0:T(8,128)(2,1)} %refs_6_.1, ...), custom_call_target="tpu_custom_call" | custom-call | tf_op jit(solution)/shard_map/cell/pallas_call | solution.py:202
  4.3 0.0 copy-start.8
  4.4 2.5 %collective-permute-start.2 = (bf16[16,1024]{1,0:T(8,128)(2,1)S(1)}, bf16[16,1024]{1,0:T(8,128)(2,1)S(1)}, u32[]{:S(2)}, u32[]{:S(2)}) collective-permute-start(bf16[16,1024]{1,0:T(8,128)(2,1)S(1)} %cell.1.refs_1_), channel_id=1, source_target_pairs={{0,3},{1,2},{2,1},{3,0},{4,7},{5,6},{6,5},{7,4},{8,11},{9,10},{10,... | collective-permute-start | bytes 98312 | tf_op jit(solution)/shard_map/ppermute | solution.py:84
  6.9 0.6 %collective-permute-start.1 = (bf16[16,1024]{1,0:T(8,128)(2,1)S(1)}, bf16[16,1024]{1,0:T(8,128)(2,1)S(1)}, u32[]{:S(2)}, u32[]{:S(2)}) collective-permute-start(bf16[16,1024]{1,0:T(8,128)(2,1)S(1)} %cell.1.refs_1_), channel_id=1, source_target_pairs={{0,2},{1,3},{2,0},{3,1},{4,6},{5,7},{6,4},{7,5},{8,10},{9,11},{10,... | collective-permute-start | bytes 98312 | tf_op jit(solution)/shard_map/ppermute | solution.py:84
  7.5 0.0 collective-permute-start
  7.5 0.0 copy-done.6
  7.5 0.0 copy-done.7
  7.6 1.1 %collective-permute-done.2.refs_4_ = bf16[16,1024]{1,0:T(8,128)(2,1)S(1)} collective-permute-done((bf16[16,1024]{1,0:T(8,128)(2,1)S(1)}, bf16[16,1024]{1,0:T(8,128)(2,1)S(1)}, u32[]{:S(2)}, u32[]{:S(2)}) %collective-permute-start.2) | collective-permute-done | bytes 32800 | tf_op jit(solution)/shard_map/ppermute | solution.py:84
  8.6 2.2 %collective-permute-done.1.refs_3_ = bf16[16,1024]{1,0:T(8,128)(2,1)S(1)} collective-permute-done((bf16[16,1024]{1,0:T(8,128)(2,1)S(1)}, bf16[16,1024]{1,0:T(8,128)(2,1)S(1)}, u32[]{:S(2)}, u32[]{:S(2)}) %collective-permute-start.1) | collective-permute-done | bytes 32800 | tf_op jit(solution)/shard_map/ppermute | solution.py:84
  10.8 0.0 collective-permute-done.refs_2_
  10.8 0.0 copy-done.3
  10.8 0.0 copy-done.5
  10.8 0.0 copy-done.4
  10.9 0.2 after_mix.1
  11.1 14.5 %all_to_all.10 = bf16[8,16,1024]{2,1,0:T(8,128)(2,1)S(1)} all-to-all(bf16[8,16,1024]{2,1,0:T(8,128)(2,1)S(1)} %broadcast_in_dim.14), channel_id=1, replica_groups=mesh['ep'=8,'tp'=4] {'ep'}, dimensions={0} | all-to-all | bytes 524288 | tf_op jit(solution)/shard_map/all_to_all | solution.py:290
  25.6 0.0 copy-done
  25.6 0.0 copy-done.1
  25.6 0.0 copy-done.2
  25.6 0.5 %expert.1 = bf16[32,16,256]{2,1,0:T(8,128)(2,1)S(1)} custom-call(bf16[128,1024]{1,0:T(8,128)(2,1)S(1)} %bitcast.15, bf16[1024,256]{1,0:T(8,128)(2,1)S(1)} %bitcast.16, bf16[1024,256]{1,0:T(8,128)(2,1)S(1)} %bitcast.17, bf16[256,1024]{1,0:T(8,128)(2,1)S(1)} %bitcast.18), custom_call_target="tpu_custom_call" | custom-call | tf_op jit(solution)/shard_map/expert/pallas_call | solution.py:267
  26.1 13.8 %all_to_all.11 = bf16[32,16,256]{2,1,0:T(8,128)(2,1)S(1)} all-to-all(bf16[32,16,256]{2,1,0:T(8,128)(2,1)S(1)} %expert.1), channel_id=1, replica_groups=mesh['ep'=8,'tp'=4] {'ep','tp'}, dimensions={0} | all-to-all | bytes 524288 | tf_op jit(solution)/shard_map/all_to_all | solution.py:293
  39.9 0.1 multiply_reduce_fusion
  40.0 0.1 multiply_reduce_fusion.1
  40.1 0.5 %collective-permute-start.5 = (f32[16]{0:T(128)S(1)}, f32[16]{0:T(128)S(1)}, u32[]{:S(2)}, u32[]{:S(2)}) collective-permute-start(f32[16]{0:T(128)S(1)} %multiply_reduce_fusion.1), channel_id=1, source_target_pairs={{0,3},{1,2},{2,1},{3,0},{4,7},{5,6},{6,5},{7,4},{8,11},{9,10},{10,... | collective-permute-start | bytes 200 | tf_op jit(solution)/shard_map/ppermute | solution.py:84
  40.6 1.1 %collective-permute-start.4 = (f32[16]{0:T(128)S(1)}, f32[16]{0:T(128)S(1)}, u32[]{:S(2)}, u32[]{:S(2)}) collective-permute-start(f32[16]{0:T(128)S(1)} %multiply_reduce_fusion.1), channel_id=1, source_target_pairs={{0,2},{1,3},{2,0},{3,1},{4,6},{5,7},{6,4},{7,5},{8,10},{9,11},{10,... | collective-permute-start | bytes 200 | tf_op jit(solution)/shard_map/ppermute | solution.py:84
  41.7 0.3 collective-permute-start.3
  42.0 1.1 %collective-permute-done.5 = f32[16]{0:T(128)S(1)} collective-permute-done((f32[16]{0:T(128)S(1)}, f32[16]{0:T(128)S(1)}, u32[]{:S(2)}, u32[]{:S(2)}) %collective-permute-start.5) | collective-permute-done | bytes 96 | tf_op jit(solution)/shard_map/ppermute | solution.py:84
  43.2 1.0 %collective-permute-done.4 = f32[16]{0:T(128)S(1)} collective-permute-done((f32[16]{0:T(128)S(1)}, f32[16]{0:T(128)S(1)}, u32[]{:S(2)}, u32[]{:S(2)}) %collective-permute-start.4) | collective-permute-done | bytes 96 | tf_op jit(solution)/shard_map/ppermute | solution.py:84
  44.2 0.0 collective-permute-done.3
  44.2 0.0 copy-done.8
  44.2 0.7 %add_convert_fusion = bf16[16,256]{1,0:T(8,128)(2,1)} fusion(f32[16,256]{1,0:T(8,128)S(1)} %multiply_reduce_fusion, bf16[16,256]{1,0:T(8,128)(2,1)S(1)} %get-tuple-element.12, f32[256]{0:T(256)S(1)} %copy-done.8, f32[16]{0:T(128)S(1)} %add_rsqrt_fusion), kind=kLoop, calls=%fused_computation.4 | loop fusion | flops 20480 | bytes 33856 | tf_op jit(solution)/shard_map/convert_element_type | solution.py:73
  (4 shorter events, 0.1 us)
Async XLA Ops:
  0.0 10.8 %copy-start.3 = (bf16[16,1024]{1,0:T(8,128)(2,1)S(1)}, bf16[16,1024]{1,0:T(8,128)(2,1)}, u32[]{:S(2)}) copy-start(bf16[16,1024]{1,0:T(8,128)(2,1)} %refs_5_.3) | copy-start | bytes 98308
  0.0 7.5 %copy-start.6 = (f32[16,6]{0,1:T(8,128)S(1)}, f32[16,6]{0,1:T(8,128)}, u32[]{:S(2)}) copy-start(f32[16,6]{0,1:T(8,128)} %param.37) | copy-start | bytes 1156
  0.0 7.5 %copy-start.7 = (s32[16,6]{0,1:T(8,128)S(1)}, s32[16,6]{0,1:T(8,128)}, u32[]{:S(2)}) copy-start(s32[16,6]{0,1:T(8,128)} %param.36) | copy-start | bytes 1156
  0.0 10.8 %copy-start.5 = (f32[1024]{0:T(1024)S(1)}, f32[1024]{0:T(1024)}, u32[]{:S(2)}) copy-start(f32[1024]{0:T(1024)} %param.35) | copy-start | bytes 12292
  0.0 10.8 %copy-start.4 = (f32[1024]{0:T(1024)S(1)}, f32[1024]{0:T(1024)}, u32[]{:S(2)}) copy-start(f32[1024]{0:T(1024)} %param.34) | copy-start | bytes 12292
  1.4 24.2 %copy-start = (bf16[1,1024,256]{2,1,0:T(8,128)(2,1)S(1)}, bf16[1,1024,256]{2,1,0:T(8,128)(2,1)}, u32[]{:S(2)}) copy-start(bf16[1,1024,256]{2,1,0:T(8,128)(2,1)} %param.38) | copy-start | bytes 1572868
  1.4 24.2 %copy-start.1 = (bf16[1,1024,256]{2,1,0:T(8,128)(2,1)S(1)}, bf16[1,1024,256]{2,1,0:T(8,128)(2,1)}, u32[]{:S(2)}) copy-start(bf16[1,1024,256]{2,1,0:T(8,128)(2,1)} %param.39) | copy-start | bytes 1572868
  1.4 24.2 %copy-start.2 = (bf16[1,256,1024]{2,1,0:T(8,128)(2,1)S(1)}, bf16[1,256,1024]{2,1,0:T(8,128)(2,1)}, u32[]{:S(2)}) copy-start(bf16[1,256,1024]{2,1,0:T(8,128)(2,1)} %param.40) | copy-start | bytes 1572868
  4.3 39.8 %copy-start.8 = (f32[256]{0:T(256)S(1)}, f32[256]{0:T(256)}, u32[]{:S(2)}) copy-start(f32[256]{0:T(256)} %param.41) | copy-start | bytes 3076
  4.4 4.3 %collective-permute-start.2 = (bf16[16,1024]{1,0:T(8,128)(2,1)S(1)}, bf16[16,1024]{1,0:T(8,128)(2,1)S(1)}, u32[]{:S(2)}, u32[]{:S(2)}) collective-permute-start(bf16[16,1024]{1,0:T(8,128)(2,1)S(1)} %cell.1.refs_1_), channel_id=1, source_target_pairs={{0,3},{1,2},{2,1},{3,0},{4,7},{5,6},{6,5},{7,4},{8,11},{9,10},{10,... | collective-permute-start | bytes 98312 | tf_op jit(solution)/shard_map/ppermute | solution.py:84
  6.9 4.0 %collective-permute-start.1 = (bf16[16,1024]{1,0:T(8,128)(2,1)S(1)}, bf16[16,1024]{1,0:T(8,128)(2,1)S(1)}, u32[]{:S(2)}, u32[]{:S(2)}) collective-permute-start(bf16[16,1024]{1,0:T(8,128)(2,1)S(1)} %cell.1.refs_1_), channel_id=1, source_target_pairs={{0,2},{1,3},{2,0},{3,1},{4,6},{5,7},{6,4},{7,5},{8,10},{9,11},{10,... | collective-permute-start | bytes 98312 | tf_op jit(solution)/shard_map/ppermute | solution.py:84
  7.5 3.3 %collective-permute-start = (bf16[16,1024]{1,0:T(8,128)(2,1)S(1)}, bf16[16,1024]{1,0:T(8,128)(2,1)S(1)}, u32[]{:S(2)}, u32[]{:S(2)}) collective-permute-start(bf16[16,1024]{1,0:T(8,128)(2,1)S(1)} %cell.1.refs_1_), channel_id=1, source_target_pairs={{0,1},{1,0},{2,3},{3,2},{4,5},{5,4},{6,7},{7,6},{8,9},{9,8},{10,11... | collective-permute-start | bytes 98312 | tf_op jit(solution)/shard_map/ppermute | solution.py:84
  40.1 3.1 %collective-permute-start.5 = (f32[16]{0:T(128)S(1)}, f32[16]{0:T(128)S(1)}, u32[]{:S(2)}, u32[]{:S(2)}) collective-permute-start(f32[16]{0:T(128)S(1)} %multiply_reduce_fusion.1), channel_id=1, source_target_pairs={{0,3},{1,2},{2,1},{3,0},{4,7},{5,6},{6,5},{7,4},{8,11},{9,10},{10,... | collective-permute-start | bytes 200 | tf_op jit(solution)/shard_map/ppermute | solution.py:84
  40.6 3.6 %collective-permute-start.4 = (f32[16]{0:T(128)S(1)}, f32[16]{0:T(128)S(1)}, u32[]{:S(2)}, u32[]{:S(2)}) collective-permute-start(f32[16]{0:T(128)S(1)} %multiply_reduce_fusion.1), channel_id=1, source_target_pairs={{0,2},{1,3},{2,0},{3,1},{4,6},{5,7},{6,4},{7,5},{8,10},{9,11},{10,... | collective-permute-start | bytes 200 | tf_op jit(solution)/shard_map/ppermute | solution.py:84
  41.7 2.5 %collective-permute-start.3 = (f32[16]{0:T(128)S(1)}, f32[16]{0:T(128)S(1)}, u32[]{:S(2)}, u32[]{:S(2)}) collective-permute-start(f32[16]{0:T(128)S(1)} %multiply_reduce_fusion.1), channel_id=1, source_target_pairs={{0,1},{1,0},{2,3},{3,2},{4,5},{5,4},{6,7},{7,6},{8,9},{9,8},{10,11... | collective-permute-start | bytes 200 | tf_op jit(solution)/shard_map/ppermute | solution.py:84

commit v4 on v2

v4 whole, which is shorter than its diff:
```python
import jax
import jax.numpy as jnp
from jax import lax
from jax.experimental import pallas as pl
from jax.experimental.pallas import tpu as pltpu
from jax.sharding import PartitionSpec as P

EPS = 1e-06


def rms_scale(values):
    return lax.rsqrt(jnp.mean(values * values, axis=-1, keepdims=True) + EPS)


def per_device(
    tokens,
    memory,
    log_scale,
    mix_gain_in,
    w_query,
    w_key,
    w_value,
    w_igate,
    w_fgate,
    igate_bias,
    fgate_bias,
    head_gain,
    w_output,
    mix_gain_out,
    ffn_gain_in,
    routes,
    route_weights,
    expert_gate,
    expert_up,
    expert_down,
    ffn_gain_out,
):
    f32 = jnp.float32
    bf16 = jnp.bfloat16
    seqs, width = tokens.shape
    lanes = lax.axis_size("tp")
    groups = lax.axis_size("ep")
    local_experts = expert_gate.shape[0]
    experts_all = local_experts * groups
    top = routes.shape[1]
    cap = min(seqs, max(2, 3 * seqs * top // (2 * experts_all)))
    dense = cap == seqs and local_experts == 1 and lanes == 4 and seqs % 16 == 0
    partial_value = cell(
        tokens,
        memory,
        log_scale,
        mix_gain_in,
        w_query,
        w_key,
        w_value,
        w_igate,
        w_fgate,
        igate_bias,
        fgate_bias,
        head_gain,
        w_output,
        dense,
    )
    if dense:
        return every_token(
            partial_value,
            tokens,
            mix_gain_out,
            ffn_gain_in,
            routes,
            route_weights,
            expert_gate,
            expert_up,
            expert_down,
            ffn_gain_out,
        )
    quarter = width // lanes
    own = lax.axis_index("tp") * quarter
    mixed = sum_over(partial_value, "tp")
    resid = (tokens.astype(f32) + mixed * rms_scale(mixed) * mix_gain_out).astype(bf16)
    rf = resid.astype(f32)
    ffn_in = (rf * rms_scale(rf) * ffn_gain_in).astype(bf16)
    routed = slotted(ffn_in, routes, route_weights, expert_gate, expert_up, expert_down, cap)
    resid_part = lax.dynamic_slice_in_dim(rf, own, quarter, 1)
    total = sum_over(jnp.sum(routed * routed, axis=1), "tp")
    scaled = routed * lax.rsqrt(total / width + EPS)[:, None]
    return (resid_part + scaled * ffn_gain_out).astype(bf16)


def exchange(value, axis, step):
    size = lax.axis_size(axis)
    if size & (size - 1) == 0:
        pairs = [(i, i ^ step) for i in range(size)]
    else:
        pairs = [(i, (i + step) % size) for i in range(size)]
    return lax.ppermute(value, axis, pairs)


def sum_over(value, axis):
    total = value.astype(jnp.float32)
    for step in range(1, lax.axis_size(axis)):
        total = total + exchange(value, axis, step).astype(jnp.float32)
    return total


def whole():
    return pl.BlockSpec(memory_space=pltpu.VMEM)


def cell_body(heads, key_dim, value_dim, chunk, halves, *refs):
    f32 = jnp.float32
    bf16 = jnp.bfloat16
    sources, outs, rest = refs[:13], refs[13 : 14 + halves], refs[14 + halves :]
    targets, (recall, sems) = rest[:13], rest[13:]
    (tokens, gain, wi, wf, ib, fb, scale, wq, wk, wv, mem, hg, wo) = targets
    seqs = tokens.shape[0]
    count = seqs // chunk
    pairs = list(zip(sources, targets))
    pieces = [pairs[i] for i in (0, 1, 7, 2, 3, 4, 5, 6, 8)]
    for c in range(count):
        rows = pl.ds(c * chunk, chunk)
        pieces.append((pairs[10][0].at[rows], mem.at[rows]))
    pieces += [pairs[9], pairs[11], pairs[12]]
    copies = [pltpu.make_async_copy(src, dst, sems.at[i]) for i, (src, dst) in enumerate(pieces)]
    for copy in copies:
        copy.start()
    copies[0].wait()
    copies[1].wait()
    xf = tokens[...].astype(f32)
    inv = lax.rsqrt(jnp.mean(xf * xf, axis=1, keepdims=True) + EPS)
    normed = (xf * inv * gain[...]).astype(bf16)
    copies[2].wait()
    query = jnp.dot(normed, wq[...], preferred_element_type=f32) * key_dim ** (-0.5)
    for i in range(3, 8):
        copies[i].wait()
    wide = normed.astype(f32)
    diagonal = lax.broadcasted_iota(jnp.int32, (seqs, seqs), 0) == lax.broadcasted_iota(
        jnp.int32, (seqs, seqs), 1
    )
    carries, fresh = [], []
    for h in range(heads):
        in_pre = jnp.sum(wide * wi[h : h + 1, :].astype(f32), axis=1, keepdims=True) + ib[:, h : h + 1]
        forget = jnp.sum(wide * wf[h : h + 1, :].astype(f32), axis=1, keepdims=True) + fb[:, h : h + 1]
        forget_log = jnp.minimum(forget, 0.0) - jnp.log1p(jnp.exp(-jnp.abs(forget)))
        column = jnp.sum(jnp.where(diagonal, scale[h : h + 1, :], 0.0), axis=1, keepdims=True)
        carried = forget_log + column
        new_max = jnp.maximum(carried, in_pre)
        carries.append(jnp.exp(carried - new_max))
        fresh.append(jnp.exp(in_pre - new_max))
    copies[8].wait()
    keys = jnp.dot(normed, wk[...], preferred_element_type=f32)
    turned = [query[:, h * key_dim : (h + 1) * key_dim].T for h in range(heads)]
    for c in range(count):
        copies[9 + c].wait()
        for b in range(c * chunk, (c + 1) * chunk):
            for h in range(heads):
                product = turned[h][:, b : b + 1] * mem[b, h]
                recall[h, b : b + 1, :] = jnp.sum(product, axis=0, keepdims=True)
    copies[9 + count].wait()
    copies[10 + count].wait()
    values = jnp.dot(normed, wv[...], preferred_element_type=f32)
    parts = []
    for h in range(heads):
        ks = slice(h * key_dim, (h + 1) * key_dim)
        vs = slice(h * value_dim, (h + 1) * value_dim)
        match = jnp.sum(query[:, ks] * keys[:, ks], axis=1, keepdims=True)
        read = carries[h] * recall[h] + (fresh[h] * match) * values[:, vs]
        inv = lax.rsqrt(jnp.mean(read * read, axis=1, keepdims=True) + EPS)
        parts.append((read * inv * hg[:, vs]).astype(bf16))
    copies[11 + count].wait()
    headout = parts[0] if heads == 1 else jnp.concatenate(parts, axis=1)
    product = jnp.dot(headout, wo[...], preferred_element_type=f32)
    if halves:
        low, high = product[: seqs // 2], product[seqs // 2 :]
        odd = lax.axis_index("tp") % 2 == 1
        outs[0][...] = jnp.where(odd, high, low).astype(bf16)
        outs[1][...] = jnp.where(odd, low, high).astype(bf16)
    else:
        outs[0][...] = product.astype(bf16)


def cell(
    tokens,
    memory,
    log_scale,
    mix_gain_in,
    w_query,
    w_key,
    w_value,
    w_igate,
    w_fgate,
    igate_bias,
    fgate_bias,
    head_gain,
    w_output,
    halves,
):
    f32 = jnp.float32
    bf16 = jnp.bfloat16
    seqs, width = tokens.shape
    heads, key_dim, value_dim = memory.shape[1:]
    chunk = 4 if seqs % 4 == 0 else 1
    body = lambda *refs: cell_body(heads, key_dim, value_dim, chunk, halves, *refs)
    operands = [
        tokens,
        mix_gain_in.reshape(1, width),
        w_igate.T,
        w_fgate.T,
        igate_bias.reshape(1, heads),
        fgate_bias.reshape(1, heads),
        log_scale.T,
        w_query,
        w_key,
        w_value,
        memory,
        head_gain.reshape(1, heads * value_dim),
        w_output,
    ]
    shape = jax.ShapeDtypeStruct((seqs // 2 if halves else seqs, w_output.shape[1]), bf16)
    result = pl.pallas_call(
        body,
        out_shape=[shape] * (2 if halves else 1),
        in_specs=[pl.BlockSpec(memory_space=pltpu.HBM)] * len(operands),
        out_specs=[whole()] * (2 if halves else 1),
        scratch_shapes=[pltpu.VMEM(o.shape, o.dtype) for o in operands]
        + [
            pltpu.VMEM((heads, seqs, value_dim), f32),
            pltpu.SemaphoreType.DMA((12 + seqs // chunk,)),
        ],
        compiler_params=pltpu.CompilerParams(vmem_limit_bytes=12 << 20),
        name="cell",
    )(*[o if o.size == heads else pltpu.with_memory_space_constraint(o, pltpu.HBM) for o in operands])
    return result if halves else result[0]


def after_mix_body(parts, tokens, gain_out, spread):
    f32 = jnp.float32
    half = tokens.shape[0] // 2
    mixed = parts[0][...].astype(f32)
    for part in parts[1:]:
        mixed = mixed + part[...].astype(f32)
    odd = lax.axis_index("tp") % 2 == 1
    xf = tokens[...].astype(f32)
    xf = jnp.where(odd, xf[half:], xf[:half])
    resid = (xf + mixed * rms_scale(mixed) * gain_out[...]).astype(jnp.bfloat16)
    for g in range(spread.shape[0]):
        spread[g] = resid


def after_mix(parts, tokens, gain_out, groups):
    seqs, width = tokens.shape
    count = len(parts)
    return pl.pallas_call(
        lambda *refs: after_mix_body(refs[:count], *refs[count:]),
        out_shape=jax.ShapeDtypeStruct((groups, seqs // 2, width), jnp.bfloat16),
        in_specs=[whole()] * (count + 2),
        out_specs=whole(),
        compiler_params=pltpu.CompilerParams(vmem_limit_bytes=8 << 20),
        name="after_mix",
    )(*parts, tokens, gain_out.reshape(1, width))


def expert_body(near, far, gain, gate_w, up_w, down_w, keep, send, resid_part, rows):
    f32 = jnp.float32
    bf16 = jnp.bfloat16
    groups, half, width = near.shape
    seqs = 2 * half
    quarter = resid_part.shape[1]
    lane = lax.axis_index("tp")
    odd = lane % 2 == 1
    mine, theirs = near[...].astype(f32), far[...].astype(f32)
    rows[:, :half] = jnp.where(odd, theirs, mine)
    rows[:, half:] = jnp.where(odd, mine, theirs)
    columns = pl.ds(pl.multiple_of(lane * quarter, quarter), quarter)
    resid_part[...] = rows[lax.axis_index("ep"), :, columns]
    rf = rows[...].reshape(groups * seqs, width)
    ffn_in = (rf * rms_scale(rf) * gain[...]).astype(bf16)
    gate = jnp.dot(ffn_in, gate_w[...], preferred_element_type=f32)
    up = jnp.dot(ffn_in, up_w[...], preferred_element_type=f32)
    act = (gate * jax.nn.sigmoid(gate) * up).astype(bf16)
    for s in range(width // quarter // 2):
        places = slice(2 * s * quarter, (2 * s + 1) * quarter)
        even_part = jnp.dot(act, down_w[:, places], preferred_element_type=f32)
        places = slice((2 * s + 1) * quarter, (2 * s + 2) * quarter)
        odd_part = jnp.dot(act, down_w[:, places], preferred_element_type=f32)
        kept = jnp.where(odd, odd_part, even_part).astype(bf16).reshape(groups, seqs, quarter)
        sent = jnp.where(odd, even_part, odd_part).astype(bf16).reshape(groups, seqs, quarter)
        places = slice(s * quarter, (s + 1) * quarter)
        keep[:, :, places] = kept
        send[:, :, places] = sent


def expert(near, far, gain, gate_w, up_w, down_w, lanes):
    groups, half, width = near.shape
    quarter = width // lanes
    shape = jax.ShapeDtypeStruct((groups, 2 * half, width // 2), jnp.bfloat16)
    return pl.pallas_call(
        expert_body,
        out_shape=(shape, shape, jax.ShapeDtypeStruct((2 * half, quarter), jnp.float32)),
        in_specs=[whole()] * 6,
        out_specs=(whole(), whole(), whole()),
        scratch_shapes=[pltpu.VMEM((groups, 2 * half, width), jnp.float32)],
        compiler_params=pltpu.CompilerParams(vmem_limit_bytes=16 << 20),
        name="expert",
    )(near, far, gain.reshape(1, width), gate_w, up_w, down_w)


def last_body(r0, r1, r2, r3, resid_part, gain, out, same):
    f32 = jnp.float32
    quarter = out.shape[1]
    width = 2 * r0.shape[1]
    kept = r0[...].astype(f32) + r2[...].astype(f32)
    other = r1[...].astype(f32) + r3[...].astype(f32)
    same[...] = kept
    total = jnp.sum(kept * kept, axis=1, keepdims=True) + jnp.sum(
        other * other, axis=1, keepdims=True
    )
    place = lax.axis_index("tp") // 2
    routed = same[:, pl.ds(pl.multiple_of(place * quarter, quarter), quarter)]
    scaled = routed * lax.rsqrt(total / width + EPS)
    out[...] = (resid_part[...] + scaled * gain[...]).astype(jnp.bfloat16)


def last(parts, resid_part, gain):
    seqs, quarter = resid_part.shape
    return pl.pallas_call(
        last_body,
        out_shape=jax.ShapeDtypeStruct((seqs, quarter), jnp.bfloat16),
        in_specs=[whole()] * 6,
        out_specs=whole(),
        scratch_shapes=[pltpu.VMEM(parts[0].shape, jnp.float32)],
        compiler_params=pltpu.CompilerParams(vmem_limit_bytes=8 << 20),
        name="last",
    )(*parts, resid_part, gain.reshape(1, quarter))


def every_token(
    halves,
    tokens,
    mix_gain_out,
    ffn_gain_in,
    routes,
    route_weights,
    expert_gate,
    expert_up,
    expert_down,
    ffn_gain_out,
):
    f32 = jnp.float32
    bf16 = jnp.bfloat16
    lanes = lax.axis_size("tp")
    groups = lax.axis_size("ep")
    mine, theirs = halves
    parts = [mine] + [exchange(theirs if step % 2 else mine, "tp", step) for step in (1, 2, 3)]
    spread = after_mix(parts, tokens, mix_gain_out, groups)
    named = routes[:, :, None] == jnp.arange(groups, dtype=jnp.int32)[None, None, :]
    weights = jnp.sum(jnp.where(named, route_weights[:, :, None], 0.0), axis=1).T
    spread, weights, gate_w, up_w, down_w, gain_in = lax.optimization_barrier(
        (spread, weights, expert_gate[0], expert_up[0], expert_down[0], ffn_gain_in)
    )
    near = lax.all_to_all(spread, "ep", split_axis=0, concat_axis=0, tiled=True)
    far = exchange(near, "tp", 1)
    keep, send, resid_part = expert(near, far, gain_in, gate_w, up_w, down_w, lanes)
    got = exchange(send, "tp", 1)
    blocks = (keep.astype(f32) + got.astype(f32)).astype(bf16)
    blocks, resid_part, ffn_gain_out = lax.optimization_barrier((blocks, resid_part, ffn_gain_out))
    back = lax.all_to_all(blocks, "ep", split_axis=0, concat_axis=0, tiled=True)
    share = jnp.sum(weights[:, :, None] * back.astype(f32), axis=0).astype(bf16)
    parts = [share] + [exchange(share, "tp", step) for step in (1, 2, 3)]
    return last(parts, resid_part, ffn_gain_out)


def slotted(ffn_in, routes, route_weights, expert_gate, expert_up, expert_down, cap):
    f32 = jnp.float32
    bf16 = jnp.bfloat16
    seqs, width = ffn_in.shape
    top = routes.shape[1]
    local_experts = expert_gate.shape[0]
    experts_all = local_experts * lax.axis_size("ep")
    flat = routes.reshape(-1)
    hits = (flat[:, None] == jnp.arange(experts_all, dtype=jnp.int32)[None, :]).astype(jnp.int32)
    earlier = jnp.cumsum(hits, axis=0) - hits
    slot = jnp.sum(earlier * hits, axis=1)
    place = (flat * cap + slot).reshape(seqs, top)
    picker = jnp.any(
        jnp.arange(experts_all * cap, dtype=jnp.int32)[:, None, None] == place[None, :, :], axis=2
    ).astype(bf16)
    outbound = (
        jnp.dot(picker, ffn_in, preferred_element_type=f32)
        .astype(bf16)
        .reshape(experts_all, cap, width)
    )
    arrived = lax.all_to_all(outbound, "ep", split_axis=0, concat_axis=0, tiled=True)
    items = arrived.shape[1]
    rows = arrived.reshape(-1, local_experts, items, width)
    gate = jnp.einsum("secd,edf->secf", rows, expert_gate, preferred_element_type=f32)
    up = jnp.einsum("secd,edf->secf", rows, expert_up, preferred_element_type=f32)
    act = (jax.nn.silu(gate) * up).astype(bf16)
    part = jnp.einsum("secf,efd->secd", act, expert_down, preferred_element_type=f32).reshape(
        -1, items, width
    )
    summed = lax.psum_scatter(
        part.astype(jnp.bfloat16), "tp", scatter_dimension=2, tiled=True
    ).astype(jnp.float32)
    done = summed.astype(bf16)
    returned = lax.all_to_all(done, "ep", split_axis=0, concat_axis=0, tiled=True)
    columns = returned.shape[2]
    chosen = jnp.take(returned.reshape(-1, columns), place.reshape(-1), axis=0).reshape(
        seqs, top, columns
    )
    return jnp.sum(route_weights[:, :, None] * chosen.astype(f32), axis=1)


def solution(mesh):
    return jax.shard_map(
        per_device,
        mesh=mesh,
        in_specs=(
            P("ep", None),
            P("ep", "tp", None, None),
            P("ep", "tp"),
            P(),
            P(None, "tp"),
            P(None, "tp"),
            P(None, "tp"),
            P(None, "tp"),
            P(None, "tp"),
            P("tp"),
            P("tp"),
            P("tp"),
            P("tp", None),
            P(),
            P(),
            P("ep", None),
            P("ep", None),
            P("ep", None, "tp"),
            P("ep", None, "tp"),
            P("ep", "tp", None),
            P("tp"),
        ),
        out_specs=P("ep", "tp"),
        check_vma=False,
    )
```

time: 51.6 us -> 42.7 us (0.83)
  blocking collectives: 14.9 us -> 22.9 us
  waiting for transfers between devices: 16 us -> 8.2 us
  Pallas kernels: 7.69 us -> 4.31 us
  starting transfers between devices: 8.06 us -> 5.36 us
  other arithmetic: 1.63 us -> 0.13 us
  local copies, waits for them, and re-layouts: 1.4 us -> 0.04 us
    all_to_all x1 -> x0, waiting for transfers between devices: 10.5 us -> none  [every_token(): lax.all_to_all(blocks, ('ep', 'tp'), split_axis=0, concat_axis=0, tiled=T...]
    all_to_all x1 -> x2, blocking collectives: 14.9 us -> 22.9 us  [the longest x1 12.9 us: every_token(): near = lax.all_to_all(spread, 'ep', split_axis=0, concat_axis=0, tiled=True)]
    pallas_call x3 -> x4, Pallas kernels: 7.69 us -> 4.31 us  [the longest x1 2.89 us: cell(): pl.pallas_call(body, out_shape=[shape] * (2 if halves else 1), in_specs=[...]
    all_to_all x1 -> x0, starting transfers between devices: 2.97 us -> none  [every_token(): lax.all_to_all(blocks, ('ep', 'tp'), split_axis=0, concat_axis=0, tiled=T...]
    ppermute x6 -> x8, waiting for transfers between devices: 5.48 us -> 8.2 us  [exchange(): return lax.ppermute(value, axis, pairs)]
    convert_element_type x1, other arithmetic: 1.38 us -> 0.03 us  [every_token(): blocks = (keep.astype(f32) + got.astype(f32)).astype(bf16)]
    broadcast_in_dim x1 -> x0, local copies, waits for them, and re-layouts: 0.77 us -> none  [every_token(): spread = jnp.broadcast_to(ffn_in[None], (groups, seqs, width))]
    unnamed x12 -> x18, local copies, waits for them, and re-layouts: 0.63 us -> 0.04 us
  transfers between devices with their start and end apart: 7 -> 8, of which waited for: 5 -> 5; matrix products, arithmetic and copies ran while one was open for 0% -> 0% of each run, Pallas kernels for 0% -> 0%
where the time goes in v4:
time: 42.7 us; the launch traced here: 42.4 us
  blocking collectives  22.9 us (54%)
  waiting for transfers between devices  8.2 us (19%)
  starting transfers between devices  5.36 us (13%)
  Pallas kernels  4.31 us (10%)
  between operations  1.46 us (3%)
    all_to_all x1, blocking collectives, every_token(): near = lax.all_to_all(spread, 'ep', split_axis=0, concat_axis=0, tiled=True)  12.9 us
    all_to_all x1, blocking collectives, every_token(): back = lax.all_to_all(blocks, 'ep', split_axis=0, concat_axis=0, tiled=True)  9.97 us
    ppermute x8, waiting for transfers between devices, exchange(): return lax.ppermute(value, axis, pairs)  8.2 us
    ppermute x8, starting transfers between devices, exchange(): return lax.ppermute(value, axis, pairs)  5.36 us
    pallas_call x1, Pallas kernels, cell(): pl.pallas_call(body, out_shape=[shape] * (2 if halves else 1), in_specs=[...  2.89 us
  transfers between devices with their start and end apart: 8, of which 5 were waited for; matrix products, arithmetic and copies ran while one was open for 0% of the time, Pallas kernels for 0%

profile of v4, /device:TPU:0, one launch (start us, length us, event | category | flops | bytes accessed | tf_op | source)
XLA Modules:
  0.0 42.4 jit_solution(5319732791517851338)
XLA Ops:
  0.0 0.0 copy-start.3
  0.0 0.0 copy-start.7
  0.0 0.0 copy-start.8
  0.0 0.0 copy-start.4
  1.3 0.0 copy-start
  1.4 0.0 copy-start.1
  1.4 0.0 copy-start.2
  1.4 0.0 copy-start.5
  1.4 2.9 %cell.1 = (bf16[8,1024]{1,0:T(8,128)(2,1)S(1)}, bf16[8,1024]{1,0:T(8,128)(2,1)S(1)}) custom-call(bf16[16,1024]{1,0:T(8,128)(2,1)} %refs_4_.1, f32[1,1024]{1,0:T(1,128)} %bitcast.23, bf16[1,1024]{1,0:T(2,128)(2,1)} %bitcast.24, bf16[1,1024]{1,0:T(2,128)(2,1)} %bitcast.25, f32[1,1]{1,0:T(1,128)} %bitcast.14.refs_4_, f32[1,1]{1,0:T(1,128)} %bitcast.15.refs_5_, ...), custom_call_target="tpu_custom_call" | custom-call | tf_op jit(solution)/shard_map/cell/pallas_call | solution.py:220
  4.3 0.0 copy-start.6
  4.3 2.5 %collective-permute-start.2 = (bf16[8,1024]{1,0:T(8,128)(2,1)S(1)}, bf16[8,1024]{1,0:T(8,128)(2,1)S(1)}, u32[]{:S(2)}, u32[]{:S(2)}) collective-permute-start(bf16[8,1024]{1,0:T(8,128)(2,1)S(1)} %get-tuple-element.20), channel_id=1, source_target_pairs={{0,3},{1,2},{2,1},{3,0},{4,7},{5,6},{6,5},{7,4},{8,11},{9,10},{10,... | collective-permute-start | bytes 49160 | tf_op jit(solution)/shard_map/ppermute | solution.py:96
  6.8 0.7 %collective-permute-start = (bf16[8,1024]{1,0:T(8,128)(2,1)S(1)}, bf16[8,1024]{1,0:T(8,128)(2,1)S(1)}, u32[]{:S(2)}, u32[]{:S(2)}) collective-permute-start(bf16[8,1024]{1,0:T(8,128)(2,1)S(1)} %get-tuple-element.20), channel_id=1, source_target_pairs={{0,1},{1,0},{2,3},{3,2},{4,5},{5,4},{6,7},{7,6},{8,9},{9,8},{10,11... | collective-permute-start | bytes 49160 | tf_op jit(solution)/shard_map/ppermute | solution.py:96
  7.5 0.0 collective-permute-start.1
  7.5 0.0 copy-done.7
  7.5 0.0 copy-done.8
  7.5 3.7 %collective-permute-done.1.refs_2_ = bf16[8,1024]{1,0:T(8,128)(2,1)S(1)} collective-permute-done((bf16[8,1024]{1,0:T(8,128)(2,1)S(1)}, bf16[8,1024]{1,0:T(8,128)(2,1)S(1)}, u32[]{:S(2)}, u32[]{:S(2)}) %collective-permute-start.1) | collective-permute-done | bytes 16416 | tf_op jit(solution)/shard_map/ppermute | solution.py:96
  11.2 0.0 collective-permute-done.2.refs_3_
  11.2 0.0 collective-permute-done.refs_1_
  11.2 0.0 copy-done.3
  11.2 0.0 copy-done.4
  11.2 0.1 after_mix.1
  11.4 12.9 %all_to_all.10.near = bf16[8,8,1024]{2,1,0:T(8,128)(2,1)S(1)} all-to-all(bf16[8,8,1024]{2,1,0:T(8,128)(2,1)S(1)} %after_mix.1), channel_id=1, replica_groups=mesh['ep'=8,'tp'=4] {'ep'}, dimensions={0} | all-to-all | bytes 262144 | tf_op jit(solution)/shard_map/all_to_all | solution.py:361
  24.3 0.0 collective-permute-start.3
  24.3 1.3 %collective-permute-done.3.far = bf16[8,8,1024]{2,1,0:T(8,128)(2,1)S(1)} collective-permute-done((bf16[8,8,1024]{2,1,0:T(8,128)(2,1)S(1)}, bf16[8,8,1024]{2,1,0:T(8,128)(2,1)S(1)}, u32[]{:S(2)}, u32[]{:S(2)}) %collective-permute-start.3) | collective-permute-done | bytes 131104 | tf_op jit(solution)/shard_map/ppermute | solution.py:96
  25.7 0.0 copy-done
  25.7 0.0 copy-done.1
  25.7 0.0 copy-done.2
  25.7 0.0 copy-done.5
  25.7 0.6 %expert.1 = (bf16[8,16,512]{2,1,0:T(8,128)(2,1)S(1)}, bf16[8,16,512]{2,1,0:T(8,128)(2,1)S(1)}, f32[16,256]{1,0:T(8,128)S(1)}) custom-call(bf16[8,8,1024]{2,1,0:T(8,128)(2,1)S(1)} %all_to_all.10.near, bf16[8,8,1024]{2,1,0:T(8,128)(2,1)S(1)} %collective-permute-done.3.far, f32[1,1024]{1,0:T(1,128)S(1)} %bitcast.20, bf16[1024,256]{1,0:T(8,128)(2,1)S(1)} %bitcast.16, ...), custom_call_target="tpu_custom_call" | custom-call | tf_op jit(solution)/shard_map/expert/pallas_call | solution.py:297
  26.3 0.2 collective-permute-start.4
  26.5 1.2 %collective-permute-done.4 = bf16[8,16,512]{2,1,0:T(8,128)(2,1)S(1)} collective-permute-done((bf16[8,16,512]{2,1,0:T(8,128)(2,1)S(1)}, bf16[8,16,512]{2,1,0:T(8,128)(2,1)S(1)}, u32[]{:S(2)}, u32[]{:S(2)}) %collective-permute-start.4) | collective-permute-done | bytes 131104 | tf_op jit(solution)/shard_map/ppermute | solution.py:96
  27.8 10.0 %all_to_all.11 = bf16[8,16,512]{2,1,0:T(8,128)(2,1)S(1)} all-to-all(bf16[8,16,512]{2,1,0:T(8,128)(2,1)S(1)} %add_convert_fusion), channel_id=1, replica_groups=mesh['ep'=8,'tp'=4] {'ep'}, dimensions={0} | all-to-all | bytes 262144 | tf_op jit(solution)/shard_map/all_to_all | solution.py:367
  37.7 0.1 multiply_reduce_fusion.r0
  37.8 0.1 collective-permute-start.7
  37.9 0.6 %collective-permute-start.6 = (bf16[16,512]{1,0:T(8,128)(2,1)S(1)}, bf16[16,512]{1,0:T(8,128)(2,1)S(1)}, u32[]{:S(2)}, u32[]{:S(2)}) collective-permute-start(bf16[16,512]{1,0:T(8,128)(2,1)S(1)} %multiply_reduce_fusion.r0), channel_id=1, source_target_pairs={{0,2},{1,3},{2,0},{3,1},{4,6},{5,7},{6,4},{7,5},{8,10},{9,11},{10,... | collective-permute-start | bytes 49160 | tf_op jit(solution)/shard_map/ppermute | solution.py:96
  38.5 1.3 %collective-permute-start.5 = (bf16[16,512]{1,0:T(8,128)(2,1)S(1)}, bf16[16,512]{1,0:T(8,128)(2,1)S(1)}, u32[]{:S(2)}, u32[]{:S(2)}) collective-permute-start(bf16[16,512]{1,0:T(8,128)(2,1)S(1)} %multiply_reduce_fusion.r0), channel_id=1, source_target_pairs={{0,1},{1,0},{2,3},{3,2},{4,5},{5,4},{6,7},{7,6},{8,9},{9,8},{10,11... | collective-permute-start | bytes 49160 | tf_op jit(solution)/shard_map/ppermute | solution.py:96
  39.7 1.3 %collective-permute-done.7.r3 = bf16[16,512]{1,0:T(8,128)(2,1)S(1)} collective-permute-done((bf16[16,512]{1,0:T(8,128)(2,1)S(1)}, bf16[16,512]{1,0:T(8,128)(2,1)S(1)}, u32[]{:S(2)}, u32[]{:S(2)}) %collective-permute-start.7) | collective-permute-done | bytes 16416 | tf_op jit(solution)/shard_map/ppermute | solution.py:96
  41.0 0.7 %collective-permute-done.6.r2 = bf16[16,512]{1,0:T(8,128)(2,1)S(1)} collective-permute-done((bf16[16,512]{1,0:T(8,128)(2,1)S(1)}, bf16[16,512]{1,0:T(8,128)(2,1)S(1)}, u32[]{:S(2)}, u32[]{:S(2)}) %collective-permute-start.6) | collective-permute-done | bytes 16416 | tf_op jit(solution)/shard_map/ppermute | solution.py:96
  41.7 0.0 collective-permute-done.5.r1
  41.7 0.0 copy-done.6
  41.7 0.7 %last.1 = bf16[16,256]{1,0:T(8,128)(2,1)} custom-call(bf16[16,512]{1,0:T(8,128)(2,1)S(1)} %multiply_reduce_fusion.r0, bf16[16,512]{1,0:T(8,128)(2,1)S(1)} %collective-permute-done.5.r1, bf16[16,512]{1,0:T(8,128)(2,1)S(1)} %collective-permute-done.6.r2, bf16[16,512]{1,0:T(8,128)(2,1)S(1)} %collective-permute-done.7.r3, ...), custom_call_target="tpu_custom_call" | custom-call | tf_op jit(solution)/shard_map/last/pallas_call | solution.py:326
  (2 shorter events, 0.0 us)
Async XLA Ops:
  0.0 11.2 %copy-start.3 = (bf16[16,1024]{1,0:T(8,128)(2,1)S(1)}, bf16[16,1024]{1,0:T(8,128)(2,1)}, u32[]{:S(2)}) copy-start(bf16[16,1024]{1,0:T(8,128)(2,1)} %refs_4_.1) | copy-start | bytes 98308
  0.0 7.5 %copy-start.7 = (f32[16,6]{0,1:T(8,128)S(1)}, f32[16,6]{0,1:T(8,128)}, u32[]{:S(2)}) copy-start(f32[16,6]{0,1:T(8,128)} %param.37) | copy-start | bytes 1156
  0.0 7.5 %copy-start.8 = (s32[16,6]{0,1:T(8,128)S(1)}, s32[16,6]{0,1:T(8,128)}, u32[]{:S(2)}) copy-start(s32[16,6]{0,1:T(8,128)} %param.36) | copy-start | bytes 1156
  0.0 11.2 %copy-start.4 = (f32[1024]{0:T(1024)S(1)}, f32[1024]{0:T(1024)}, u32[]{:S(2)}) copy-start(f32[1024]{0:T(1024)} %param.34) | copy-start | bytes 12292
  1.3 24.3 %copy-start = (bf16[1,1024,256]{2,1,0:T(8,128)(2,1)S(1)}, bf16[1,1024,256]{2,1,0:T(8,128)(2,1)}, u32[]{:S(2)}) copy-start(bf16[1,1024,256]{2,1,0:T(8,128)(2,1)} %param.38) | copy-start | bytes 1572868
  1.4 24.3 %copy-start.1 = (bf16[1,1024,256]{2,1,0:T(8,128)(2,1)S(1)}, bf16[1,1024,256]{2,1,0:T(8,128)(2,1)}, u32[]{:S(2)}) copy-start(bf16[1,1024,256]{2,1,0:T(8,128)(2,1)} %param.39) | copy-start | bytes 1572868
  1.4 24.3 %copy-start.2 = (bf16[1,256,1024]{2,1,0:T(8,128)(2,1)S(1)}, bf16[1,256,1024]{2,1,0:T(8,128)(2,1)}, u32[]{:S(2)}) copy-start(bf16[1,256,1024]{2,1,0:T(8,128)(2,1)} %param.40) | copy-start | bytes 1572868
  1.4 24.3 %copy-start.5 = (f32[1024]{0:T(1024)S(1)}, f32[1024]{0:T(1024)}, u32[]{:S(2)}) copy-start(f32[1024]{0:T(1024)} %param.35) | copy-start | bytes 12292
  4.3 37.4 %copy-start.6 = (f32[256]{0:T(256)S(1)}, f32[256]{0:T(256)}, u32[]{:S(2)}) copy-start(f32[256]{0:T(256)} %param.41) | copy-start | bytes 3076
  4.3 6.9 %collective-permute-start.2 = (bf16[8,1024]{1,0:T(8,128)(2,1)S(1)}, bf16[8,1024]{1,0:T(8,128)(2,1)S(1)}, u32[]{:S(2)}, u32[]{:S(2)}) collective-permute-start(bf16[8,1024]{1,0:T(8,128)(2,1)S(1)} %get-tuple-element.20), channel_id=1, source_target_pairs={{0,3},{1,2},{2,1},{3,0},{4,7},{5,6},{6,5},{7,4},{8,11},{9,10},{10,... | collective-permute-start | bytes 49160 | tf_op jit(solution)/shard_map/ppermute | solution.py:96
  6.8 4.4 %collective-permute-start = (bf16[8,1024]{1,0:T(8,128)(2,1)S(1)}, bf16[8,1024]{1,0:T(8,128)(2,1)S(1)}, u32[]{:S(2)}, u32[]{:S(2)}) collective-permute-start(bf16[8,1024]{1,0:T(8,128)(2,1)S(1)} %get-tuple-element.20), channel_id=1, source_target_pairs={{0,1},{1,0},{2,3},{3,2},{4,5},{5,4},{6,7},{7,6},{8,9},{9,8},{10,11... | collective-permute-start | bytes 49160 | tf_op jit(solution)/shard_map/ppermute | solution.py:96
  7.5 3.7 %collective-permute-start.1 = (bf16[8,1024]{1,0:T(8,128)(2,1)S(1)}, bf16[8,1024]{1,0:T(8,128)(2,1)S(1)}, u32[]{:S(2)}, u32[]{:S(2)}) collective-permute-start(bf16[8,1024]{1,0:T(8,128)(2,1)S(1)} %get-tuple-element.19.refs_0_), channel_id=1, source_target_pairs={{0,2},{1,3},{2,0},{3,1},{4,6},{5,7},{6,4},{7,5},{8,10},{9,11},{10,... | collective-permute-start | bytes 49160 | tf_op jit(solution)/shard_map/ppermute | solution.py:96
  24.3 1.3 %collective-permute-start.3 = (bf16[8,8,1024]{2,1,0:T(8,128)(2,1)S(1)}, bf16[8,8,1024]{2,1,0:T(8,128)(2,1)S(1)}, u32[]{:S(2)}, u32[]{:S(2)}) collective-permute-start(bf16[8,8,1024]{2,1,0:T(8,128)(2,1)S(1)} %all_to_all.10.near), channel_id=1, source_target_pairs={{0,1},{1,0},{2,3},{3,2},{4,5},{5,4},{6,7},{7,6},{8,9},{9,8},{10,11... | collective-permute-start | bytes 393224 | tf_op jit(solution)/shard_map/ppermute | solution.py:96
  26.3 1.4 %collective-permute-start.4 = (bf16[8,16,512]{2,1,0:T(8,128)(2,1)S(1)}, bf16[8,16,512]{2,1,0:T(8,128)(2,1)S(1)}, u32[]{:S(2)}, u32[]{:S(2)}) collective-permute-start(bf16[8,16,512]{2,1,0:T(8,128)(2,1)S(1)} %get-tuple-element.28), channel_id=1, source_target_pairs={{0,1},{1,0},{2,3},{3,2},{4,5},{5,4},{6,7},{7,6},{8,9},{9,8},{10,11... | collective-permute-start | bytes 393224 | tf_op jit(solution)/shard_map/ppermute | solution.py:96
  37.8 3.2 %collective-permute-start.7 = (bf16[16,512]{1,0:T(8,128)(2,1)S(1)}, bf16[16,512]{1,0:T(8,128)(2,1)S(1)}, u32[]{:S(2)}, u32[]{:S(2)}) collective-permute-start(bf16[16,512]{1,0:T(8,128)(2,1)S(1)} %multiply_reduce_fusion.r0), channel_id=1, source_target_pairs={{0,3},{1,2},{2,1},{3,0},{4,7},{5,6},{6,5},{7,4},{8,11},{9,10},{10,... | collective-permute-start | bytes 49160 | tf_op jit(solution)/shard_map/ppermute | solution.py:96
  37.9 3.8 %collective-permute-start.6 = (bf16[16,512]{1,0:T(8,128)(2,1)S(1)}, bf16[16,512]{1,0:T(8,128)(2,1)S(1)}, u32[]{:S(2)}, u32[]{:S(2)}) collective-permute-start(bf16[16,512]{1,0:T(8,128)(2,1)S(1)} %multiply_reduce_fusion.r0), channel_id=1, source_target_pairs={{0,2},{1,3},{2,0},{3,1},{4,6},{5,7},{6,4},{7,5},{8,10},{9,11},{10,... | collective-permute-start | bytes 49160 | tf_op jit(solution)/shard_map/ppermute | solution.py:96
  38.5 3.2 %collective-permute-start.5 = (bf16[16,512]{1,0:T(8,128)(2,1)S(1)}, bf16[16,512]{1,0:T(8,128)(2,1)S(1)}, u32[]{:S(2)}, u32[]{:S(2)}) collective-permute-start(bf16[16,512]{1,0:T(8,128)(2,1)S(1)} %multiply_reduce_fusion.r0), channel_id=1, source_target_pairs={{0,1},{1,0},{2,3},{3,2},{4,5},{5,4},{6,7},{7,6},{8,9},{9,8},{10,11... | collective-permute-start | bytes 49160 | tf_op jit(solution)/shard_map/ppermute | solution.py:96

commit v5 on v4

--- a/solution.py
+++ b/solution.py
@@ -4,6 +4,7 @@
 from jax.experimental import pallas as pl
 from jax.experimental.pallas import tpu as pltpu
 from jax.sharding import PartitionSpec as P
+
 
 EPS = 1e-06
 
@@ -233,7 +234,7 @@
     return result if halves else result[0]
 
 
-def after_mix_body(parts, tokens, gain_out, spread):
+def after_mix_body(parts, tokens, gain_out, gain_in, resid, spread):
     f32 = jnp.float32
     half = tokens.shape[0] // 2
     mixed = parts[0][...].astype(f32)
@@ -242,96 +243,115 @@
     odd = lax.axis_index("tp") % 2 == 1
     xf = tokens[...].astype(f32)
     xf = jnp.where(odd, xf[half:], xf[:half])
-    resid = (xf + mixed * rms_scale(mixed) * gain_out[...]).astype(jnp.bfloat16)
+    kept = (xf + mixed * rms_scale(mixed) * gain_out[...]).astype(jnp.bfloat16)
+    resid[...] = kept
+    rf = kept.astype(f32)
+    ffn_in = (rf * rms_scale(rf) * gain_in[...]).astype(jnp.bfloat16)
     for g in range(spread.shape[0]):
-        spread[g] = resid
-
-
-def after_mix(parts, tokens, gain_out, groups):
+        spread[g] = ffn_in
+
+
+def after_mix(parts, tokens, gain_out, gain_in, groups):
     seqs, width = tokens.shape
     count = len(parts)
     return pl.pallas_call(
         lambda *refs: after_mix_body(refs[:count], *refs[count:]),
-        out_shape=jax.ShapeDtypeStruct((groups, seqs // 2, width), jnp.bfloat16),
-        in_specs=[whole()] * (count + 2),
-        out_specs=whole(),
+        out_shape=(
+            jax.ShapeDtypeStruct((seqs // 2, width), jnp.bfloat16),
+            jax.ShapeDtypeStruct((groups, seqs // 2, width), jnp.bfloat16),
+        ),
+        in_specs=[whole()] * (count + 3),
+        out_specs=(whole(), whole()),
         compiler_params=pltpu.CompilerParams(vmem_limit_bytes=8 << 20),
         name="after_mix",
-    )(*parts, tokens, gain_out.reshape(1, width))
-
-
-def expert_body(near, far, gain, gate_w, up_w, down_w, keep, send, resid_part, rows):
-    f32 = jnp.float32
-    bf16 = jnp.bfloat16
-    groups, half, width = near.shape
-    seqs = 2 * half
-    quarter = resid_part.shape[1]
+    )(*parts, tokens, gain_out.reshape(1, width), gain_in.reshape(1, width))
+
+
+def expert_body(rows, gate_w, up_w, down_w, gate_n, up_n, down_n, out):
+    f32 = jnp.float32
+    groups, half, width = rows.shape
+    ffn_in = rows[...].reshape(groups * half, width)
+    total = None
+    for gates, ups, downs in ((gate_w, up_w, down_w), (gate_n, up_n, down_n)):
+        gate = jnp.dot(ffn_in, gates[...], preferred_element_type=f32)
+        up = jnp.dot(ffn_in, ups[...], preferred_element_type=f32)
+        act = (gate * jax.nn.sigmoid(gate) * up).astype(jnp.bfloat16)
+        part = jnp.dot(act, downs[...], preferred_element_type=f32)
+        total = part if total is None else total + part
+    out[...] = total.astype(jnp.bfloat16).reshape(groups, half, width)
+
+
+def expert(rows, own, neighbour):
+    return pl.pallas_call(
+        expert_body,
+        out_shape=jax.ShapeDtypeStruct(rows.shape, jnp.bfloat16),
+        in_specs=[whole()] * 7,
+        out_specs=whole(),
+        compiler_params=pltpu.CompilerParams(vmem_limit_bytes=16 << 20),
+        name="expert",
+    )(rows, *own, *neighbour)
+
+
+def share_body(back, weights, resid, share, both):
+    f32 = jnp.float32
+    groups, half, _ = back.shape
+    odd = lax.axis_index("tp") % 2 == 1
+    turned = weights[...].T
+    mine = jnp.where(odd, turned[half:], turned[:half])
+    total = mine[:, 0:1] * back[0].astype(f32)
+    for e in range(1, groups):
+        total = total + mine[:, e : e + 1] * back[e].astype(f32)
+    rounded = total.astype(jnp.bfloat16)
+    share[...] = rounded
+    both[0] = rounded
+    both[1] = resid[...]
+
+
+def combine(back, weights, resid):
+    _, half, width = back.shape
+    return pl.pallas_call(
+        share_body,
+        out_shape=(
+            jax.ShapeDtypeStruct((half, width), jnp.bfloat16),
+            jax.ShapeDtypeStruct((2, half, width), jnp.bfloat16),
+        ),
+        in_specs=[whole()] * 3,
+        out_specs=(whole(), whole()),
+        compiler_params=pltpu.CompilerParams(vmem_limit_bytes=8 << 20),
+        name="share",
+    )(back, weights, resid)
+
+
+def last_body(share, both, other_y, other_far, resid, gain, out, picks):
+    f32 = jnp.float32
+    quarter = out.shape[1]
+    kept = share[...].astype(f32) + other_y[...].astype(f32)
+    other = both[0].astype(f32) + other_far[...].astype(f32)
+    picks[0] = kept * rms_scale(kept)
+    picks[1] = other * rms_scale(other)
+    picks[2] = resid[...].astype(f32)
+    picks[3] = both[1].astype(f32)
     lane = lax.axis_index("tp")
     odd = lane % 2 == 1
-    mine, theirs = near[...].astype(f32), far[...].astype(f32)
-    rows[:, :half] = jnp.where(odd, theirs, mine)
-    rows[:, half:] = jnp.where(odd, mine, theirs)
-    columns = pl.ds(pl.multiple_of(lane * quarter, quarter), quarter)
-    resid_part[...] = rows[lax.axis_index("ep"), :, columns]
-    rf = rows[...].reshape(groups * seqs, width)
-    ffn_in = (rf * rms_scale(rf) * gain[...]).astype(bf16)
-    gate = jnp.dot(ffn_in, gate_w[...], preferred_element_type=f32)
-    up = jnp.dot(ffn_in, up_w[...], preferred_element_type=f32)
-    act = (gate * jax.nn.sigmoid(gate) * up).astype(bf16)
-    for s in range(width // quarter // 2):
-        places = slice(2 * s * quarter, (2 * s + 1) * quarter)
-        even_part = jnp.dot(act, down_w[:, places], preferred_element_type=f32)
-        places = slice((2 * s + 1) * quarter, (2 * s + 2) * quarter)
-        odd_part = jnp.dot(act, down_w[:, places], preferred_element_type=f32)
-        kept = jnp.where(odd, odd_part, even_part).astype(bf16).reshape(groups, seqs, quarter)
-        sent = jnp.where(odd, even_part, odd_part).astype(bf16).reshape(groups, seqs, quarter)
-        places = slice(s * quarter, (s + 1) * quarter)
-        keep[:, :, places] = kept
-        send[:, :, places] = sent
-
-
-def expert(near, far, gain, gate_w, up_w, down_w, lanes):
-    groups, half, width = near.shape
-    quarter = width // lanes
-    shape = jax.ShapeDtypeStruct((groups, 2 * half, width // 2), jnp.bfloat16)
-    return pl.pallas_call(
-        expert_body,
-        out_shape=(shape, shape, jax.ShapeDtypeStruct((2 * half, quarter), jnp.float32)),
-        in_specs=[whole()] * 6,
-        out_specs=(whole(), whole(), whole()),
-        scratch_shapes=[pltpu.VMEM((groups, 2 * half, width), jnp.float32)],
-        compiler_params=pltpu.CompilerParams(vmem_limit_bytes=16 << 20),
-        name="expert",
-    )(near, far, gain.reshape(1, width), gate_w, up_w, down_w)
-
-
-def last_body(r0, r1, r2, r3, resid_part, gain, out, same):
-    f32 = jnp.float32
-    quarter = out.shape[1]
-    width = 2 * r0.shape[1]
-    kept = r0[...].astype(f32) + r2[...].astype(f32)
-    other = r1[...].astype(f32) + r3[...].astype(f32)
-    same[...] = kept
-    total = jnp.sum(kept * kept, axis=1, keepdims=True) + jnp.sum(
-        other * other, axis=1, keepdims=True
-    )
-    place = lax.axis_index("tp") // 2
-    routed = same[:, pl.ds(pl.multiple_of(place * quarter, quarter), quarter)]
-    scaled = routed * lax.rsqrt(total / width + EPS)
-    out[...] = (resid_part[...] + scaled * gain[...]).astype(jnp.bfloat16)
-
-
-def last(parts, resid_part, gain):
-    seqs, quarter = resid_part.shape
+    places = pl.ds(pl.multiple_of(lane * quarter, quarter), quarter)
+    mine = picks[2, :, places] + picks[0, :, places] * gain[...]
+    theirs = picks[3, :, places] + picks[1, :, places] * gain[...]
+    low, high = jnp.where(odd, theirs, mine), jnp.where(odd, mine, theirs)
+    out[...] = jnp.concatenate([low, high], axis=0).astype(jnp.bfloat16)
+
+
+def last(share, both, other_y, other_far, resid, gain):
+    half, width = share.shape
+    quarter = gain.shape[0]
     return pl.pallas_call(
         last_body,
-        out_shape=jax.ShapeDtypeStruct((seqs, quarter), jnp.bfloat16),
+        out_shape=jax.ShapeDtypeStruct((2 * half, quarter), jnp.bfloat16),
         in_specs=[whole()] * 6,
         out_specs=whole(),
-        scratch_shapes=[pltpu.VMEM(parts[0].shape, jnp.float32)],
+        scratch_shapes=[pltpu.VMEM((4, half, width), jnp.float32)],
         compiler_params=pltpu.CompilerParams(vmem_limit_bytes=8 << 20),
         name="last",
-    )(*parts, resid_part, gain.reshape(1, quarter))
+    )(share, both, other_y, other_far, resid, gain.reshape(1, quarter))
 
 
 def every_token(
@@ -346,28 +366,30 @@
     expert_down,
     ffn_gain_out,
 ):
-    f32 = jnp.float32
-    bf16 = jnp.bfloat16
-    lanes = lax.axis_size("tp")
     groups = lax.axis_size("ep")
     mine, theirs = halves
-    parts = [mine] + [exchange(theirs if step % 2 else mine, "tp", step) for step in (1, 2, 3)]
-    spread = after_mix(parts, tokens, mix_gain_out, groups)
+    parts = [exchange(theirs if step % 2 else mine, "tp", step) for step in (1, 2, 3)]
+    parts = [mine] + parts
+    shards = (expert_gate[0], expert_up[0], expert_down[0])
+    *waited, _ = lax.optimization_barrier((*shards, mine))
+    neighbour = [exchange(shard, "tp", 1) for shard in waited]
+    resid, spread = after_mix(parts, tokens, mix_gain_out, ffn_gain_in, groups)
     named = routes[:, :, None] == jnp.arange(groups, dtype=jnp.int32)[None, None, :]
     weights = jnp.sum(jnp.where(named, route_weights[:, :, None], 0.0), axis=1).T
-    spread, weights, gate_w, up_w, down_w, gain_in = lax.optimization_barrier(
-        (spread, weights, expert_gate[0], expert_up[0], expert_down[0], ffn_gain_in)
-    )
-    near = lax.all_to_all(spread, "ep", split_axis=0, concat_axis=0, tiled=True)
-    far = exchange(near, "tp", 1)
-    keep, send, resid_part = expert(near, far, gain_in, gate_w, up_w, down_w, lanes)
-    got = exchange(send, "tp", 1)
-    blocks = (keep.astype(f32) + got.astype(f32)).astype(bf16)
-    blocks, resid_part, ffn_gain_out = lax.optimization_barrier((blocks, resid_part, ffn_gain_out))
+    spread, weights, gain_out = lax.optimization_barrier((spread, weights, ffn_gain_out))
+    rows = lax.all_to_all(spread, "ep", split_axis=0, concat_axis=0, tiled=True)
+    blocks = expert(rows, shards, neighbour)
+    blocks, weights, resid, gain_out = lax.optimization_barrier((blocks, weights, resid, gain_out))
     back = lax.all_to_all(blocks, "ep", split_axis=0, concat_axis=0, tiled=True)
-    share = jnp.sum(weights[:, :, None] * back.astype(f32), axis=0).astype(bf16)
-    parts = [share] + [exchange(share, "tp", step) for step in (1, 2, 3)]
-    return last(parts, resid_part, ffn_gain_out)
+    share, both = combine(back, weights, resid)
+    return last(
+        share,
+        exchange(both, "tp", 1),
+        exchange(share, "tp", 2),
+        exchange(share, "tp", 3),
+        resid,
+        gain_out,
+    )
 
 
 def slotted(ffn_in, routes, route_weights, expert_gate, expert_up, expert_down, cap):

time: 42.7 us -> 43.5 us (1.019)
  starting transfers between devices: 5.36 us -> 7.67 us
  waiting for transfers between devices: 8.2 us -> 6.62 us
    ppermute x8 -> x9, starting transfers between devices: 5.36 us -> 7.67 us  [exchange(): return lax.ppermute(value, axis, pairs)]
    ppermute x8 -> x9, waiting for transfers between devices: 8.2 us -> 6.62 us  [exchange(): return lax.ppermute(value, axis, pairs)]
    pallas_call x2 -> x3, Pallas kernels: 1.32 us -> 1.6 us  [the longest x1 0.74 us: expert(): pl.pallas_call(expert_body, out_shape=jax.ShapeDtypeStruct(rows.shape, jn...]
  transfers between devices with their start and end apart: 8 -> 9, of which waited for: 5 -> 4; matrix products, arithmetic and copies ran while one was open for 0% -> 0% of each run, Pallas kernels for 0% -> 0%
where the time goes in v5:
time: 43.5 us; the launch traced here: 43.3 us
  blocking collectives  22.9 us (53%)
  starting transfers between devices  7.67 us (18%)
  waiting for transfers between devices  6.62 us (15%)
  Pallas kernels  4.58 us (11%)
  between operations  1.52 us (3%)
    all_to_all x1, blocking collectives, every_token(): rows = lax.all_to_all(spread, 'ep', split_axis=0, concat_axis=0, tiled=True)  13.1 us
    all_to_all x1, blocking collectives, every_token(): back = lax.all_to_all(blocks, 'ep', split_axis=0, concat_axis=0, tiled=True)  9.74 us
    ppermute x9, starting transfers between devices, exchange(): return lax.ppermute(value, axis, pairs)  7.67 us
    ppermute x9, waiting for transfers between devices, exchange(): return lax.ppermute(value, axis, pairs)  6.62 us
    pallas_call x1, Pallas kernels, cell(): pl.pallas_call(body, out_shape=[shape] * (2 if halves else 1), in_specs=[...  2.77 us
  transfers between devices with their start and end apart: 9, of which 4 were waited for; matrix products, arithmetic and copies ran while one was open for 0% of the time, Pallas kernels for 0%

profile of v5, /device:TPU:0, one launch (start us, length us, event | category | flops | bytes accessed | tf_op | source)
XLA Modules:
  0.0 43.3 jit_solution(10780577883212978527)
XLA Ops:
  0.0 0.0 copy-start.3
  0.0 0.0 copy-start.2
  0.0 0.0 copy-start.1
  0.0 0.0 copy-start
  0.0 0.0 copy-start.7
  0.0 0.0 copy-start.8
  0.0 0.0 copy-start.5
  0.0 0.0 copy-start.4
  1.4 2.8 %cell.1 = (bf16[8,1024]{1,0:T(8,128)(2,1)S(1)}, bf16[8,1024]{1,0:T(8,128)(2,1)S(1)}) custom-call(bf16[16,1024]{1,0:T(8,128)(2,1)} %refs_4_.1, f32[1,1024]{1,0:T(1,128)} %bitcast.26, bf16[1,1024]{1,0:T(2,128)(2,1)} %bitcast.27, bf16[1,1024]{1,0:T(2,128)(2,1)} %bitcast.28, f32[1,1]{1,0:T(1,128)} %bitcast.14.refs_4_, f32[1,1]{1,0:T(1,128)} %bitcast.15.refs_5_, ...), custom_call_target="tpu_custom_call" | custom-call | tf_op jit(solution)/shard_map/cell/pallas_call | solution.py:221
  4.2 0.0 copy-done
  4.2 0.6 %collective-permute-start.3 = (bf16[1024,256]{1,0:T(8,128)(2,1)S(1)}, bf16[1024,256]{1,0:T(8,128)(2,1)S(1)}, u32[]{:S(2)}, u32[]{:S(2)}) collective-permute-start(bf16[1024,256]{1,0:T(8,128)(2,1)S(1)} %bitcast.16), channel_id=1, source_target_pairs={{0,1},{1,0},{2,3},{3,2},{4,5},{5,4},{6,7},{7,6},{8,9},{9,8},{10,11... | collective-permute-start | bytes 1572872 | tf_op jit(solution)/shard_map/ppermute | solution.py:97
  4.8 0.0 copy-done.1
  4.8 0.1 collective-permute-start.4
  4.9 0.0 copy-done.2
  4.9 0.4 collective-permute-start.5
  5.3 2.6 %collective-permute-start.2 = (bf16[8,1024]{1,0:T(8,128)(2,1)S(1)}, bf16[8,1024]{1,0:T(8,128)(2,1)S(1)}, u32[]{:S(2)}, u32[]{:S(2)}) collective-permute-start(bf16[8,1024]{1,0:T(8,128)(2,1)S(1)} %get-tuple-element.22), channel_id=1, source_target_pairs={{0,3},{1,2},{2,1},{3,0},{4,7},{5,6},{6,5},{7,4},{8,11},{9,10},{10,... | collective-permute-start | bytes 49160 | tf_op jit(solution)/shard_map/ppermute | solution.py:97
  7.9 0.1 collective-permute-start
  8.0 1.4 %collective-permute-done.2.refs_3_ = bf16[8,1024]{1,0:T(8,128)(2,1)S(1)} collective-permute-done((bf16[8,1024]{1,0:T(8,128)(2,1)S(1)}, bf16[8,1024]{1,0:T(8,128)(2,1)S(1)}, u32[]{:S(2)}, u32[]{:S(2)}) %collective-permute-start.2) | collective-permute-done | bytes 16416 | tf_op jit(solution)/shard_map/ppermute | solution.py:97
  9.4 1.7 %collective-permute-start.1 = (bf16[8,1024]{1,0:T(8,128)(2,1)S(1)}, bf16[8,1024]{1,0:T(8,128)(2,1)S(1)}, u32[]{:S(2)}, u32[]{:S(2)}) collective-permute-start(bf16[8,1024]{1,0:T(8,128)(2,1)S(1)} %get-tuple-element.21.refs_0_), channel_id=1, source_target_pairs={{0,2},{1,3},{2,0},{3,1},{4,6},{5,7},{6,4},{7,5},{8,10},{9,11},{10,... | collective-permute-start | bytes 49160 | tf_op jit(solution)/shard_map/ppermute | solution.py:97
  11.1 0.0 copy-done.7
  11.1 0.0 copy-done.8
  11.1 0.0 collective-permute-done.refs_1_
  11.1 2.0 %collective-permute-done.1.refs_2_ = bf16[8,1024]{1,0:T(8,128)(2,1)S(1)} collective-permute-done((bf16[8,1024]{1,0:T(8,128)(2,1)S(1)}, bf16[8,1024]{1,0:T(8,128)(2,1)S(1)}, u32[]{:S(2)}, u32[]{:S(2)}) %collective-permute-start.1) | collective-permute-done | bytes 16416 | tf_op jit(solution)/shard_map/ppermute | solution.py:97
  13.1 0.0 copy-done.3
  13.1 0.0 copy-done.5
  13.1 0.0 copy-done.4
  13.1 0.0 copy-start.6
  13.2 0.2 after_mix.1
  13.4 13.1 %all_to_all.10.rows = bf16[8,8,1024]{2,1,0:T(8,128)(2,1)S(1)} all-to-all(bf16[8,8,1024]{2,1,0:T(8,128)(2,1)S(1)} %get-tuple-element.24), channel_id=1, replica_groups=mesh['ep'=8,'tp'=4] {'ep'}, dimensions={0} | all-to-all | bytes 262144 | tf_op jit(solution)/shard_map/all_to_all | solution.py:380
  26.5 0.0 collective-permute-done.3.gate_n
  26.5 0.0 collective-permute-done.4.up_n
  26.5 0.0 collective-permute-done.5.down_n
  26.5 0.7 %expert.1 = bf16[8,8,1024]{2,1,0:T(8,128)(2,1)S(1)} custom-call(bf16[8,8,1024]{2,1,0:T(8,128)(2,1)S(1)} %all_to_all.10.rows, bf16[1024,256]{1,0:T(8,128)(2,1)S(1)} %bitcast.17, bf16[1024,256]{1,0:T(8,128)(2,1)S(1)} %bitcast.19, bf16[256,1024]{1,0:T(8,128)(2,1)S(1)} %bitcast.21, bf16[1024,256]{1,0:T(8,128)(2,1)S(1)} %collective-permute-done.3.gate_n, ...), custom_call_target="tpu_custom_call" | custom-call | tf_op jit(solution)/shard_map/expert/pallas_call | solution.py:285
  27.2 9.7 %all_to_all.11.back = bf16[8,8,1024]{2,1,0:T(8,128)(2,1)S(1)} all-to-all(bf16[8,8,1024]{2,1,0:T(8,128)(2,1)S(1)} %expert.1), channel_id=1, replica_groups=mesh['ep'=8,'tp'=4] {'ep'}, dimensions={0} | all-to-all | bytes 262144 | tf_op jit(solution)/shard_map/all_to_all | solution.py:383
  37.0 0.2 share.1
  37.1 0.1 collective-permute-start.6
  37.2 1.6 %collective-permute-start.8 = (bf16[8,1024]{1,0:T(8,128)(2,1)S(1)}, bf16[8,1024]{1,0:T(8,128)(2,1)S(1)}, u32[]{:S(2)}, u32[]{:S(2)}) collective-permute-start(bf16[8,1024]{1,0:T(8,128)(2,1)S(1)} %get-tuple-element.34.share), channel_id=1, source_target_pairs={{0,3},{1,2},{2,1},{3,0},{4,7},{5,6},{6,5},{7,4},{8,11},{9,10},{10,... | collective-permute-start | bytes 49160 | tf_op jit(solution)/shard_map/ppermute | solution.py:97
  38.8 0.5 %collective-permute-start.7 = (bf16[8,1024]{1,0:T(8,128)(2,1)S(1)}, bf16[8,1024]{1,0:T(8,128)(2,1)S(1)}, u32[]{:S(2)}, u32[]{:S(2)}) collective-permute-start(bf16[8,1024]{1,0:T(8,128)(2,1)S(1)} %get-tuple-element.34.share), channel_id=1, source_target_pairs={{0,2},{1,3},{2,0},{3,1},{4,6},{5,7},{6,4},{7,5},{8,10},{9,11},{10,... | collective-permute-start | bytes 49160 | tf_op jit(solution)/shard_map/ppermute | solution.py:97
  39.4 1.1 %collective-permute-done.8.other_far = bf16[8,1024]{1,0:T(8,128)(2,1)S(1)} collective-permute-done((bf16[8,1024]{1,0:T(8,128)(2,1)S(1)}, bf16[8,1024]{1,0:T(8,128)(2,1)S(1)}, u32[]{:S(2)}, u32[]{:S(2)}) %collective-permute-start.8) | collective-permute-done | bytes 16416 | tf_op jit(solution)/shard_map/ppermute | solution.py:97
  40.5 2.1 %collective-permute-done.7.other_y = bf16[8,1024]{1,0:T(8,128)(2,1)S(1)} collective-permute-done((bf16[8,1024]{1,0:T(8,128)(2,1)S(1)}, bf16[8,1024]{1,0:T(8,128)(2,1)S(1)}, u32[]{:S(2)}, u32[]{:S(2)}) %collective-permute-start.7) | collective-permute-done | bytes 16416 | tf_op jit(solution)/shard_map/ppermute | solution.py:97
  42.6 0.0 collective-permute-done.6.both
  42.6 0.0 copy-done.6
  42.6 0.7 %last.1 = bf16[16,256]{1,0:T(8,128)(2,1)} custom-call(bf16[8,1024]{1,0:T(8,128)(2,1)S(1)} %get-tuple-element.34.share, bf16[2,8,1024]{2,1,0:T(8,128)(2,1)S(1)} %collective-permute-done.6.both, bf16[8,1024]{1,0:T(8,128)(2,1)S(1)} %collective-permute-done.7.other_y, bf16[8,1024]{1,0:T(8,128)(2,1)S(1)} %collective-permute-done.8.other_far, ...), custom_call_target="tpu_custom_call" | custom-call | tf_op jit(solution)/shard_map/last/pallas_call | solution.py:346
  (1 shorter events, 0.0 us)
Async XLA Ops:
  0.0 13.1 %copy-start.3 = (bf16[16,1024]{1,0:T(8,128)(2,1)S(1)}, bf16[16,1024]{1,0:T(8,128)(2,1)}, u32[]{:S(2)}) copy-start(bf16[16,1024]{1,0:T(8,128)(2,1)} %refs_4_.1) | copy-start | bytes 98308
  0.0 4.9 %copy-start.2 = (bf16[1,256,1024]{2,1,0:T(8,128)(2,1)S(1)}, bf16[1,256,1024]{2,1,0:T(8,128)(2,1)}, u32[]{:S(2)}) copy-start(bf16[1,256,1024]{2,1,0:T(8,128)(2,1)} %param.40) | copy-start | bytes 1572868
  0.0 4.8 %copy-start.1 = (bf16[1,1024,256]{2,1,0:T(8,128)(2,1)S(1)}, bf16[1,1024,256]{2,1,0:T(8,128)(2,1)}, u32[]{:S(2)}) copy-start(bf16[1,1024,256]{2,1,0:T(8,128)(2,1)} %param.39) | copy-start | bytes 1572868
  0.0 4.2 %copy-start = (bf16[1,1024,256]{2,1,0:T(8,128)(2,1)S(1)}, bf16[1,1024,256]{2,1,0:T(8,128)(2,1)}, u32[]{:S(2)}) copy-start(bf16[1,1024,256]{2,1,0:T(8,128)(2,1)} %param.38) | copy-start | bytes 1572868
  0.0 11.1 %copy-start.7 = (f32[16,6]{0,1:T(8,128)S(1)}, f32[16,6]{0,1:T(8,128)}, u32[]{:S(2)}) copy-start(f32[16,6]{0,1:T(8,128)} %param.37) | copy-start | bytes 1156
  0.0 11.1 %copy-start.8 = (s32[16,6]{0,1:T(8,128)S(1)}, s32[16,6]{0,1:T(8,128)}, u32[]{:S(2)}) copy-start(s32[16,6]{0,1:T(8,128)} %param.36) | copy-start | bytes 1156
  0.0 13.1 %copy-start.5 = (f32[1024]{0:T(1024)S(1)}, f32[1024]{0:T(1024)}, u32[]{:S(2)}) copy-start(f32[1024]{0:T(1024)} %param.35) | copy-start | bytes 12292
  0.0 13.1 %copy-start.4 = (f32[1024]{0:T(1024)S(1)}, f32[1024]{0:T(1024)}, u32[]{:S(2)}) copy-start(f32[1024]{0:T(1024)} %param.34) | copy-start | bytes 12292
  4.2 22.2 %collective-permute-start.3 = (bf16[1024,256]{1,0:T(8,128)(2,1)S(1)}, bf16[1024,256]{1,0:T(8,128)(2,1)S(1)}, u32[]{:S(2)}, u32[]{:S(2)}) collective-permute-start(bf16[1024,256]{1,0:T(8,128)(2,1)S(1)} %bitcast.16), channel_id=1, source_target_pairs={{0,1},{1,0},{2,3},{3,2},{4,5},{5,4},{6,7},{7,6},{8,9},{9,8},{10,11... | collective-permute-start | bytes 1572872 | tf_op jit(solution)/shard_map/ppermute | solution.py:97
  4.8 21.7 %collective-permute-start.4 = (bf16[1024,256]{1,0:T(8,128)(2,1)S(1)}, bf16[1024,256]{1,0:T(8,128)(2,1)S(1)}, u32[]{:S(2)}, u32[]{:S(2)}) collective-permute-start(bf16[1024,256]{1,0:T(8,128)(2,1)S(1)} %bitcast.18), channel_id=1, source_target_pairs={{0,1},{1,0},{2,3},{3,2},{4,5},{5,4},{6,7},{7,6},{8,9},{9,8},{10,11... | collective-permute-start | bytes 1572872 | tf_op jit(solution)/shard_map/ppermute | solution.py:97
  4.9 21.6 %collective-permute-start.5 = (bf16[256,1024]{1,0:T(8,128)(2,1)S(1)}, bf16[256,1024]{1,0:T(8,128)(2,1)S(1)}, u32[]{:S(2)}, u32[]{:S(2)}) collective-permute-start(bf16[256,1024]{1,0:T(8,128)(2,1)S(1)} %bitcast.20), channel_id=1, source_target_pairs={{0,1},{1,0},{2,3},{3,2},{4,5},{5,4},{6,7},{7,6},{8,9},{9,8},{10,11... | collective-permute-start | bytes 1572872 | tf_op jit(solution)/shard_map/ppermute | solution.py:97
  5.3 4.1 %collective-permute-start.2 = (bf16[8,1024]{1,0:T(8,128)(2,1)S(1)}, bf16[8,1024]{1,0:T(8,128)(2,1)S(1)}, u32[]{:S(2)}, u32[]{:S(2)}) collective-permute-start(bf16[8,1024]{1,0:T(8,128)(2,1)S(1)} %get-tuple-element.22), channel_id=1, source_target_pairs={{0,3},{1,2},{2,1},{3,0},{4,7},{5,6},{6,5},{7,4},{8,11},{9,10},{10,... | collective-permute-start | bytes 49160 | tf_op jit(solution)/shard_map/ppermute | solution.py:97
  7.9 3.2 %collective-permute-start = (bf16[8,1024]{1,0:T(8,128)(2,1)S(1)}, bf16[8,1024]{1,0:T(8,128)(2,1)S(1)}, u32[]{:S(2)}, u32[]{:S(2)}) collective-permute-start(bf16[8,1024]{1,0:T(8,128)(2,1)S(1)} %get-tuple-element.22), channel_id=1, source_target_pairs={{0,1},{1,0},{2,3},{3,2},{4,5},{5,4},{6,7},{7,6},{8,9},{9,8},{10,11... | collective-permute-start | bytes 49160 | tf_op jit(solution)/shard_map/ppermute | solution.py:97
  9.4 3.7 %collective-permute-start.1 = (bf16[8,1024]{1,0:T(8,128)(2,1)S(1)}, bf16[8,1024]{1,0:T(8,128)(2,1)S(1)}, u32[]{:S(2)}, u32[]{:S(2)}) collective-permute-start(bf16[8,1024]{1,0:T(8,128)(2,1)S(1)} %get-tuple-element.21.refs_0_), channel_id=1, source_target_pairs={{0,2},{1,3},{2,0},{3,1},{4,6},{5,7},{6,4},{7,5},{8,10},{9,11},{10,... | collective-permute-start | bytes 49160 | tf_op jit(solution)/shard_map/ppermute | solution.py:97
  13.1 29.4 %copy-start.6 = (f32[256]{0:T(256)S(1)}, f32[256]{0:T(256)}, u32[]{:S(2)}) copy-start(f32[256]{0:T(256)} %param.41) | copy-start | bytes 3076
  37.1 5.4 %collective-permute-start.6 = (bf16[2,8,1024]{2,1,0:T(8,128)(2,1)S(1)}, bf16[2,8,1024]{2,1,0:T(8,128)(2,1)S(1)}, u32[]{:S(2)}, u32[]{:S(2)}) collective-permute-start(bf16[2,8,1024]{2,1,0:T(8,128)(2,1)S(1)} %get-tuple-element.35), channel_id=1, source_target_pairs={{0,1},{1,0},{2,3},{3,2},{4,5},{5,4},{6,7},{7,6},{8,9},{9,8},{10,11... | collective-permute-start | bytes 98312 | tf_op jit(solution)/shard_map/ppermute | solution.py:97
  37.2 3.2 %collective-permute-start.8 = (bf16[8,1024]{1,0:T(8,128)(2,1)S(1)}, bf16[8,1024]{1,0:T(8,128)(2,1)S(1)}, u32[]{:S(2)}, u32[]{:S(2)}) collective-permute-start(bf16[8,1024]{1,0:T(8,128)(2,1)S(1)} %get-tuple-element.34.share), channel_id=1, source_target_pairs={{0,3},{1,2},{2,1},{3,0},{4,7},{5,6},{6,5},{7,4},{8,11},{9,10},{10,... | collective-permute-start | bytes 49160 | tf_op jit(solution)/shard_map/ppermute | solution.py:97
  38.8 3.7 %collective-permute-start.7 = (bf16[8,1024]{1,0:T(8,128)(2,1)S(1)}, bf16[8,1024]{1,0:T(8,128)(2,1)S(1)}, u32[]{:S(2)}, u32[]{:S(2)}) collective-permute-start(bf16[8,1024]{1,0:T(8,128)(2,1)S(1)} %get-tuple-element.34.share), channel_id=1, source_target_pairs={{0,2},{1,3},{2,0},{3,1},{4,6},{5,7},{6,4},{7,5},{8,10},{9,11},{10,... | collective-permute-start | bytes 49160 | tf_op jit(solution)/shard_map/ppermute | solution.py:97

commit v6 on v5

--- a/solution.py
+++ b/solution.py
@@ -108,67 +108,78 @@
     return pl.BlockSpec(memory_space=pltpu.VMEM)
 
 
-def cell_body(heads, key_dim, value_dim, chunk, halves, *refs):
+def scan_body(heads, key_dim, chunk, *refs):
     f32 = jnp.float32
     bf16 = jnp.bfloat16
-    sources, outs, rest = refs[:13], refs[13 : 14 + halves], refs[14 + halves :]
-    targets, (recall, sems) = rest[:13], rest[13:]
-    (tokens, gain, wi, wf, ib, fb, scale, wq, wk, wv, mem, hg, wo) = targets
+    sources, outs, targets = refs[:11], refs[11:18], refs[18:27]
+    sems = refs[27]
+    recall, values, match, in_dot, forget_dot, hg, wo = outs
+    tokens, gain, wi, wf, scale, wq, wk, wv, mem = targets
     seqs = tokens.shape[0]
     count = seqs // chunk
-    pairs = list(zip(sources, targets))
-    pieces = [pairs[i] for i in (0, 1, 7, 2, 3, 4, 5, 6, 8)]
+    pairs = list(zip(sources, (*targets, hg, wo)))
+    pieces = [pairs[i] for i in (0, 1, 5, 2, 3, 4, 6)]
     for c in range(count):
         rows = pl.ds(c * chunk, chunk)
-        pieces.append((pairs[10][0].at[rows], mem.at[rows]))
-    pieces += [pairs[9], pairs[11], pairs[12]]
+        pieces.append((pairs[8][0].at[rows], mem.at[rows]))
+    pieces += [pairs[7], pairs[9], pairs[10]]
     copies = [pltpu.make_async_copy(src, dst, sems.at[i]) for i, (src, dst) in enumerate(pieces)]
     for copy in copies:
         copy.start()
     copies[0].wait()
     copies[1].wait()
     xf = tokens[...].astype(f32)
-    inv = lax.rsqrt(jnp.mean(xf * xf, axis=1, keepdims=True) + EPS)
-    normed = (xf * inv * gain[...]).astype(bf16)
+    normed = (xf * rms_scale(xf) * gain[...]).astype(bf16)
     copies[2].wait()
     query = jnp.dot(normed, wq[...], preferred_element_type=f32) * key_dim ** (-0.5)
-    for i in range(3, 8):
+    for i in range(3, 6):
         copies[i].wait()
     wide = normed.astype(f32)
     diagonal = lax.broadcasted_iota(jnp.int32, (seqs, seqs), 0) == lax.broadcasted_iota(
         jnp.int32, (seqs, seqs), 1
     )
-    carries, fresh = [], []
     for h in range(heads):
-        in_pre = jnp.sum(wide * wi[h : h + 1, :].astype(f32), axis=1, keepdims=True) + ib[:, h : h + 1]
-        forget = jnp.sum(wide * wf[h : h + 1, :].astype(f32), axis=1, keepdims=True) + fb[:, h : h + 1]
-        forget_log = jnp.minimum(forget, 0.0) - jnp.log1p(jnp.exp(-jnp.abs(forget)))
-        column = jnp.sum(jnp.where(diagonal, scale[h : h + 1, :], 0.0), axis=1, keepdims=True)
-        carried = forget_log + column
-        new_max = jnp.maximum(carried, in_pre)
-        carries.append(jnp.exp(carried - new_max))
-        fresh.append(jnp.exp(in_pre - new_max))
-    copies[8].wait()
+        row = slice(h, h + 1)
+        in_dot[:, row] = jnp.sum(wide * wi[row, :].astype(f32), axis=1, keepdims=True)
+        forget_dot[0, :, row] = jnp.sum(wide * wf[row, :].astype(f32), axis=1, keepdims=True)
+        column = jnp.sum(jnp.where(diagonal, scale[row, :], 0.0), axis=1, keepdims=True)
+        forget_dot[1, :, row] = column
+    copies[6].wait()
     keys = jnp.dot(normed, wk[...], preferred_element_type=f32)
+    for h in range(heads):
+        ks = slice(h * key_dim, (h + 1) * key_dim)
+        match[:, h : h + 1] = jnp.sum(query[:, ks] * keys[:, ks], axis=1, keepdims=True)
     turned = [query[:, h * key_dim : (h + 1) * key_dim].T for h in range(heads)]
     for c in range(count):
-        copies[9 + c].wait()
+        copies[7 + c].wait()
         for b in range(c * chunk, (c + 1) * chunk):
             for h in range(heads):
                 product = turned[h][:, b : b + 1] * mem[b, h]
                 recall[h, b : b + 1, :] = jnp.sum(product, axis=0, keepdims=True)
+    copies[7 + count].wait()
+    values[...] = jnp.dot(normed, wv[...], preferred_element_type=f32)
+    copies[8 + count].wait()
     copies[9 + count].wait()
-    copies[10 + count].wait()
-    values = jnp.dot(normed, wv[...], preferred_element_type=f32)
+
+
+def close_body(heads, halves, recall, values, match, in_dot, forget_dot, hg, wo, ib, fb, *outs):
+    f32 = jnp.float32
+    bf16 = jnp.bfloat16
+    value_dim = recall.shape[2]
+    seqs = values.shape[0]
     parts = []
     for h in range(heads):
-        ks = slice(h * key_dim, (h + 1) * key_dim)
+        one = slice(h, h + 1)
         vs = slice(h * value_dim, (h + 1) * value_dim)
-        match = jnp.sum(query[:, ks] * keys[:, ks], axis=1, keepdims=True)
-        read = carries[h] * recall[h] + (fresh[h] * match) * values[:, vs]
-        inv = lax.rsqrt(jnp.mean(read * read, axis=1, keepdims=True) + EPS)
-        parts.append((read * inv * hg[:, vs]).astype(bf16))
-    copies[11 + count].wait()
+        in_pre = in_dot[:, one] + ib[:, one]
+        forget = forget_dot[0, :, one] + fb[:, one]
+        forget_log = jnp.minimum(forget, 0.0) - jnp.log1p(jnp.exp(-jnp.abs(forget)))
+        carried = forget_log + forget_dot[1, :, one]
+        new_max = jnp.maximum(carried, in_pre)
+        carry = jnp.exp(carried - new_max)
+        fresh = jnp.exp(in_pre - new_max)
+        read = carry * recall[h] + (fresh * match[:, one]) * values[:, vs]
+        parts.append((read * rms_scale(read) * hg[:, vs]).astype(bf16))
     headout = parts[0] if heads == 1 else jnp.concatenate(parts, axis=1)
     product = jnp.dot(headout, wo[...], preferred_element_type=f32)
     if halves:
@@ -201,14 +212,13 @@
     seqs, width = tokens.shape
     heads, key_dim, value_dim = memory.shape[1:]
     chunk = 4 if seqs % 4 == 0 else 1
-    body = lambda *refs: cell_body(heads, key_dim, value_dim, chunk, halves, *refs)
+    stay = [(i, i) for i in range(lax.axis_size("tp"))]
+    biases = [lax.ppermute(b, "tp", stay).reshape(1, heads) for b in (igate_bias, fgate_bias)]
     operands = [
         tokens,
         mix_gain_in.reshape(1, width),
         w_igate.T,
         w_fgate.T,
-        igate_bias.reshape(1, heads),
-        fgate_bias.reshape(1, heads),
         log_scale.T,
         w_query,
         w_key,
@@ -217,20 +227,33 @@
         head_gain.reshape(1, heads * value_dim),
         w_output,
     ]
+    found = pl.pallas_call(
+        lambda *refs: scan_body(heads, key_dim, chunk, *refs),
+        out_shape=[
+            jax.ShapeDtypeStruct((heads, seqs, value_dim), f32),
+            jax.ShapeDtypeStruct((seqs, heads * value_dim), f32),
+            jax.ShapeDtypeStruct((seqs, heads), f32),
+            jax.ShapeDtypeStruct((seqs, heads), f32),
+            jax.ShapeDtypeStruct((2, seqs, heads), f32),
+            jax.ShapeDtypeStruct((1, heads * value_dim), f32),
+            jax.ShapeDtypeStruct(w_output.shape, bf16),
+        ],
+        in_specs=[pl.BlockSpec(memory_space=pltpu.HBM)] * len(operands),
+        out_specs=[whole()] * 7,
+        scratch_shapes=[pltpu.VMEM(o.shape, o.dtype) for o in operands[:9]]
+        + [pltpu.SemaphoreType.DMA((10 + seqs // chunk,))],
+        compiler_params=pltpu.CompilerParams(vmem_limit_bytes=12 << 20),
+        name="scan",
+    )(*[pltpu.with_memory_space_constraint(o, pltpu.HBM) for o in operands])
     shape = jax.ShapeDtypeStruct((seqs // 2 if halves else seqs, w_output.shape[1]), bf16)
     result = pl.pallas_call(
-        body,
+        lambda *refs: close_body(heads, halves, *refs),
         out_shape=[shape] * (2 if halves else 1),
-        in_specs=[pl.BlockSpec(memory_space=pltpu.HBM)] * len(operands),
+        in_specs=[whole()] * 9,
         out_specs=[whole()] * (2 if halves else 1),
-        scratch_shapes=[pltpu.VMEM(o.shape, o.dtype) for o in operands]
-        + [
-            pltpu.VMEM((heads, seqs, value_dim), f32),
-            pltpu.SemaphoreType.DMA((12 + seqs // chunk,)),
-        ],
-        compiler_params=pltpu.CompilerParams(vmem_limit_bytes=12 << 20),
-        name="cell",
-    )(*[o if o.size == heads else pltpu.with_memory_space_constraint(o, pltpu.HBM) for o in operands])
+        compiler_params=pltpu.CompilerParams(vmem_limit_bytes=8 << 20),
+        name="close",
+    )(*found, *biases)
     return result if halves else result[0]
 
 
@@ -368,8 +391,9 @@
 ):
     groups = lax.axis_size("ep")
     mine, theirs = halves
-    parts = [exchange(theirs if step % 2 else mine, "tp", step) for step in (1, 2, 3)]
-    parts = [mine] + parts
+    parts = [mine]
+    for step in (2, 3, 1):
+        parts.append(exchange(theirs if step % 2 else mine, "tp", step))
     shards = (expert_gate[0], expert_up[0], expert_down[0])
     *waited, _ = lax.optimization_barrier((*shards, mine))
     neighbour = [exchange(shard, "tp", 1) for shard in waited]
@@ -382,14 +406,10 @@
     blocks, weights, resid, gain_out = lax.optimization_barrier((blocks, weights, resid, gain_out))
     back = lax.all_to_all(blocks, "ep", split_axis=0, concat_axis=0, tiled=True)
     share, both = combine(back, weights, resid)
-    return last(
-        share,
-        exchange(both, "tp", 1),
-        exchange(share, "tp", 2),
-        exchange(share, "tp", 3),
-        resid,
-        gain_out,
-    )
+    sums = {}
+    for step in (2, 3, 1):
+        sums[step] = exchange(both if step == 1 else share, "tp", step)
+    return last(share, sums[1], sums[2], sums[3], resid, gain_out)
 
 
 def slotted(ffn_in, routes, route_weights, expert_gate, expert_up, expert_down, cap):

time: 43.5 us -> 45.5 us (1.046)
  starting transfers between devices: 7.67 us -> 11.1 us
  waiting for transfers between devices: 6.62 us -> 4.94 us
  between operations: 1.52 us -> 0.13 us
  Pallas kernels: 4.58 us -> 5.88 us
    ppermute x0 -> x2, starting transfers between devices: none -> 2.38 us  [cell(): lax.ppermute(b, 'tp', stay).reshape(1, heads)]
    ppermute x9, waiting for transfers between devices: 6.62 us -> 4.93 us  [exchange(): return lax.ppermute(value, axis, pairs)]
    pallas_call x1 -> x2, Pallas kernels: 2.77 us -> 4.07 us  [the longest x1 2.49 us: cell(): pl.pallas_call(lambda *refs: scan_body(heads, key_dim, chunk, *refs), out...]
    ppermute x9, starting transfers between devices: 7.67 us -> 8.67 us  [exchange(): return lax.ppermute(value, axis, pairs)]
  transfers between devices with their start and end apart: 9 -> 11, of which waited for: 4 -> 3; matrix products, arithmetic and copies ran while one was open for 0% -> 0% of each run, Pallas kernels for 0% -> 6%
where the time goes in v6:
time: 45.5 us; the launch traced here: 45.2 us
  blocking collectives  23.2 us (51%)
  starting transfers between devices  11.1 us (24%)
  Pallas kernels  5.88 us (13%)
  waiting for transfers between devices  4.94 us (11%)
    all_to_all x1, blocking collectives, every_token(): rows = lax.all_to_all(spread, 'ep', split_axis=0, concat_axis=0, tiled=True)  13.4 us
    all_to_all x1, blocking collectives, every_token(): back = lax.all_to_all(blocks, 'ep', split_axis=0, concat_axis=0, tiled=True)  9.74 us
    ppermute x9, starting transfers between devices, exchange(): return lax.ppermute(value, axis, pairs)  8.67 us
    ppermute x9, waiting for transfers between devices, exchange(): return lax.ppermute(value, axis, pairs)  4.93 us
    pallas_call x1, Pallas kernels, cell(): pl.pallas_call(lambda *refs: scan_body(heads, key_dim, chunk, *refs), out...  2.49 us
    ppermute x2, starting transfers between devices, cell(): lax.ppermute(b, 'tp', stay).reshape(1, heads)  2.38 us
    pallas_call x1, Pallas kernels, cell(): pl.pallas_call(lambda *refs: close_body(heads, halves, *refs), out_shape=...  1.58 us
  transfers between devices with their start and end apart: 11, of which 3 were waited for; matrix products, arithmetic and copies ran while one was open for 0% of the time, Pallas kernels for 6%

profile of v6, /device:TPU:0, one launch (start us, length us, event | category | flops | bytes accessed | tf_op | source)
XLA Modules:
  0.0 45.2 jit_solution(3256765884357047640)
XLA Ops:
  0.0 1.2 %collective-permute-start = (f32[1]{0:T(128)}, f32[1]{0:T(128)}, u32[]{:S(2)}, u32[]{:S(2)}) collective-permute-start(f32[1]{0:T(128)} %param.30), channel_id=1, source_target_pairs={{0,0},{1,1},{2,2},{3,3},{4,4},{5,5},{6,6},{7,7},{8,8},{9,9},{10,10... | collective-permute-start | bytes 20 | tf_op jit(solution)/shard_map/ppermute | solution.py:216
  1.2 1.2 %collective-permute-start.1 = (f32[1]{0:T(128)}, f32[1]{0:T(128)}, u32[]{:S(2)}, u32[]{:S(2)}) collective-permute-start(f32[1]{0:T(128)} %param.31), channel_id=1, source_target_pairs={{0,0},{1,1},{2,2},{3,3},{4,4},{5,5},{6,6},{7,7},{8,8},{9,9},{10,10... | collective-permute-start | bytes 20 | tf_op jit(solution)/shard_map/ppermute | solution.py:216
  2.4 0.0 copy-start
  2.4 0.0 copy-start.1
  2.4 0.0 copy-start.2
  2.4 0.0 copy-start.7
  2.4 0.0 copy-start.8
  2.4 0.0 copy-start.3
  2.4 0.0 copy-start.4
  2.4 0.0 copy-start.5
  2.4 2.5 %scan.1 = (f32[1,16,256]{2,1,0:T(8,128)S(1)}, f32[16,256]{1,0:T(8,128)S(1)}, f32[16,1]{1,0:T(8,128)S(1)}, f32[16,1]{1,0:T(8,128)S(1)}, f32[2,16,1]{2,1,0:T(8,128...) custom-call(bf16[16,1024]{1,0:T(8,128)(2,1)} %refs_4_.1, f32[1,1024]{1,0:T(1,128)} %bitcast.24, ...), custom_call_target="tpu_custom_call" | custom-call | tf_op jit(solution)/shard_map/scan/pallas_call | solution.py:230
  4.9 0.0 collective-permute-done
  4.9 0.0 collective-permute-done.1
  4.9 1.6 %close.1 = (bf16[8,1024]{1,0:T(8,128)(2,1)S(1)}, bf16[8,1024]{1,0:T(8,128)(2,1)S(1)}) custom-call(f32[1,16,256]{2,1,0:T(8,128)S(1)} %get-tuple-element.28.refs_0_, f32[16,256]{1,0:T(8,128)S(1)} %get-tuple-element.29.refs_1_, f32[16,1]{1,0:T(8,128)S(1)} %get-tuple-element.30.refs_2_, f32[16,1]{1,0:T(8,128)S(1)} %get-tuple-element.31.refs_3_, ...), custom_call_target="tpu_custom_call" | custom-call | tf_op jit(solution)/shard_map/close/pallas_call | solution.py:249
  6.5 0.0 copy-done
  6.5 0.5 %collective-permute-start.5 = (bf16[1024,256]{1,0:T(8,128)(2,1)S(1)}, bf16[1024,256]{1,0:T(8,128)(2,1)S(1)}, u32[]{:S(2)}, u32[]{:S(2)}) collective-permute-start(bf16[1024,256]{1,0:T(8,128)(2,1)S(1)} %bitcast.14), channel_id=1, source_target_pairs={{0,1},{1,0},{2,3},{3,2},{4,5},{5,4},{6,7},{7,6},{8,9},{9,8},{10,11... | collective-permute-start | bytes 1572872 | tf_op jit(solution)/shard_map/ppermute | solution.py:97
  7.1 0.0 copy-done.1
  7.1 0.1 collective-permute-start.6
  7.2 0.0 copy-done.2
  7.2 0.4 collective-permute-start.7
  7.6 0.1 collective-permute-start.4
  7.7 2.6 %collective-permute-start.3 = (bf16[8,1024]{1,0:T(8,128)(2,1)S(1)}, bf16[8,1024]{1,0:T(8,128)(2,1)S(1)}, u32[]{:S(2)}, u32[]{:S(2)}) collective-permute-start(bf16[8,1024]{1,0:T(8,128)(2,1)S(1)} %get-tuple-element.36), channel_id=1, source_target_pairs={{0,3},{1,2},{2,1},{3,0},{4,7},{5,6},{6,5},{7,4},{8,11},{9,10},{10,... | collective-permute-start | bytes 49160 | tf_op jit(solution)/shard_map/ppermute | solution.py:97
  10.3 0.0 collective-permute-done.4.refs_3_
  10.3 2.7 %collective-permute-start.2 = (bf16[8,1024]{1,0:T(8,128)(2,1)S(1)}, bf16[8,1024]{1,0:T(8,128)(2,1)S(1)}, u32[]{:S(2)}, u32[]{:S(2)}) collective-permute-start(bf16[8,1024]{1,0:T(8,128)(2,1)S(1)} %get-tuple-element.35.refs_0_), channel_id=1, source_target_pairs={{0,2},{1,3},{2,0},{3,1},{4,6},{5,7},{6,4},{7,5},{8,10},{9,11},{10,... | collective-permute-start | bytes 49160 | tf_op jit(solution)/shard_map/ppermute | solution.py:97
  13.0 0.0 copy-done.7
  13.0 0.0 copy-done.8
  13.0 0.0 collective-permute-done.3.refs_2_
  13.0 1.7 %collective-permute-done.2.refs_1_ = bf16[8,1024]{1,0:T(8,128)(2,1)S(1)} collective-permute-done((bf16[8,1024]{1,0:T(8,128)(2,1)S(1)}, bf16[8,1024]{1,0:T(8,128)(2,1)S(1)}, u32[]{:S(2)}, u32[]{:S(2)}) %collective-permute-start.2) | collective-permute-done | bytes 16416 | tf_op jit(solution)/shard_map/ppermute | solution.py:97
  14.7 0.0 copy-done.3
  14.7 0.0 copy-done.4
  14.7 0.0 copy-done.5
  14.7 0.0 copy-start.6
  14.8 0.2 after_mix.1
  15.0 13.4 %all_to_all.10.rows = bf16[8,8,1024]{2,1,0:T(8,128)(2,1)S(1)} all-to-all(bf16[8,8,1024]{2,1,0:T(8,128)(2,1)S(1)} %get-tuple-element.38), channel_id=1, replica_groups=mesh['ep'=8,'tp'=4] {'ep'}, dimensions={0} | all-to-all | bytes 262144 | tf_op jit(solution)/shard_map/all_to_all | solution.py:404
  28.4 0.0 collective-permute-done.5.gate_n
  28.4 0.0 collective-permute-done.6.up_n
  28.4 0.0 collective-permute-done.7.down_n
  28.4 0.7 %expert.1 = bf16[8,8,1024]{2,1,0:T(8,128)(2,1)S(1)} custom-call(bf16[8,8,1024]{2,1,0:T(8,128)(2,1)S(1)} %all_to_all.10.rows, bf16[1024,256]{1,0:T(8,128)(2,1)S(1)} %bitcast.15, bf16[1024,256]{1,0:T(8,128)(2,1)S(1)} %bitcast.17, bf16[256,1024]{1,0:T(8,128)(2,1)S(1)} %bitcast.19, bf16[1024,256]{1,0:T(8,128)(2,1)S(1)} %collective-permute-done.5.gate_n, ...), custom_call_target="tpu_custom_call" | custom-call | tf_op jit(solution)/shard_map/expert/pallas_call | solution.py:308
  29.2 9.7 %all_to_all.11.back = bf16[8,8,1024]{2,1,0:T(8,128)(2,1)S(1)} all-to-all(bf16[8,8,1024]{2,1,0:T(8,128)(2,1)S(1)} %expert.1), channel_id=1, replica_groups=mesh['ep'=8,'tp'=4] {'ep'}, dimensions={0} | all-to-all | bytes 262144 | tf_op jit(solution)/shard_map/all_to_all | solution.py:407
  38.9 0.2 share.1
  39.1 0.1 collective-permute-start.8
  39.2 1.6 %collective-permute-start.10 = (bf16[8,1024]{1,0:T(8,128)(2,1)S(1)}, bf16[8,1024]{1,0:T(8,128)(2,1)S(1)}, u32[]{:S(2)}, u32[]{:S(2)}) collective-permute-start(bf16[8,1024]{1,0:T(8,128)(2,1)S(1)} %get-tuple-element.48.share), channel_id=1, source_target_pairs={{0,3},{1,2},{2,1},{3,0},{4,7},{5,6},{6,5},{7,4},{8,11},{9,10},{10,... | collective-permute-start | bytes 49160 | tf_op jit(solution)/shard_map/ppermute | solution.py:97
  40.8 0.5 %collective-permute-start.9 = (bf16[8,1024]{1,0:T(8,128)(2,1)S(1)}, bf16[8,1024]{1,0:T(8,128)(2,1)S(1)}, u32[]{:S(2)}, u32[]{:S(2)}) collective-permute-start(bf16[8,1024]{1,0:T(8,128)(2,1)S(1)} %get-tuple-element.48.share), channel_id=1, source_target_pairs={{0,2},{1,3},{2,0},{3,1},{4,6},{5,7},{6,4},{7,5},{8,10},{9,11},{10,... | collective-permute-start | bytes 49160 | tf_op jit(solution)/shard_map/ppermute | solution.py:97
  41.3 1.1 %collective-permute-done.10.other_far = bf16[8,1024]{1,0:T(8,128)(2,1)S(1)} collective-permute-done((bf16[8,1024]{1,0:T(8,128)(2,1)S(1)}, bf16[8,1024]{1,0:T(8,128)(2,1)S(1)}, u32[]{:S(2)}, u32[]{:S(2)}) %collective-permute-start.10) | collective-permute-done | bytes 16416 | tf_op jit(solution)/shard_map/ppermute | solution.py:97
  42.4 2.1 %collective-permute-done.9.other_y = bf16[8,1024]{1,0:T(8,128)(2,1)S(1)} collective-permute-done((bf16[8,1024]{1,0:T(8,128)(2,1)S(1)}, bf16[8,1024]{1,0:T(8,128)(2,1)S(1)}, u32[]{:S(2)}, u32[]{:S(2)}) %collective-permute-start.9) | collective-permute-done | bytes 16416 | tf_op jit(solution)/shard_map/ppermute | solution.py:97
  44.5 0.0 collective-permute-done.8.both
  44.5 0.0 copy-done.6
  44.5 0.7 %last.1 = bf16[16,256]{1,0:T(8,128)(2,1)} custom-call(bf16[8,1024]{1,0:T(8,128)(2,1)S(1)} %get-tuple-element.48.share, bf16[2,8,1024]{2,1,0:T(8,128)(2,1)S(1)} %collective-permute-done.8.both, bf16[8,1024]{1,0:T(8,128)(2,1)S(1)} %collective-permute-done.9.other_y, bf16[8,1024]{1,0:T(8,128)(2,1)S(1)} %collective-permute-done.10.other_far, ...), custom_call_target="tpu_custom_call" | custom-call | tf_op jit(solution)/shard_map/last/pallas_call | solution.py:369
  (1 shorter events, 0.0 us)
Async XLA Ops:
  0.0 4.9 %collective-permute-start = (f32[1]{0:T(128)}, f32[1]{0:T(128)}, u32[]{:S(2)}, u32[]{:S(2)}) collective-permute-start(f32[1]{0:T(128)} %param.30), channel_id=1, source_target_pairs={{0,0},{1,1},{2,2},{3,3},{4,4},{5,5},{6,6},{7,7},{8,8},{9,9},{10,10... | collective-permute-start | bytes 20 | tf_op jit(solution)/shard_map/ppermute | solution.py:216
  1.2 3.8 %collective-permute-start.1 = (f32[1]{0:T(128)}, f32[1]{0:T(128)}, u32[]{:S(2)}, u32[]{:S(2)}) collective-permute-start(f32[1]{0:T(128)} %param.31), channel_id=1, source_target_pairs={{0,0},{1,1},{2,2},{3,3},{4,4},{5,5},{6,6},{7,7},{8,8},{9,9},{10,10... | collective-permute-start | bytes 20 | tf_op jit(solution)/shard_map/ppermute | solution.py:216
  2.4 4.2 %copy-start = (bf16[1,1024,256]{2,1,0:T(8,128)(2,1)S(1)}, bf16[1,1024,256]{2,1,0:T(8,128)(2,1)}, u32[]{:S(2)}) copy-start(bf16[1,1024,256]{2,1,0:T(8,128)(2,1)} %param.38) | copy-start | bytes 1572868
  2.4 4.7 %copy-start.1 = (bf16[1,1024,256]{2,1,0:T(8,128)(2,1)S(1)}, bf16[1,1024,256]{2,1,0:T(8,128)(2,1)}, u32[]{:S(2)}) copy-start(bf16[1,1024,256]{2,1,0:T(8,128)(2,1)} %param.39) | copy-start | bytes 1572868
  2.4 4.8 %copy-start.2 = (bf16[1,256,1024]{2,1,0:T(8,128)(2,1)S(1)}, bf16[1,256,1024]{2,1,0:T(8,128)(2,1)}, u32[]{:S(2)}) copy-start(bf16[1,256,1024]{2,1,0:T(8,128)(2,1)} %param.40) | copy-start | bytes 1572868
  2.4 10.6 %copy-start.7 = (f32[16,6]{0,1:T(8,128)S(1)}, f32[16,6]{0,1:T(8,128)}, u32[]{:S(2)}) copy-start(f32[16,6]{0,1:T(8,128)} %param.37) | copy-start | bytes 1156
  2.4 10.6 %copy-start.8 = (s32[16,6]{0,1:T(8,128)S(1)}, s32[16,6]{0,1:T(8,128)}, u32[]{:S(2)}) copy-start(s32[16,6]{0,1:T(8,128)} %param.36) | copy-start | bytes 1156
  2.4 12.3 %copy-start.3 = (bf16[16,1024]{1,0:T(8,128)(2,1)S(1)}, bf16[16,1024]{1,0:T(8,128)(2,1)}, u32[]{:S(2)}) copy-start(bf16[16,1024]{1,0:T(8,128)(2,1)} %refs_4_.1) | copy-start | bytes 98308
  2.4 12.3 %copy-start.4 = (f32[1024]{0:T(1024)S(1)}, f32[1024]{0:T(1024)}, u32[]{:S(2)}) copy-start(f32[1024]{0:T(1024)} %param.34) | copy-start | bytes 12292
  2.4 12.3 %copy-start.5 = (f32[1024]{0:T(1024)S(1)}, f32[1024]{0:T(1024)}, u32[]{:S(2)}) copy-start(f32[1024]{0:T(1024)} %param.35) | copy-start | bytes 12292
  6.5 21.9 %collective-permute-start.5 = (bf16[1024,256]{1,0:T(8,128)(2,1)S(1)}, bf16[1024,256]{1,0:T(8,128)(2,1)S(1)}, u32[]{:S(2)}, u32[]{:S(2)}) collective-permute-start(bf16[1024,256]{1,0:T(8,128)(2,1)S(1)} %bitcast.14), channel_id=1, source_target_pairs={{0,1},{1,0},{2,3},{3,2},{4,5},{5,4},{6,7},{7,6},{8,9},{9,8},{10,11... | collective-permute-start | bytes 1572872 | tf_op jit(solution)/shard_map/ppermute | solution.py:97
  7.1 21.3 %collective-permute-start.6 = (bf16[1024,256]{1,0:T(8,128)(2,1)S(1)}, bf16[1024,256]{1,0:T(8,128)(2,1)S(1)}, u32[]{:S(2)}, u32[]{:S(2)}) collective-permute-start(bf16[1024,256]{1,0:T(8,128)(2,1)S(1)} %bitcast.16), channel_id=1, source_target_pairs={{0,1},{1,0},{2,3},{3,2},{4,5},{5,4},{6,7},{7,6},{8,9},{9,8},{10,11... | collective-permute-start | bytes 1572872 | tf_op jit(solution)/shard_map/ppermute | solution.py:97
  7.2 21.3 %collective-permute-start.7 = (bf16[256,1024]{1,0:T(8,128)(2,1)S(1)}, bf16[256,1024]{1,0:T(8,128)(2,1)S(1)}, u32[]{:S(2)}, u32[]{:S(2)}) collective-permute-start(bf16[256,1024]{1,0:T(8,128)(2,1)S(1)} %bitcast.18), channel_id=1, source_target_pairs={{0,1},{1,0},{2,3},{3,2},{4,5},{5,4},{6,7},{7,6},{8,9},{9,8},{10,11... | collective-permute-start | bytes 1572872 | tf_op jit(solution)/shard_map/ppermute | solution.py:97
  7.6 2.7 %collective-permute-start.4 = (bf16[8,1024]{1,0:T(8,128)(2,1)S(1)}, bf16[8,1024]{1,0:T(8,128)(2,1)S(1)}, u32[]{:S(2)}, u32[]{:S(2)}) collective-permute-start(bf16[8,1024]{1,0:T(8,128)(2,1)S(1)} %get-tuple-element.36), channel_id=1, source_target_pairs={{0,1},{1,0},{2,3},{3,2},{4,5},{5,4},{6,7},{7,6},{8,9},{9,8},{10,11... | collective-permute-start | bytes 49160 | tf_op jit(solution)/shard_map/ppermute | solution.py:97
  7.7 5.4 %collective-permute-start.3 = (bf16[8,1024]{1,0:T(8,128)(2,1)S(1)}, bf16[8,1024]{1,0:T(8,128)(2,1)S(1)}, u32[]{:S(2)}, u32[]{:S(2)}) collective-permute-start(bf16[8,1024]{1,0:T(8,128)(2,1)S(1)} %get-tuple-element.36), channel_id=1, source_target_pairs={{0,3},{1,2},{2,1},{3,0},{4,7},{5,6},{6,5},{7,4},{8,11},{9,10},{10,... | collective-permute-start | bytes 49160 | tf_op jit(solution)/shard_map/ppermute | solution.py:97
  10.3 4.4 %collective-permute-start.2 = (bf16[8,1024]{1,0:T(8,128)(2,1)S(1)}, bf16[8,1024]{1,0:T(8,128)(2,1)S(1)}, u32[]{:S(2)}, u32[]{:S(2)}) collective-permute-start(bf16[8,1024]{1,0:T(8,128)(2,1)S(1)} %get-tuple-element.35.refs_0_), channel_id=1, source_target_pairs={{0,2},{1,3},{2,0},{3,1},{4,6},{5,7},{6,4},{7,5},{8,10},{9,11},{10,... | collective-permute-start | bytes 49160 | tf_op jit(solution)/shard_map/ppermute | solution.py:97
  14.7 29.8 %copy-start.6 = (f32[256]{0:T(256)S(1)}, f32[256]{0:T(256)}, u32[]{:S(2)}) copy-start(f32[256]{0:T(256)} %param.41) | copy-start | bytes 3076
  39.1 5.4 %collective-permute-start.8 = (bf16[2,8,1024]{2,1,0:T(8,128)(2,1)S(1)}, bf16[2,8,1024]{2,1,0:T(8,128)(2,1)S(1)}, u32[]{:S(2)}, u32[]{:S(2)}) collective-permute-start(bf16[2,8,1024]{2,1,0:T(8,128)(2,1)S(1)} %get-tuple-element.49), channel_id=1, source_target_pairs={{0,1},{1,0},{2,3},{3,2},{4,5},{5,4},{6,7},{7,6},{8,9},{9,8},{10,11... | collective-permute-start | bytes 98312 | tf_op jit(solution)/shard_map/ppermute | solution.py:97
  39.2 3.2 %collective-permute-start.10 = (bf16[8,1024]{1,0:T(8,128)(2,1)S(1)}, bf16[8,1024]{1,0:T(8,128)(2,1)S(1)}, u32[]{:S(2)}, u32[]{:S(2)}) collective-permute-start(bf16[8,1024]{1,0:T(8,128)(2,1)S(1)} %get-tuple-element.48.share), channel_id=1, source_target_pairs={{0,3},{1,2},{2,1},{3,0},{4,7},{5,6},{6,5},{7,4},{8,11},{9,10},{10,... | collective-permute-start | bytes 49160 | tf_op jit(solution)/shard_map/ppermute | solution.py:97
  40.8 3.7 %collective-permute-start.9 = (bf16[8,1024]{1,0:T(8,128)(2,1)S(1)}, bf16[8,1024]{1,0:T(8,128)(2,1)S(1)}, u32[]{:S(2)}, u32[]{:S(2)}) collective-permute-start(bf16[8,1024]{1,0:T(8,128)(2,1)S(1)} %get-tuple-element.48.share), channel_id=1, source_target_pairs={{0,2},{1,3},{2,0},{3,1},{4,6},{5,7},{6,4},{7,5},{8,10},{9,11},{10,... | collective-permute-start | bytes 49160 | tf_op jit(solution)/shard_map/ppermute | solution.py:97

commit v7 on v5

--- a/solution.py
+++ b/solution.py
@@ -368,8 +368,9 @@
 ):
     groups = lax.axis_size("ep")
     mine, theirs = halves
-    parts = [exchange(theirs if step % 2 else mine, "tp", step) for step in (1, 2, 3)]
-    parts = [mine] + parts
+    parts = [mine]
+    for step in (2, 3, 1):
+        parts.append(exchange(theirs if step % 2 else mine, "tp", step))
     shards = (expert_gate[0], expert_up[0], expert_down[0])
     *waited, _ = lax.optimization_barrier((*shards, mine))
     neighbour = [exchange(shard, "tp", 1) for shard in waited]
@@ -382,14 +383,10 @@
     blocks, weights, resid, gain_out = lax.optimization_barrier((blocks, weights, resid, gain_out))
     back = lax.all_to_all(blocks, "ep", split_axis=0, concat_axis=0, tiled=True)
     share, both = combine(back, weights, resid)
-    return last(
-        share,
-        exchange(both, "tp", 1),
-        exchange(share, "tp", 2),
-        exchange(share, "tp", 3),
-        resid,
-        gain_out,
-    )
+    sums = {}
+    for step in (3, 2, 1):
+        sums[step] = exchange(both if step == 1 else share, "tp", step)
+    return last(share, sums[1], sums[2], sums[3], resid, gain_out)
 
 
 def slotted(ffn_in, routes, route_weights, expert_gate, expert_up, expert_down, cap):

time: 43.5 us -> 43.2 us (level)
  waiting for transfers between devices: 6.62 us -> 4.94 us
  starting transfers between devices: 7.67 us -> 8.7 us
    ppermute x9, waiting for transfers between devices: 6.62 us -> 4.94 us  [exchange(): return lax.ppermute(value, axis, pairs)]
    ppermute x9, starting transfers between devices: 7.67 us -> 8.7 us  [exchange(): return lax.ppermute(value, axis, pairs)]
  transfers between devices with their start and end apart: 9 -> 9, of which waited for: 4 -> 3; matrix products, arithmetic and copies ran while one was open for 0% -> 0% of each run, Pallas kernels for 0% -> 0%
where the time goes in v7:
time: 43.2 us; the launch traced here: 43 us
  blocking collectives  23.2 us (54%)
  starting transfers between devices  8.7 us (20%)
  waiting for transfers between devices  4.94 us (11%)
  Pallas kernels  4.58 us (11%)
  between operations  1.52 us (4%)
    all_to_all x1, blocking collectives, every_token(): rows = lax.all_to_all(spread, 'ep', split_axis=0, concat_axis=0, tiled=True)  13.4 us
    all_to_all x1, blocking collectives, every_token(): back = lax.all_to_all(blocks, 'ep', split_axis=0, concat_axis=0, tiled=True)  9.74 us
    ppermute x9, starting transfers between devices, exchange(): return lax.ppermute(value, axis, pairs)  8.7 us
    ppermute x9, waiting for transfers between devices, exchange(): return lax.ppermute(value, axis, pairs)  4.94 us
    pallas_call x1, Pallas kernels, cell(): pl.pallas_call(body, out_shape=[shape] * (2 if halves else 1), in_specs=[...  2.77 us
  transfers between devices with their start and end apart: 9, of which 3 were waited for; matrix products, arithmetic and copies ran while one was open for 0% of the time, Pallas kernels for 0%

profile of v7, /device:TPU:0, one launch (start us, length us, event | category | flops | bytes accessed | tf_op | source)
XLA Modules:
  0.0 43.0 jit_solution(7595055900158832473)
XLA Ops:
  0.0 0.0 copy-start.3
  0.0 0.0 copy-start.2
  0.0 0.0 copy-start.1
  0.0 0.0 copy-start
  0.0 0.0 copy-start.7
  0.0 0.0 copy-start.8
  0.0 0.0 copy-start.5
  0.0 0.0 copy-start.4
  1.4 2.8 %cell.1 = (bf16[8,1024]{1,0:T(8,128)(2,1)S(1)}, bf16[8,1024]{1,0:T(8,128)(2,1)S(1)}) custom-call(bf16[16,1024]{1,0:T(8,128)(2,1)} %refs_4_.1, f32[1,1024]{1,0:T(1,128)} %bitcast.26, bf16[1,1024]{1,0:T(2,128)(2,1)} %bitcast.27, bf16[1,1024]{1,0:T(2,128)(2,1)} %bitcast.28, f32[1,1]{1,0:T(1,128)} %bitcast.14.refs_4_, f32[1,1]{1,0:T(1,128)} %bitcast.15.refs_5_, ...), custom_call_target="tpu_custom_call" | custom-call | tf_op jit(solution)/shard_map/cell/pallas_call | solution.py:221
  4.2 0.0 copy-done
  4.2 0.6 %collective-permute-start.3 = (bf16[1024,256]{1,0:T(8,128)(2,1)S(1)}, bf16[1024,256]{1,0:T(8,128)(2,1)S(1)}, u32[]{:S(2)}, u32[]{:S(2)}) collective-permute-start(bf16[1024,256]{1,0:T(8,128)(2,1)S(1)} %bitcast.16), channel_id=1, source_target_pairs={{0,1},{1,0},{2,3},{3,2},{4,5},{5,4},{6,7},{7,6},{8,9},{9,8},{10,11... | collective-permute-start | bytes 1572872 | tf_op jit(solution)/shard_map/ppermute | solution.py:97
  4.8 0.0 copy-done.1
  4.8 0.1 collective-permute-start.4
  4.9 0.0 copy-done.2
  4.9 0.4 collective-permute-start.5
  5.3 0.1 collective-permute-start.2
  5.4 2.6 %collective-permute-start.1 = (bf16[8,1024]{1,0:T(8,128)(2,1)S(1)}, bf16[8,1024]{1,0:T(8,128)(2,1)S(1)}, u32[]{:S(2)}, u32[]{:S(2)}) collective-permute-start(bf16[8,1024]{1,0:T(8,128)(2,1)S(1)} %get-tuple-element.22), channel_id=1, source_target_pairs={{0,3},{1,2},{2,1},{3,0},{4,7},{5,6},{6,5},{7,4},{8,11},{9,10},{10,... | collective-permute-start | bytes 49160 | tf_op jit(solution)/shard_map/ppermute | solution.py:97
  8.0 0.0 collective-permute-done.2.refs_3_
  8.0 2.7 %collective-permute-start = (bf16[8,1024]{1,0:T(8,128)(2,1)S(1)}, bf16[8,1024]{1,0:T(8,128)(2,1)S(1)}, u32[]{:S(2)}, u32[]{:S(2)}) collective-permute-start(bf16[8,1024]{1,0:T(8,128)(2,1)S(1)} %get-tuple-element.21.refs_0_), channel_id=1, source_target_pairs={{0,2},{1,3},{2,0},{3,1},{4,6},{5,7},{6,4},{7,5},{8,10},{9,11},{10,... | collective-permute-start | bytes 49160 | tf_op jit(solution)/shard_map/ppermute | solution.py:97
  10.7 0.0 copy-done.7
  10.8 0.0 copy-done.8
  10.8 0.0 collective-permute-done.1.refs_2_
  10.8 1.7 %collective-permute-done.refs_1_ = bf16[8,1024]{1,0:T(8,128)(2,1)S(1)} collective-permute-done((bf16[8,1024]{1,0:T(8,128)(2,1)S(1)}, bf16[8,1024]{1,0:T(8,128)(2,1)S(1)}, u32[]{:S(2)}, u32[]{:S(2)}) %collective-permute-start) | collective-permute-done | bytes 16416 | tf_op jit(solution)/shard_map/ppermute | solution.py:97
  12.5 0.0 copy-done.3
  12.5 0.0 copy-done.5
  12.5 0.0 copy-done.4
  12.5 0.0 copy-start.6
  12.5 0.2 after_mix.1
  12.7 13.4 %all_to_all.10.rows = bf16[8,8,1024]{2,1,0:T(8,128)(2,1)S(1)} all-to-all(bf16[8,8,1024]{2,1,0:T(8,128)(2,1)S(1)} %get-tuple-element.24), channel_id=1, replica_groups=mesh['ep'=8,'tp'=4] {'ep'}, dimensions={0} | all-to-all | bytes 262144 | tf_op jit(solution)/shard_map/all_to_all | solution.py:381
  26.1 0.0 collective-permute-done.3.gate_n
  26.2 0.0 collective-permute-done.4.up_n
  26.2 0.0 collective-permute-done.5.down_n
  26.2 0.7 %expert.1 = bf16[8,8,1024]{2,1,0:T(8,128)(2,1)S(1)} custom-call(bf16[8,8,1024]{2,1,0:T(8,128)(2,1)S(1)} %all_to_all.10.rows, bf16[1024,256]{1,0:T(8,128)(2,1)S(1)} %bitcast.17, bf16[1024,256]{1,0:T(8,128)(2,1)S(1)} %bitcast.19, bf16[256,1024]{1,0:T(8,128)(2,1)S(1)} %bitcast.21, bf16[1024,256]{1,0:T(8,128)(2,1)S(1)} %collective-permute-done.3.gate_n, ...), custom_call_target="tpu_custom_call" | custom-call | tf_op jit(solution)/shard_map/expert/pallas_call | solution.py:285
  26.9 9.7 %all_to_all.11.back = bf16[8,8,1024]{2,1,0:T(8,128)(2,1)S(1)} all-to-all(bf16[8,8,1024]{2,1,0:T(8,128)(2,1)S(1)} %expert.1), channel_id=1, replica_groups=mesh['ep'=8,'tp'=4] {'ep'}, dimensions={0} | all-to-all | bytes 262144 | tf_op jit(solution)/shard_map/all_to_all | solution.py:384
  36.6 0.2 share.1
  36.8 0.1 collective-permute-start.6
  36.9 1.6 %collective-permute-start.8 = (bf16[8,1024]{1,0:T(8,128)(2,1)S(1)}, bf16[8,1024]{1,0:T(8,128)(2,1)S(1)}, u32[]{:S(2)}, u32[]{:S(2)}) collective-permute-start(bf16[8,1024]{1,0:T(8,128)(2,1)S(1)} %get-tuple-element.34.share), channel_id=1, source_target_pairs={{0,3},{1,2},{2,1},{3,0},{4,7},{5,6},{6,5},{7,4},{8,11},{9,10},{10,... | collective-permute-start | bytes 49160 | tf_op jit(solution)/shard_map/ppermute | solution.py:97
  38.5 0.5 %collective-permute-start.7 = (bf16[8,1024]{1,0:T(8,128)(2,1)S(1)}, bf16[8,1024]{1,0:T(8,128)(2,1)S(1)}, u32[]{:S(2)}, u32[]{:S(2)}) collective-permute-start(bf16[8,1024]{1,0:T(8,128)(2,1)S(1)} %get-tuple-element.34.share), channel_id=1, source_target_pairs={{0,2},{1,3},{2,0},{3,1},{4,6},{5,7},{6,4},{7,5},{8,10},{9,11},{10,... | collective-permute-start | bytes 49160 | tf_op jit(solution)/shard_map/ppermute | solution.py:97
  39.0 1.1 %collective-permute-done.8.other_far = bf16[8,1024]{1,0:T(8,128)(2,1)S(1)} collective-permute-done((bf16[8,1024]{1,0:T(8,128)(2,1)S(1)}, bf16[8,1024]{1,0:T(8,128)(2,1)S(1)}, u32[]{:S(2)}, u32[]{:S(2)}) %collective-permute-start.8) | collective-permute-done | bytes 16416 | tf_op jit(solution)/shard_map/ppermute | solution.py:97
  40.1 2.1 %collective-permute-done.7.other_y = bf16[8,1024]{1,0:T(8,128)(2,1)S(1)} collective-permute-done((bf16[8,1024]{1,0:T(8,128)(2,1)S(1)}, bf16[8,1024]{1,0:T(8,128)(2,1)S(1)}, u32[]{:S(2)}, u32[]{:S(2)}) %collective-permute-start.7) | collective-permute-done | bytes 16416 | tf_op jit(solution)/shard_map/ppermute | solution.py:97
  42.3 0.0 collective-permute-done.6.both
  42.3 0.0 copy-done.6
  42.3 0.7 %last.1 = bf16[16,256]{1,0:T(8,128)(2,1)} custom-call(bf16[8,1024]{1,0:T(8,128)(2,1)S(1)} %get-tuple-element.34.share, bf16[2,8,1024]{2,1,0:T(8,128)(2,1)S(1)} %collective-permute-done.6.both, bf16[8,1024]{1,0:T(8,128)(2,1)S(1)} %collective-permute-done.7.other_y, bf16[8,1024]{1,0:T(8,128)(2,1)S(1)} %collective-permute-done.8.other_far, ...), custom_call_target="tpu_custom_call" | custom-call | tf_op jit(solution)/shard_map/last/pallas_call | solution.py:346
  (1 shorter events, 0.0 us)
Async XLA Ops:
  0.0 12.5 %copy-start.3 = (bf16[16,1024]{1,0:T(8,128)(2,1)S(1)}, bf16[16,1024]{1,0:T(8,128)(2,1)}, u32[]{:S(2)}) copy-start(bf16[16,1024]{1,0:T(8,128)(2,1)} %refs_4_.1) | copy-start | bytes 98308
  0.0 4.9 %copy-start.2 = (bf16[1,256,1024]{2,1,0:T(8,128)(2,1)S(1)}, bf16[1,256,1024]{2,1,0:T(8,128)(2,1)}, u32[]{:S(2)}) copy-start(bf16[1,256,1024]{2,1,0:T(8,128)(2,1)} %param.40) | copy-start | bytes 1572868
  0.0 4.8 %copy-start.1 = (bf16[1,1024,256]{2,1,0:T(8,128)(2,1)S(1)}, bf16[1,1024,256]{2,1,0:T(8,128)(2,1)}, u32[]{:S(2)}) copy-start(bf16[1,1024,256]{2,1,0:T(8,128)(2,1)} %param.39) | copy-start | bytes 1572868
  0.0 4.2 %copy-start = (bf16[1,1024,256]{2,1,0:T(8,128)(2,1)S(1)}, bf16[1,1024,256]{2,1,0:T(8,128)(2,1)}, u32[]{:S(2)}) copy-start(bf16[1,1024,256]{2,1,0:T(8,128)(2,1)} %param.38) | copy-start | bytes 1572868
  0.0 10.7 %copy-start.7 = (f32[16,6]{0,1:T(8,128)S(1)}, f32[16,6]{0,1:T(8,128)}, u32[]{:S(2)}) copy-start(f32[16,6]{0,1:T(8,128)} %param.37) | copy-start | bytes 1156
  0.0 10.7 %copy-start.8 = (s32[16,6]{0,1:T(8,128)S(1)}, s32[16,6]{0,1:T(8,128)}, u32[]{:S(2)}) copy-start(s32[16,6]{0,1:T(8,128)} %param.36) | copy-start | bytes 1156
  0.0 12.4 %copy-start.5 = (f32[1024]{0:T(1024)S(1)}, f32[1024]{0:T(1024)}, u32[]{:S(2)}) copy-start(f32[1024]{0:T(1024)} %param.35) | copy-start | bytes 12292
  0.0 12.4 %copy-start.4 = (f32[1024]{0:T(1024)S(1)}, f32[1024]{0:T(1024)}, u32[]{:S(2)}) copy-start(f32[1024]{0:T(1024)} %param.34) | copy-start | bytes 12292
  4.2 21.9 %collective-permute-start.3 = (bf16[1024,256]{1,0:T(8,128)(2,1)S(1)}, bf16[1024,256]{1,0:T(8,128)(2,1)S(1)}, u32[]{:S(2)}, u32[]{:S(2)}) collective-permute-start(bf16[1024,256]{1,0:T(8,128)(2,1)S(1)} %bitcast.16), channel_id=1, source_target_pairs={{0,1},{1,0},{2,3},{3,2},{4,5},{5,4},{6,7},{7,6},{8,9},{9,8},{10,11... | collective-permute-start | bytes 1572872 | tf_op jit(solution)/shard_map/ppermute | solution.py:97
  4.8 21.3 %collective-permute-start.4 = (bf16[1024,256]{1,0:T(8,128)(2,1)S(1)}, bf16[1024,256]{1,0:T(8,128)(2,1)S(1)}, u32[]{:S(2)}, u32[]{:S(2)}) collective-permute-start(bf16[1024,256]{1,0:T(8,128)(2,1)S(1)} %bitcast.18), channel_id=1, source_target_pairs={{0,1},{1,0},{2,3},{3,2},{4,5},{5,4},{6,7},{7,6},{8,9},{9,8},{10,11... | collective-permute-start | bytes 1572872 | tf_op jit(solution)/shard_map/ppermute | solution.py:97
  4.9 21.3 %collective-permute-start.5 = (bf16[256,1024]{1,0:T(8,128)(2,1)S(1)}, bf16[256,1024]{1,0:T(8,128)(2,1)S(1)}, u32[]{:S(2)}, u32[]{:S(2)}) collective-permute-start(bf16[256,1024]{1,0:T(8,128)(2,1)S(1)} %bitcast.20), channel_id=1, source_target_pairs={{0,1},{1,0},{2,3},{3,2},{4,5},{5,4},{6,7},{7,6},{8,9},{9,8},{10,11... | collective-permute-start | bytes 1572872 | tf_op jit(solution)/shard_map/ppermute | solution.py:97
  5.3 2.7 %collective-permute-start.2 = (bf16[8,1024]{1,0:T(8,128)(2,1)S(1)}, bf16[8,1024]{1,0:T(8,128)(2,1)S(1)}, u32[]{:S(2)}, u32[]{:S(2)}) collective-permute-start(bf16[8,1024]{1,0:T(8,128)(2,1)S(1)} %get-tuple-element.22), channel_id=1, source_target_pairs={{0,1},{1,0},{2,3},{3,2},{4,5},{5,4},{6,7},{7,6},{8,9},{9,8},{10,11... | collective-permute-start | bytes 49160 | tf_op jit(solution)/shard_map/ppermute | solution.py:97
  5.4 5.4 %collective-permute-start.1 = (bf16[8,1024]{1,0:T(8,128)(2,1)S(1)}, bf16[8,1024]{1,0:T(8,128)(2,1)S(1)}, u32[]{:S(2)}, u32[]{:S(2)}) collective-permute-start(bf16[8,1024]{1,0:T(8,128)(2,1)S(1)} %get-tuple-element.22), channel_id=1, source_target_pairs={{0,3},{1,2},{2,1},{3,0},{4,7},{5,6},{6,5},{7,4},{8,11},{9,10},{10,... | collective-permute-start | bytes 49160 | tf_op jit(solution)/shard_map/ppermute | solution.py:97
  8.0 4.4 %collective-permute-start = (bf16[8,1024]{1,0:T(8,128)(2,1)S(1)}, bf16[8,1024]{1,0:T(8,128)(2,1)S(1)}, u32[]{:S(2)}, u32[]{:S(2)}) collective-permute-start(bf16[8,1024]{1,0:T(8,128)(2,1)S(1)} %get-tuple-element.21.refs_0_), channel_id=1, source_target_pairs={{0,2},{1,3},{2,0},{3,1},{4,6},{5,7},{6,4},{7,5},{8,10},{9,11},{10,... | collective-permute-start | bytes 49160 | tf_op jit(solution)/shard_map/ppermute | solution.py:97
  12.5 29.8 %copy-start.6 = (f32[256]{0:T(256)S(1)}, f32[256]{0:T(256)}, u32[]{:S(2)}) copy-start(f32[256]{0:T(256)} %param.41) | copy-start | bytes 3076
  36.8 5.4 %collective-permute-start.6 = (bf16[2,8,1024]{2,1,0:T(8,128)(2,1)S(1)}, bf16[2,8,1024]{2,1,0:T(8,128)(2,1)S(1)}, u32[]{:S(2)}, u32[]{:S(2)}) collective-permute-start(bf16[2,8,1024]{2,1,0:T(8,128)(2,1)S(1)} %get-tuple-element.35), channel_id=1, source_target_pairs={{0,1},{1,0},{2,3},{3,2},{4,5},{5,4},{6,7},{7,6},{8,9},{9,8},{10,11... | collective-permute-start | bytes 98312 | tf_op jit(solution)/shard_map/ppermute | solution.py:97
  36.9 3.2 %collective-permute-start.8 = (bf16[8,1024]{1,0:T(8,128)(2,1)S(1)}, bf16[8,1024]{1,0:T(8,128)(2,1)S(1)}, u32[]{:S(2)}, u32[]{:S(2)}) collective-permute-start(bf16[8,1024]{1,0:T(8,128)(2,1)S(1)} %get-tuple-element.34.share), channel_id=1, source_target_pairs={{0,3},{1,2},{2,1},{3,0},{4,7},{5,6},{6,5},{7,4},{8,11},{9,10},{10,... | collective-permute-start | bytes 49160 | tf_op jit(solution)/shard_map/ppermute | solution.py:97
  38.5 3.7 %collective-permute-start.7 = (bf16[8,1024]{1,0:T(8,128)(2,1)S(1)}, bf16[8,1024]{1,0:T(8,128)(2,1)S(1)}, u32[]{:S(2)}, u32[]{:S(2)}) collective-permute-start(bf16[8,1024]{1,0:T(8,128)(2,1)S(1)} %get-tuple-element.34.share), channel_id=1, source_target_pairs={{0,2},{1,3},{2,0},{3,1},{4,6},{5,7},{6,4},{7,5},{8,10},{9,11},{10,... | collective-permute-start | bytes 49160 | tf_op jit(solution)/shard_map/ppermute | solution.py:97

commit v8 on v7

--- a/solution.py
+++ b/solution.py
@@ -108,32 +108,42 @@
     return pl.BlockSpec(memory_space=pltpu.VMEM)
 
 
-def cell_body(heads, key_dim, value_dim, chunk, halves, *refs):
-    f32 = jnp.float32
-    bf16 = jnp.bfloat16
-    sources, outs, rest = refs[:13], refs[13 : 14 + halves], refs[14 + halves :]
-    targets, (recall, sems) = rest[:13], rest[13:]
-    (tokens, gain, wi, wf, ib, fb, scale, wq, wk, wv, mem, hg, wo) = targets
-    seqs = tokens.shape[0]
-    count = seqs // chunk
-    pairs = list(zip(sources, targets))
-    pieces = [pairs[i] for i in (0, 1, 7, 2, 3, 4, 5, 6, 8)]
-    for c in range(count):
-        rows = pl.ds(c * chunk, chunk)
-        pieces.append((pairs[10][0].at[rows], mem.at[rows]))
-    pieces += [pairs[9], pairs[11], pairs[12]]
-    copies = [pltpu.make_async_copy(src, dst, sems.at[i]) for i, (src, dst) in enumerate(pieces)]
+def norm_body(tokens_h, gain_h, normed, tokens, gain, sems):
+    copies = [
+        pltpu.make_async_copy(tokens_h, tokens, sems.at[0]),
+        pltpu.make_async_copy(gain_h, gain, sems.at[1]),
+    ]
     for copy in copies:
         copy.start()
-    copies[0].wait()
-    copies[1].wait()
-    xf = tokens[...].astype(f32)
-    inv = lax.rsqrt(jnp.mean(xf * xf, axis=1, keepdims=True) + EPS)
-    normed = (xf * inv * gain[...]).astype(bf16)
-    copies[2].wait()
+    for copy in copies:
+        copy.wait()
+    xf = tokens[...].astype(jnp.float32)
+    normed[...] = (xf * rms_scale(xf) * gain[...]).astype(jnp.bfloat16)
+
+
+def norm(tokens, gain):
+    operands = [tokens, gain.reshape(1, tokens.shape[1])]
+    return pl.pallas_call(
+        norm_body,
+        out_shape=jax.ShapeDtypeStruct(tokens.shape, jnp.bfloat16),
+        in_specs=[pl.BlockSpec(memory_space=pltpu.HBM)] * 2,
+        out_specs=whole(),
+        scratch_shapes=[pltpu.VMEM(o.shape, o.dtype) for o in operands]
+        + [pltpu.SemaphoreType.DMA((2,))],
+        compiler_params=pltpu.CompilerParams(vmem_limit_bytes=4 << 20),
+        cost_estimate=pl.CostEstimate(flops=11 * 10**8, transcendentals=0, bytes_accessed=65536),
+        name="norm",
+    )(*[pltpu.with_memory_space_constraint(o, pltpu.HBM) for o in operands])
+
+
+def cell_body(heads, key_dim, value_dim, halves, *refs):
+    f32 = jnp.float32
+    bf16 = jnp.bfloat16
+    (normed_ref, wi, wf, ib, fb, scale, wq, wk, wv, mem, hg, wo) = refs[:12]
+    outs, recall = refs[12:-1], refs[-1]
+    normed = normed_ref[...]
+    seqs = normed.shape[0]
     query = jnp.dot(normed, wq[...], preferred_element_type=f32) * key_dim ** (-0.5)
-    for i in range(3, 8):
-        copies[i].wait()
     wide = normed.astype(f32)
     diagonal = lax.broadcasted_iota(jnp.int32, (seqs, seqs), 0) == lax.broadcasted_iota(
         jnp.int32, (seqs, seqs), 1
@@ -148,17 +158,12 @@
         new_max = jnp.maximum(carried, in_pre)
         carries.append(jnp.exp(carried - new_max))
         fresh.append(jnp.exp(in_pre - new_max))
-    copies[8].wait()
     keys = jnp.dot(normed, wk[...], preferred_element_type=f32)
     turned = [query[:, h * key_dim : (h + 1) * key_dim].T for h in range(heads)]
-    for c in range(count):
-        copies[9 + c].wait()
-        for b in range(c * chunk, (c + 1) * chunk):
-            for h in range(heads):
-                product = turned[h][:, b : b + 1] * mem[b, h]
-                recall[h, b : b + 1, :] = jnp.sum(product, axis=0, keepdims=True)
-    copies[9 + count].wait()
-    copies[10 + count].wait()
+    for b in range(seqs):
+        for h in range(heads):
+            product = turned[h][:, b : b + 1] * mem[b, h]
+            recall[h, b : b + 1, :] = jnp.sum(product, axis=0, keepdims=True)
     values = jnp.dot(normed, wv[...], preferred_element_type=f32)
     parts = []
     for h in range(heads):
@@ -168,7 +173,6 @@
         read = carries[h] * recall[h] + (fresh[h] * match) * values[:, vs]
         inv = lax.rsqrt(jnp.mean(read * read, axis=1, keepdims=True) + EPS)
         parts.append((read * inv * hg[:, vs]).astype(bf16))
-    copies[11 + count].wait()
     headout = parts[0] if heads == 1 else jnp.concatenate(parts, axis=1)
     product = jnp.dot(headout, wo[...], preferred_element_type=f32)
     if halves:
@@ -198,13 +202,13 @@
 ):
     f32 = jnp.float32
     bf16 = jnp.bfloat16
-    seqs, width = tokens.shape
+    seqs, _ = tokens.shape
     heads, key_dim, value_dim = memory.shape[1:]
-    chunk = 4 if seqs % 4 == 0 else 1
-    body = lambda *refs: cell_body(heads, key_dim, value_dim, chunk, halves, *refs)
+    body = lambda *refs: cell_body(heads, key_dim, value_dim, halves, *refs)
+    normed = norm(tokens, mix_gain_in)
+    normed, igate_bias, fgate_bias = lax.optimization_barrier((normed, igate_bias, fgate_bias))
     operands = [
-        tokens,
-        mix_gain_in.reshape(1, width),
+        normed,
         w_igate.T,
         w_fgate.T,
         igate_bias.reshape(1, heads),
@@ -221,16 +225,12 @@
     result = pl.pallas_call(
         body,
         out_shape=[shape] * (2 if halves else 1),
-        in_specs=[pl.BlockSpec(memory_space=pltpu.HBM)] * len(operands),
+        in_specs=[whole()] * len(operands),
         out_specs=[whole()] * (2 if halves else 1),
-        scratch_shapes=[pltpu.VMEM(o.shape, o.dtype) for o in operands]
-        + [
-            pltpu.VMEM((heads, seqs, value_dim), f32),
-            pltpu.SemaphoreType.DMA((12 + seqs // chunk,)),
-        ],
+        scratch_shapes=[pltpu.VMEM((heads, seqs, value_dim), f32)],
         compiler_params=pltpu.CompilerParams(vmem_limit_bytes=12 << 20),
         name="cell",
-    )(*[o if o.size == heads else pltpu.with_memory_space_constraint(o, pltpu.HBM) for o in operands])
+    )(*operands)
     return result if halves else result[0]
 
 

time: 43.2 us -> 43 us (level)
  Pallas kernels: 4.58 us -> 3.82 us
  between operations: 1.52 us -> 2.02 us
    pallas_call x1, Pallas kernels: 2.77 us -> 1.13 us  [cell(): pl.pallas_call(body, out_shape=[shape] * (2 if halves else 1), in_specs=[...]
    pallas_call x0 -> x1, Pallas kernels: none -> 0.88 us  [norm(): pl.pallas_call(norm_body, out_shape=jax.ShapeDtypeStruct(tokens.shape, jn...]
where the time goes in v8:
time: 43 us; the launch traced here: 42.7 us
  blocking collectives  23.2 us (54%)
  starting transfers between devices  8.68 us (20%)
  waiting for transfers between devices  4.94 us (11%)
  Pallas kernels  3.82 us (9%)
  between operations  2.02 us (5%)
    all_to_all x1, blocking collectives, every_token(): rows = lax.all_to_all(spread, 'ep', split_axis=0, concat_axis=0, tiled=True)  13.4 us
    all_to_all x1, blocking collectives, every_token(): back = lax.all_to_all(blocks, 'ep', split_axis=0, concat_axis=0, tiled=True)  9.74 us
    ppermute x9, starting transfers between devices, exchange(): return lax.ppermute(value, axis, pairs)  8.68 us
    ppermute x9, waiting for transfers between devices, exchange(): return lax.ppermute(value, axis, pairs)  4.94 us
    pallas_call x1, Pallas kernels, cell(): pl.pallas_call(body, out_shape=[shape] * (2 if halves else 1), in_specs=[...  1.13 us
    pallas_call x1, Pallas kernels, norm(): pl.pallas_call(norm_body, out_shape=jax.ShapeDtypeStruct(tokens.shape, jn...  0.88 us
  transfers between devices with their start and end apart: 9, of which 3 were waited for; matrix products, arithmetic and copies ran while one was open for 0% of the time, Pallas kernels for 0%

profile of v8, /device:TPU:0, one launch (start us, length us, event | category | flops | bytes accessed | tf_op | source)
XLA Modules:
  0.0 42.7 jit_solution(18143637756546887681)
XLA Ops:
  0.0 0.0 copy-start.7
  0.0 0.0 copy-start.6
  0.0 0.0 copy-start.15
  0.0 0.0 copy-start
  1.8 0.9 %norm.1.refs_0_ = bf16[16,1024]{1,0:T(8,128)(2,1)S(1)} custom-call(bf16[16,1024]{1,0:T(8,128)(2,1)} %refs_4_.1, f32[1,1024]{1,0:T(1,128)} %bitcast.30), custom_call_target="tpu_custom_call" | custom-call | flops 1100000000 | bytes 65536 | tf_op jit(solution)/shard_map/norm/pallas_call | solution.py:126
  2.7 0.0 copy-start.3
  2.7 0.0 copy-start.4
  2.7 0.0 copy-start.5
  2.7 0.0 copy-start.16
  2.8 0.0 copy-start.17
  2.8 0.0 copy-start.8
  2.8 0.0 copy-start.11
  2.8 0.0 copy-start.12
  2.8 0.0 copy-done.2
  2.8 0.0 copy-done.13
  2.8 0.0 copy-done.10
  2.8 0.0 copy-done.9
  2.8 0.0 copy-done.1
  2.9 0.0 copy-done.7
  2.9 0.0 copy-done.6
  2.9 1.1 %cell.1 = (bf16[8,1024]{1,0:T(8,128)(2,1)S(1)}, bf16[8,1024]{1,0:T(8,128)(2,1)S(1)}) custom-call(bf16[16,1024]{1,0:T(8,128)(2,1)S(1)} %norm.1.refs_0_, bf16[1,1024]{1,0:T(2,128)(2,1)S(1)} %bitcast.23, bf16[1,1024]{1,0:T(2,128)(2,1)S(1)} %bitcast.24, f32[1,1]{1,0:T(1,128)} %bitcast.14.refs_3_, f32[1,1]{1,0:T(1,128)} %bitcast.15.refs_4_, ...), custom_call_target="tpu_custom_call" | custom-call | tf_op jit(solution)/shard_map/cell/pallas_call | solution.py:225
  4.0 0.0 copy-done.3
  4.0 0.6 %collective-permute-start.3 = (bf16[1024,256]{1,0:T(8,128)(2,1)S(1)}, bf16[1024,256]{1,0:T(8,128)(2,1)S(1)}, u32[]{:S(2)}, u32[]{:S(2)}) collective-permute-start(bf16[1024,256]{1,0:T(8,128)(2,1)S(1)} %bitcast.16), channel_id=1, source_target_pairs={{0,1},{1,0},{2,3},{3,2},{4,5},{5,4},{6,7},{7,6},{8,9},{9,8},{10,11... | collective-permute-start | bytes 1572872 | tf_op jit(solution)/shard_map/ppermute | solution.py:97
  4.6 0.1 collective-permute-start.4
  4.7 0.4 collective-permute-start.5
  5.1 0.1 collective-permute-start.2
  5.2 2.6 %collective-permute-start.1 = (bf16[8,1024]{1,0:T(8,128)(2,1)S(1)}, bf16[8,1024]{1,0:T(8,128)(2,1)S(1)}, u32[]{:S(2)}, u32[]{:S(2)}) collective-permute-start(bf16[8,1024]{1,0:T(8,128)(2,1)S(1)} %get-tuple-element.28), channel_id=1, source_target_pairs={{0,3},{1,2},{2,1},{3,0},{4,7},{5,6},{6,5},{7,4},{8,11},{9,10},{10,... | collective-permute-start | bytes 49160 | tf_op jit(solution)/shard_map/ppermute | solution.py:97
  7.8 0.0 collective-permute-done.2.refs_3_
  7.8 2.7 %collective-permute-start = (bf16[8,1024]{1,0:T(8,128)(2,1)S(1)}, bf16[8,1024]{1,0:T(8,128)(2,1)S(1)}, u32[]{:S(2)}, u32[]{:S(2)}) collective-permute-start(bf16[8,1024]{1,0:T(8,128)(2,1)S(1)} %get-tuple-element.27.refs_0_), channel_id=1, source_target_pairs={{0,2},{1,3},{2,0},{3,1},{4,6},{5,7},{6,4},{7,5},{8,10},{9,11},{10,... | collective-permute-start | bytes 49160 | tf_op jit(solution)/shard_map/ppermute | solution.py:97
  10.5 0.0 copy-done.17
  10.5 0.0 collective-permute-done.1.refs_2_
  10.5 1.7 %collective-permute-done.refs_1_ = bf16[8,1024]{1,0:T(8,128)(2,1)S(1)} collective-permute-done((bf16[8,1024]{1,0:T(8,128)(2,1)S(1)}, bf16[8,1024]{1,0:T(8,128)(2,1)S(1)}, u32[]{:S(2)}, u32[]{:S(2)}) %collective-permute-start) | collective-permute-done | bytes 16416 | tf_op jit(solution)/shard_map/ppermute | solution.py:97
  12.2 0.0 copy-start.14
  12.3 0.2 after_mix.1
  12.5 13.4 %all_to_all.10.rows = bf16[8,8,1024]{2,1,0:T(8,128)(2,1)S(1)} all-to-all(bf16[8,8,1024]{2,1,0:T(8,128)(2,1)S(1)} %get-tuple-element.30), channel_id=1, replica_groups=mesh['ep'=8,'tp'=4] {'ep'}, dimensions={0} | all-to-all | bytes 262144 | tf_op jit(solution)/shard_map/all_to_all | solution.py:381
  25.9 0.0 collective-permute-done.3.gate_n
  25.9 0.0 collective-permute-done.4.up_n
  25.9 0.0 collective-permute-done.5.down_n
  25.9 0.7 %expert.1 = bf16[8,8,1024]{2,1,0:T(8,128)(2,1)S(1)} custom-call(bf16[8,8,1024]{2,1,0:T(8,128)(2,1)S(1)} %all_to_all.10.rows, bf16[1024,256]{1,0:T(8,128)(2,1)S(1)} %bitcast.17, bf16[1024,256]{1,0:T(8,128)(2,1)S(1)} %bitcast.19, bf16[256,1024]{1,0:T(8,128)(2,1)S(1)} %bitcast.21, bf16[1024,256]{1,0:T(8,128)(2,1)S(1)} %collective-permute-done.3.gate_n, ...), custom_call_target="tpu_custom_call" | custom-call | tf_op jit(solution)/shard_map/expert/pallas_call | solution.py:285
  26.7 9.7 %all_to_all.11.back = bf16[8,8,1024]{2,1,0:T(8,128)(2,1)S(1)} all-to-all(bf16[8,8,1024]{2,1,0:T(8,128)(2,1)S(1)} %expert.1), channel_id=1, replica_groups=mesh['ep'=8,'tp'=4] {'ep'}, dimensions={0} | all-to-all | bytes 262144 | tf_op jit(solution)/shard_map/all_to_all | solution.py:384
  36.4 0.2 share.1
  36.6 0.1 collective-permute-start.6
  36.7 1.6 %collective-permute-start.8 = (bf16[8,1024]{1,0:T(8,128)(2,1)S(1)}, bf16[8,1024]{1,0:T(8,128)(2,1)S(1)}, u32[]{:S(2)}, u32[]{:S(2)}) collective-permute-start(bf16[8,1024]{1,0:T(8,128)(2,1)S(1)} %get-tuple-element.40.share), channel_id=1, source_target_pairs={{0,3},{1,2},{2,1},{3,0},{4,7},{5,6},{6,5},{7,4},{8,11},{9,10},{10,... | collective-permute-start | bytes 49160 | tf_op jit(solution)/shard_map/ppermute | solution.py:97
  38.3 0.5 %collective-permute-start.7 = (bf16[8,1024]{1,0:T(8,128)(2,1)S(1)}, bf16[8,1024]{1,0:T(8,128)(2,1)S(1)}, u32[]{:S(2)}, u32[]{:S(2)}) collective-permute-start(bf16[8,1024]{1,0:T(8,128)(2,1)S(1)} %get-tuple-element.40.share), channel_id=1, source_target_pairs={{0,2},{1,3},{2,0},{3,1},{4,6},{5,7},{6,4},{7,5},{8,10},{9,11},{10,... | collective-permute-start | bytes 49160 | tf_op jit(solution)/shard_map/ppermute | solution.py:97
  38.8 1.1 %collective-permute-done.8.other_far = bf16[8,1024]{1,0:T(8,128)(2,1)S(1)} collective-permute-done((bf16[8,1024]{1,0:T(8,128)(2,1)S(1)}, bf16[8,1024]{1,0:T(8,128)(2,1)S(1)}, u32[]{:S(2)}, u32[]{:S(2)}) %collective-permute-start.8) | collective-permute-done | bytes 16416 | tf_op jit(solution)/shard_map/ppermute | solution.py:97
  39.9 2.1 %collective-permute-done.7.other_y = bf16[8,1024]{1,0:T(8,128)(2,1)S(1)} collective-permute-done((bf16[8,1024]{1,0:T(8,128)(2,1)S(1)}, bf16[8,1024]{1,0:T(8,128)(2,1)S(1)}, u32[]{:S(2)}, u32[]{:S(2)}) %collective-permute-start.7) | collective-permute-done | bytes 16416 | tf_op jit(solution)/shard_map/ppermute | solution.py:97
  42.0 0.0 collective-permute-done.6.both
  42.0 0.7 %last.1 = bf16[16,256]{1,0:T(8,128)(2,1)} custom-call(bf16[8,1024]{1,0:T(8,128)(2,1)S(1)} %get-tuple-element.40.share, bf16[2,8,1024]{2,1,0:T(8,128)(2,1)S(1)} %collective-permute-done.6.both, bf16[8,1024]{1,0:T(8,128)(2,1)S(1)} %collective-permute-done.7.other_y, bf16[8,1024]{1,0:T(8,128)(2,1)S(1)} %collective-permute-done.8.other_far, ...), custom_call_target="tpu_custom_call" | custom-call | tf_op jit(solution)/shard_map/last/pallas_call | solution.py:346
  (15 shorter events, 0.0 us)
Async XLA Ops:
  0.0 2.8 %copy-start.2 = (bf16[256,1024]{1,0:T(8,128)(2,1)S(1)}, bf16[256,1024]{1,0:T(8,128)(2,1)}, u32[]{:S(2)}) copy-start(bf16[256,1024]{1,0:T(8,128)(2,1)} %refs_11_.1) | copy-start | bytes 1572868
  0.0 2.8 %copy-start.13 = (f32[256]{0:T(256)S(1)}, f32[256]{0:T(256)}, u32[]{:S(2)}) copy-start(f32[256]{0:T(256)} %param.32) | copy-start | bytes 3076
  0.0 2.8 %copy-start.10 = (bf16[1024,1]{0,1:T(2,128)(2,1)S(1)}, bf16[1024,1]{0,1:T(2,128)(2,1)}, u32[]{:S(2)}) copy-start(bf16[1024,1]{0,1:T(2,128)(2,1)} %param.29) | copy-start | bytes 6148
  0.0 2.8 %copy-start.9 = (bf16[1024,1]{0,1:T(2,128)(2,1)S(1)}, bf16[1024,1]{0,1:T(2,128)(2,1)}, u32[]{:S(2)}) copy-start(bf16[1024,1]{0,1:T(2,128)(2,1)} %param.28) | copy-start | bytes 6148
  0.0 2.8 %copy-start.1 = (bf16[1024,256]{1,0:T(8,128)(2,1)S(1)}, bf16[1024,256]{1,0:T(8,128)(2,1)}, u32[]{:S(2)}) copy-start(bf16[1024,256]{1,0:T(8,128)(2,1)} %refs_8_.1) | copy-start | bytes 1572868
  0.0 2.8 %copy-start.7 = (bf16[1024,128]{1,0:T(8,128)(2,1)S(1)}, bf16[1024,128]{1,0:T(8,128)(2,1)}, u32[]{:S(2)}) copy-start(bf16[1024,128]{1,0:T(8,128)(2,1)} %refs_7_.1) | copy-start | bytes 786436
  0.0 2.8 %copy-start.6 = (bf16[1024,128]{1,0:T(8,128)(2,1)S(1)}, bf16[1024,128]{1,0:T(8,128)(2,1)}, u32[]{:S(2)}) copy-start(bf16[1024,128]{1,0:T(8,128)(2,1)} %refs_6_.1) | copy-start | bytes 786436
  0.0 2.8 %copy-start.15 = (f32[16,1]{0,1:T(1,128)S(1)}, f32[16,1]{0,1:T(1,128)}, u32[]{:S(2)}) copy-start(f32[16,1]{0,1:T(1,128)} %param.23) | copy-start | bytes 196
  0.0 2.8 %copy-start = (f32[16,1,128,256]{3,2,1,0:T(8,128)S(1)}, f32[16,1,128,256]{3,2,1,0:T(8,128)}, u32[]{:S(2)}) copy-start(f32[16,1,128,256]{3,2,1,0:T(8,128)} %refs_9_.1) | copy-start | bytes 6291460
  2.7 1.3 %copy-start.3 = (bf16[1,1024,256]{2,1,0:T(8,128)(2,1)S(1)}, bf16[1,1024,256]{2,1,0:T(8,128)(2,1)}, u32[]{:S(2)}) copy-start(bf16[1,1024,256]{2,1,0:T(8,128)(2,1)} %param.38) | copy-start | bytes 1572868
  2.7 1.9 %copy-start.4 = (bf16[1,1024,256]{2,1,0:T(8,128)(2,1)S(1)}, bf16[1,1024,256]{2,1,0:T(8,128)(2,1)}, u32[]{:S(2)}) copy-start(bf16[1,1024,256]{2,1,0:T(8,128)(2,1)} %param.39) | copy-start | bytes 1572868
  2.7 1.9 %copy-start.5 = (bf16[1,256,1024]{2,1,0:T(8,128)(2,1)S(1)}, bf16[1,256,1024]{2,1,0:T(8,128)(2,1)}, u32[]{:S(2)}) copy-start(bf16[1,256,1024]{2,1,0:T(8,128)(2,1)} %param.40) | copy-start | bytes 1572868
  2.7 7.8 %copy-start.16 = (f32[16,6]{0,1:T(8,128)S(1)}, f32[16,6]{0,1:T(8,128)}, u32[]{:S(2)}) copy-start(f32[16,6]{0,1:T(8,128)} %param.37) | copy-start | bytes 1156
  2.8 7.8 %copy-start.17 = (s32[16,6]{0,1:T(8,128)S(1)}, s32[16,6]{0,1:T(8,128)}, u32[]{:S(2)}) copy-start(s32[16,6]{0,1:T(8,128)} %param.36) | copy-start | bytes 1156
  2.8 9.5 %copy-start.8 = (bf16[16,1024]{1,0:T(8,128)(2,1)S(1)}, bf16[16,1024]{1,0:T(8,128)(2,1)}, u32[]{:S(2)}) copy-start(bf16[16,1024]{1,0:T(8,128)(2,1)} %refs_4_.1) | copy-start | bytes 98308
  2.8 9.5 %copy-start.11 = (f32[1024]{0:T(1024)S(1)}, f32[1024]{0:T(1024)}, u32[]{:S(2)}) copy-start(f32[1024]{0:T(1024)} %param.34) | copy-start | bytes 12292
  2.8 9.4 %copy-start.12 = (f32[1024]{0:T(1024)S(1)}, f32[1024]{0:T(1024)}, u32[]{:S(2)}) copy-start(f32[1024]{0:T(1024)} %param.35) | copy-start | bytes 12292
  4.0 21.9 %collective-permute-start.3 = (bf16[1024,256]{1,0:T(8,128)(2,1)S(1)}, bf16[1024,256]{1,0:T(8,128)(2,1)S(1)}, u32[]{:S(2)}, u32[]{:S(2)}) collective-permute-start(bf16[1024,256]{1,0:T(8,128)(2,1)S(1)} %bitcast.16), channel_id=1, source_target_pairs={{0,1},{1,0},{2,3},{3,2},{4,5},{5,4},{6,7},{7,6},{8,9},{9,8},{10,11... | collective-permute-start | bytes 1572872 | tf_op jit(solution)/shard_map/ppermute | solution.py:97
  4.6 21.3 %collective-permute-start.4 = (bf16[1024,256]{1,0:T(8,128)(2,1)S(1)}, bf16[1024,256]{1,0:T(8,128)(2,1)S(1)}, u32[]{:S(2)}, u32[]{:S(2)}) collective-permute-start(bf16[1024,256]{1,0:T(8,128)(2,1)S(1)} %bitcast.18), channel_id=1, source_target_pairs={{0,1},{1,0},{2,3},{3,2},{4,5},{5,4},{6,7},{7,6},{8,9},{9,8},{10,11... | collective-permute-start | bytes 1572872 | tf_op jit(solution)/shard_map/ppermute | solution.py:97
  4.7 21.3 %collective-permute-start.5 = (bf16[256,1024]{1,0:T(8,128)(2,1)S(1)}, bf16[256,1024]{1,0:T(8,128)(2,1)S(1)}, u32[]{:S(2)}, u32[]{:S(2)}) collective-permute-start(bf16[256,1024]{1,0:T(8,128)(2,1)S(1)} %bitcast.20), channel_id=1, source_target_pairs={{0,1},{1,0},{2,3},{3,2},{4,5},{5,4},{6,7},{7,6},{8,9},{9,8},{10,11... | collective-permute-start | bytes 1572872 | tf_op jit(solution)/shard_map/ppermute | solution.py:97
  5.1 2.7 %collective-permute-start.2 = (bf16[8,1024]{1,0:T(8,128)(2,1)S(1)}, bf16[8,1024]{1,0:T(8,128)(2,1)S(1)}, u32[]{:S(2)}, u32[]{:S(2)}) collective-permute-start(bf16[8,1024]{1,0:T(8,128)(2,1)S(1)} %get-tuple-element.28), channel_id=1, source_target_pairs={{0,1},{1,0},{2,3},{3,2},{4,5},{5,4},{6,7},{7,6},{8,9},{9,8},{10,11... | collective-permute-start | bytes 49160 | tf_op jit(solution)/shard_map/ppermute | solution.py:97
  5.2 5.4 %collective-permute-start.1 = (bf16[8,1024]{1,0:T(8,128)(2,1)S(1)}, bf16[8,1024]{1,0:T(8,128)(2,1)S(1)}, u32[]{:S(2)}, u32[]{:S(2)}) collective-permute-start(bf16[8,1024]{1,0:T(8,128)(2,1)S(1)} %get-tuple-element.28), channel_id=1, source_target_pairs={{0,3},{1,2},{2,1},{3,0},{4,7},{5,6},{6,5},{7,4},{8,11},{9,10},{10,... | collective-permute-start | bytes 49160 | tf_op jit(solution)/shard_map/ppermute | solution.py:97
  7.8 4.4 %collective-permute-start = (bf16[8,1024]{1,0:T(8,128)(2,1)S(1)}, bf16[8,1024]{1,0:T(8,128)(2,1)S(1)}, u32[]{:S(2)}, u32[]{:S(2)}) collective-permute-start(bf16[8,1024]{1,0:T(8,128)(2,1)S(1)} %get-tuple-element.27.refs_0_), channel_id=1, source_target_pairs={{0,2},{1,3},{2,0},{3,1},{4,6},{5,7},{6,4},{7,5},{8,10},{9,11},{10,... | collective-permute-start | bytes 49160 | tf_op jit(solution)/shard_map/ppermute | solution.py:97
  12.2 29.8 %copy-start.14 = (f32[256]{0:T(256)S(1)}, f32[256]{0:T(256)}, u32[]{:S(2)}) copy-start(f32[256]{0:T(256)} %param.41) | copy-start | bytes 3076
  36.6 5.4 %collective-permute-start.6 = (bf16[2,8,1024]{2,1,0:T(8,128)(2,1)S(1)}, bf16[2,8,1024]{2,1,0:T(8,128)(2,1)S(1)}, u32[]{:S(2)}, u32[]{:S(2)}) collective-permute-start(bf16[2,8,1024]{2,1,0:T(8,128)(2,1)S(1)} %get-tuple-element.41), channel_id=1, source_target_pairs={{0,1},{1,0},{2,3},{3,2},{4,5},{5,4},{6,7},{7,6},{8,9},{9,8},{10,11... | collective-permute-start | bytes 98312 | tf_op jit(solution)/shard_map/ppermute | solution.py:97
  36.7 3.2 %collective-permute-start.8 = (bf16[8,1024]{1,0:T(8,128)(2,1)S(1)}, bf16[8,1024]{1,0:T(8,128)(2,1)S(1)}, u32[]{:S(2)}, u32[]{:S(2)}) collective-permute-start(bf16[8,1024]{1,0:T(8,128)(2,1)S(1)} %get-tuple-element.40.share), channel_id=1, source_target_pairs={{0,3},{1,2},{2,1},{3,0},{4,7},{5,6},{6,5},{7,4},{8,11},{9,10},{10,... | collective-permute-start | bytes 49160 | tf_op jit(solution)/shard_map/ppermute | solution.py:97
  38.3 3.7 %collective-permute-start.7 = (bf16[8,1024]{1,0:T(8,128)(2,1)S(1)}, bf16[8,1024]{1,0:T(8,128)(2,1)S(1)}, u32[]{:S(2)}, u32[]{:S(2)}) collective-permute-start(bf16[8,1024]{1,0:T(8,128)(2,1)S(1)} %get-tuple-element.40.share), channel_id=1, source_target_pairs={{0,2},{1,3},{2,0},{3,1},{4,6},{5,7},{6,4},{7,5},{8,10},{9,11},{10,... | collective-permute-start | bytes 49160 | tf_op jit(solution)/shard_map/ppermute | solution.py:97

commit v9 on v8

--- a/solution.py
+++ b/solution.py
@@ -108,41 +108,33 @@
     return pl.BlockSpec(memory_space=pltpu.VMEM)
 
 
-def norm_body(tokens_h, gain_h, normed, tokens, gain, sems):
-    copies = [
-        pltpu.make_async_copy(tokens_h, tokens, sems.at[0]),
-        pltpu.make_async_copy(gain_h, gain, sems.at[1]),
-    ]
-    for copy in copies:
-        copy.start()
-    for copy in copies:
-        copy.wait()
-    xf = tokens[...].astype(jnp.float32)
-    normed[...] = (xf * rms_scale(xf) * gain[...]).astype(jnp.bfloat16)
-
-
-def norm(tokens, gain):
-    operands = [tokens, gain.reshape(1, tokens.shape[1])]
+def biases_body(heads, ib, fb, out):
+    for h in range(heads):
+        out[0:1, h : h + 1] = jnp.full((1, 1), ib[h], jnp.float32)
+        out[1:2, h : h + 1] = jnp.full((1, 1), fb[h], jnp.float32)
+
+
+def biases(igate_bias, fgate_bias):
+    heads = igate_bias.shape[0]
     return pl.pallas_call(
-        norm_body,
-        out_shape=jax.ShapeDtypeStruct(tokens.shape, jnp.bfloat16),
-        in_specs=[pl.BlockSpec(memory_space=pltpu.HBM)] * 2,
+        lambda *refs: biases_body(heads, *refs),
+        out_shape=jax.ShapeDtypeStruct((2, heads), jnp.float32),
+        in_specs=[pl.BlockSpec(memory_space=pltpu.SMEM)] * 2,
         out_specs=whole(),
-        scratch_shapes=[pltpu.VMEM(o.shape, o.dtype) for o in operands]
-        + [pltpu.SemaphoreType.DMA((2,))],
-        compiler_params=pltpu.CompilerParams(vmem_limit_bytes=4 << 20),
-        cost_estimate=pl.CostEstimate(flops=11 * 10**8, transcendentals=0, bytes_accessed=65536),
-        name="norm",
-    )(*[pltpu.with_memory_space_constraint(o, pltpu.HBM) for o in operands])
+        compiler_params=pltpu.CompilerParams(vmem_limit_bytes=1 << 20),
+        cost_estimate=pl.CostEstimate(flops=11 * 10**8, transcendentals=0, bytes_accessed=4096),
+        name="biases",
+    )(igate_bias, fgate_bias)
 
 
 def cell_body(heads, key_dim, value_dim, halves, *refs):
     f32 = jnp.float32
     bf16 = jnp.bfloat16
-    (normed_ref, wi, wf, ib, fb, scale, wq, wk, wv, mem, hg, wo) = refs[:12]
+    (tokens, gain, wi, wf, bias, scale, wq, wk, wv, mem, hg, wo) = refs[:12]
     outs, recall = refs[12:-1], refs[-1]
-    normed = normed_ref[...]
-    seqs = normed.shape[0]
+    seqs = tokens.shape[0]
+    xf = tokens[...].astype(f32)
+    normed = (xf * rms_scale(xf) * gain[...]).astype(bf16)
     query = jnp.dot(normed, wq[...], preferred_element_type=f32) * key_dim ** (-0.5)
     wide = normed.astype(f32)
     diagonal = lax.broadcasted_iota(jnp.int32, (seqs, seqs), 0) == lax.broadcasted_iota(
@@ -150,8 +142,8 @@
     )
     carries, fresh = [], []
     for h in range(heads):
-        in_pre = jnp.sum(wide * wi[h : h + 1, :].astype(f32), axis=1, keepdims=True) + ib[:, h : h + 1]
-        forget = jnp.sum(wide * wf[h : h + 1, :].astype(f32), axis=1, keepdims=True) + fb[:, h : h + 1]
+        in_pre = jnp.sum(wide * wi[h : h + 1, :].astype(f32), axis=1, keepdims=True) + bias[0:1, h : h + 1]
+        forget = jnp.sum(wide * wf[h : h + 1, :].astype(f32), axis=1, keepdims=True) + bias[1:2, h : h + 1]
         forget_log = jnp.minimum(forget, 0.0) - jnp.log1p(jnp.exp(-jnp.abs(forget)))
         column = jnp.sum(jnp.where(diagonal, scale[h : h + 1, :], 0.0), axis=1, keepdims=True)
         carried = forget_log + column
@@ -202,17 +194,15 @@
 ):
     f32 = jnp.float32
     bf16 = jnp.bfloat16
-    seqs, _ = tokens.shape
+    seqs, width = tokens.shape
     heads, key_dim, value_dim = memory.shape[1:]
     body = lambda *refs: cell_body(heads, key_dim, value_dim, halves, *refs)
-    normed = norm(tokens, mix_gain_in)
-    normed, igate_bias, fgate_bias = lax.optimization_barrier((normed, igate_bias, fgate_bias))
     operands = [
-        normed,
+        tokens,
+        mix_gain_in.reshape(1, width),
         w_igate.T,
         w_fgate.T,
-        igate_bias.reshape(1, heads),
-        fgate_bias.reshape(1, heads),
+        biases(igate_bias, fgate_bias),
         log_scale.T,
         w_query,
         w_key,

time: 43 us -> 42.3 us (0.984)
  Pallas kernels: 3.82 us -> 3.01 us
    pallas_call x1, Pallas kernels: 0.88 us -> 0.01 us  [biases(): pl.pallas_call(lambda *refs: biases_body(heads, *refs), out_shape=jax.Sha...]
where the time goes in v9:
time: 42.3 us; the launch traced here: 42.1 us
  blocking collectives  23.2 us (55%)
  starting transfers between devices  8.68 us (21%)
  waiting for transfers between devices  4.94 us (12%)
  Pallas kernels  3.01 us (7%)
  between operations  2.02 us (5%)
    all_to_all x1, blocking collectives, every_token(): rows = lax.all_to_all(spread, 'ep', split_axis=0, concat_axis=0, tiled=True)  13.4 us
    all_to_all x1, blocking collectives, every_token(): back = lax.all_to_all(blocks, 'ep', split_axis=0, concat_axis=0, tiled=True)  9.74 us
    ppermute x9, starting transfers between devices, exchange(): return lax.ppermute(value, axis, pairs)  8.68 us
    ppermute x9, waiting for transfers between devices, exchange(): return lax.ppermute(value, axis, pairs)  4.94 us
    pallas_call x1, Pallas kernels, cell(): pl.pallas_call(body, out_shape=[shape] * (2 if halves else 1), in_specs=[...  1.19 us
  transfers between devices with their start and end apart: 9, of which 3 were waited for; matrix products, arithmetic and copies ran while one was open for 0% of the time, Pallas kernels for 0%

profile of v9, /device:TPU:0, one launch (start us, length us, event | category | flops | bytes accessed | tf_op | source)
XLA Modules:
  0.0 42.1 jit_solution(16456980396155299319)
XLA Ops:
  0.0 0.0 copy-start.1
  0.0 0.0 copy-start.7
  0.0 0.0 copy-start.6
  1.8 0.0 copy-start.3
  1.9 0.0 copy-start.4
  1.9 0.0 copy-start.5
  1.9 0.0 copy-start.17
  1.9 0.0 copy-start.18
  1.9 0.0 copy-start.9
  1.9 0.0 copy-start.10
  1.9 0.0 copy-done.8
  1.9 0.0 copy-done.2
  2.0 0.0 copy-done.14
  2.0 0.0 copy-done.13
  2.0 0.0 copy-done.12
  2.0 0.0 copy-done.1
  2.0 0.0 copy-done.7
  2.0 0.0 copy-done.6
  2.0 0.0 copy-done.11
  2.0 0.0 copy-done.16
  2.0 0.1 copy-done
  2.2 1.2 %cell.1 = (bf16[8,1024]{1,0:T(8,128)(2,1)S(1)}, bf16[8,1024]{1,0:T(8,128)(2,1)S(1)}) custom-call(bf16[16,1024]{1,0:T(8,128)(2,1)S(1)} %copy-done.8, f32[1,1024]{1,0:T(1,128)S(1)} %bitcast.21, bf16[1,1024]{1,0:T(2,128)(2,1)S(1)} %bitcast.22, bf16[1,1024]{1,0:T(2,128)(2,1)S(1)} %bitcast.23, f32[2,1]{1,0:T(2,128)S(1)} %biases.1.refs_4_, f32[1,16]{1,0:T(1,128)S(1)} %bitcast.26, ...), custom_call_target="tpu_custom_call" | custom-call | tf_op jit(solution)/shard_map/cell/pallas_call | solution.py:215
  3.4 0.6 %collective-permute-start.3 = (bf16[1024,256]{1,0:T(8,128)(2,1)S(1)}, bf16[1024,256]{1,0:T(8,128)(2,1)S(1)}, u32[]{:S(2)}, u32[]{:S(2)}) collective-permute-start(bf16[1024,256]{1,0:T(8,128)(2,1)S(1)} %bitcast.12), channel_id=1, source_target_pairs={{0,1},{1,0},{2,3},{3,2},{4,5},{5,4},{6,7},{7,6},{8,9},{9,8},{10,11... | collective-permute-start | bytes 1572872 | tf_op jit(solution)/shard_map/ppermute | solution.py:97
  3.9 0.1 collective-permute-start.4
  4.0 0.0 copy-done.5
  4.0 0.4 %collective-permute-start.5 = (bf16[256,1024]{1,0:T(8,128)(2,1)S(1)}, bf16[256,1024]{1,0:T(8,128)(2,1)S(1)}, u32[]{:S(2)}, u32[]{:S(2)}) collective-permute-start(bf16[256,1024]{1,0:T(8,128)(2,1)S(1)} %bitcast.16), channel_id=1, source_target_pairs={{0,1},{1,0},{2,3},{3,2},{4,5},{5,4},{6,7},{7,6},{8,9},{9,8},{10,11... | collective-permute-start | bytes 1572872 | tf_op jit(solution)/shard_map/ppermute | solution.py:97
  4.5 0.1 collective-permute-start.2
  4.5 2.6 %collective-permute-start.1 = (bf16[8,1024]{1,0:T(8,128)(2,1)S(1)}, bf16[8,1024]{1,0:T(8,128)(2,1)S(1)}, u32[]{:S(2)}, u32[]{:S(2)}) collective-permute-start(bf16[8,1024]{1,0:T(8,128)(2,1)S(1)} %get-tuple-element.22), channel_id=1, source_target_pairs={{0,3},{1,2},{2,1},{3,0},{4,7},{5,6},{6,5},{7,4},{8,11},{9,10},{10,... | collective-permute-start | bytes 49160 | tf_op jit(solution)/shard_map/ppermute | solution.py:97
  7.2 0.0 collective-permute-done.2.refs_3_
  7.2 2.7 %collective-permute-start = (bf16[8,1024]{1,0:T(8,128)(2,1)S(1)}, bf16[8,1024]{1,0:T(8,128)(2,1)S(1)}, u32[]{:S(2)}, u32[]{:S(2)}) collective-permute-start(bf16[8,1024]{1,0:T(8,128)(2,1)S(1)} %get-tuple-element.21.refs_0_), channel_id=1, source_target_pairs={{0,2},{1,3},{2,0},{3,1},{4,6},{5,7},{6,4},{7,5},{8,10},{9,11},{10,... | collective-permute-start | bytes 49160 | tf_op jit(solution)/shard_map/ppermute | solution.py:97
  9.9 0.0 collective-permute-done.1.refs_2_
  9.9 1.7 %collective-permute-done.refs_1_ = bf16[8,1024]{1,0:T(8,128)(2,1)S(1)} collective-permute-done((bf16[8,1024]{1,0:T(8,128)(2,1)S(1)}, bf16[8,1024]{1,0:T(8,128)(2,1)S(1)}, u32[]{:S(2)}, u32[]{:S(2)}) %collective-permute-start) | collective-permute-done | bytes 16416 | tf_op jit(solution)/shard_map/ppermute | solution.py:97
  11.6 0.0 copy-done.10
  11.6 0.2 after_mix.1
  11.8 13.4 %all_to_all.10.rows = bf16[8,8,1024]{2,1,0:T(8,128)(2,1)S(1)} all-to-all(bf16[8,8,1024]{2,1,0:T(8,128)(2,1)S(1)} %get-tuple-element.24), channel_id=1, replica_groups=mesh['ep'=8,'tp'=4] {'ep'}, dimensions={0} | all-to-all | bytes 262144 | tf_op jit(solution)/shard_map/all_to_all | solution.py:371
  25.3 0.0 collective-permute-done.3.gate_n
  25.3 0.0 collective-permute-done.4.up_n
  25.3 0.0 collective-permute-done.5.down_n
  25.3 0.7 %expert.1 = bf16[8,8,1024]{2,1,0:T(8,128)(2,1)S(1)} custom-call(bf16[8,8,1024]{2,1,0:T(8,128)(2,1)S(1)} %all_to_all.10.rows, bf16[1024,256]{1,0:T(8,128)(2,1)S(1)} %bitcast.13, bf16[1024,256]{1,0:T(8,128)(2,1)S(1)} %bitcast.15, bf16[256,1024]{1,0:T(8,128)(2,1)S(1)} %bitcast.17, bf16[1024,256]{1,0:T(8,128)(2,1)S(1)} %collective-permute-done.3.gate_n, ...), custom_call_target="tpu_custom_call" | custom-call | tf_op jit(solution)/shard_map/expert/pallas_call | solution.py:275
  26.0 9.7 %all_to_all.11.back = bf16[8,8,1024]{2,1,0:T(8,128)(2,1)S(1)} all-to-all(bf16[8,8,1024]{2,1,0:T(8,128)(2,1)S(1)} %expert.1), channel_id=1, replica_groups=mesh['ep'=8,'tp'=4] {'ep'}, dimensions={0} | all-to-all | bytes 262144 | tf_op jit(solution)/shard_map/all_to_all | solution.py:374
  35.8 0.2 share.1
  35.9 0.1 collective-permute-start.6
  36.0 1.6 %collective-permute-start.8 = (bf16[8,1024]{1,0:T(8,128)(2,1)S(1)}, bf16[8,1024]{1,0:T(8,128)(2,1)S(1)}, u32[]{:S(2)}, u32[]{:S(2)}) collective-permute-start(bf16[8,1024]{1,0:T(8,128)(2,1)S(1)} %get-tuple-element.34.share), channel_id=1, source_target_pairs={{0,3},{1,2},{2,1},{3,0},{4,7},{5,6},{6,5},{7,4},{8,11},{9,10},{10,... | collective-permute-start | bytes 49160 | tf_op jit(solution)/shard_map/ppermute | solution.py:97
  37.6 0.5 %collective-permute-start.7 = (bf16[8,1024]{1,0:T(8,128)(2,1)S(1)}, bf16[8,1024]{1,0:T(8,128)(2,1)S(1)}, u32[]{:S(2)}, u32[]{:S(2)}) collective-permute-start(bf16[8,1024]{1,0:T(8,128)(2,1)S(1)} %get-tuple-element.34.share), channel_id=1, source_target_pairs={{0,2},{1,3},{2,0},{3,1},{4,6},{5,7},{6,4},{7,5},{8,10},{9,11},{10,... | collective-permute-start | bytes 49160 | tf_op jit(solution)/shard_map/ppermute | solution.py:97
  38.1 1.1 %collective-permute-done.8.other_far = bf16[8,1024]{1,0:T(8,128)(2,1)S(1)} collective-permute-done((bf16[8,1024]{1,0:T(8,128)(2,1)S(1)}, bf16[8,1024]{1,0:T(8,128)(2,1)S(1)}, u32[]{:S(2)}, u32[]{:S(2)}) %collective-permute-start.8) | collective-permute-done | bytes 16416 | tf_op jit(solution)/shard_map/ppermute | solution.py:97
  39.2 2.1 %collective-permute-done.7.other_y = bf16[8,1024]{1,0:T(8,128)(2,1)S(1)} collective-permute-done((bf16[8,1024]{1,0:T(8,128)(2,1)S(1)}, bf16[8,1024]{1,0:T(8,128)(2,1)S(1)}, u32[]{:S(2)}, u32[]{:S(2)}) %collective-permute-start.7) | collective-permute-done | bytes 16416 | tf_op jit(solution)/shard_map/ppermute | solution.py:97
  41.4 0.0 collective-permute-done.6.both
  41.4 0.7 %last.1 = bf16[16,256]{1,0:T(8,128)(2,1)} custom-call(bf16[8,1024]{1,0:T(8,128)(2,1)S(1)} %get-tuple-element.34.share, bf16[2,8,1024]{2,1,0:T(8,128)(2,1)S(1)} %collective-permute-done.6.both, bf16[8,1024]{1,0:T(8,128)(2,1)S(1)} %collective-permute-done.7.other_y, bf16[8,1024]{1,0:T(8,128)(2,1)S(1)} %collective-permute-done.8.other_far, ...), custom_call_target="tpu_custom_call" | custom-call | tf_op jit(solution)/shard_map/last/pallas_call | solution.py:336
  (17 shorter events, 0.0 us)
Async XLA Ops:
  0.0 1.9 %copy-start.8 = (bf16[16,1024]{1,0:T(8,128)(2,1)S(1)}, bf16[16,1024]{1,0:T(8,128)(2,1)}, u32[]{:S(2)}) copy-start(bf16[16,1024]{1,0:T(8,128)(2,1)} %refs_4_.1) | copy-start | bytes 98308
  0.0 1.9 %copy-start.2 = (bf16[256,1024]{1,0:T(8,128)(2,1)S(1)}, bf16[256,1024]{1,0:T(8,128)(2,1)}, u32[]{:S(2)}) copy-start(bf16[256,1024]{1,0:T(8,128)(2,1)} %refs_11_.1) | copy-start | bytes 1572868
  0.0 2.0 %copy-start.14 = (f32[256]{0:T(256)S(1)}, f32[256]{0:T(256)}, u32[]{:S(2)}) copy-start(f32[256]{0:T(256)} %param.32) | copy-start | bytes 3076
  0.0 2.0 %copy-start.13 = (bf16[1024,1]{0,1:T(2,128)(2,1)S(1)}, bf16[1024,1]{0,1:T(2,128)(2,1)}, u32[]{:S(2)}) copy-start(bf16[1024,1]{0,1:T(2,128)(2,1)} %param.29) | copy-start | bytes 6148
  0.0 2.0 %copy-start.12 = (bf16[1024,1]{0,1:T(2,128)(2,1)S(1)}, bf16[1024,1]{0,1:T(2,128)(2,1)}, u32[]{:S(2)}) copy-start(bf16[1024,1]{0,1:T(2,128)(2,1)} %param.28) | copy-start | bytes 6148
  0.0 2.0 %copy-start.1 = (bf16[1024,256]{1,0:T(8,128)(2,1)S(1)}, bf16[1024,256]{1,0:T(8,128)(2,1)}, u32[]{:S(2)}) copy-start(bf16[1024,256]{1,0:T(8,128)(2,1)} %refs_8_.1) | copy-start | bytes 1572868
  0.0 2.0 %copy-start.7 = (bf16[1024,128]{1,0:T(8,128)(2,1)S(1)}, bf16[1024,128]{1,0:T(8,128)(2,1)}, u32[]{:S(2)}) copy-start(bf16[1024,128]{1,0:T(8,128)(2,1)} %refs_7_.1) | copy-start | bytes 786436
  0.0 2.0 %copy-start.6 = (bf16[1024,128]{1,0:T(8,128)(2,1)S(1)}, bf16[1024,128]{1,0:T(8,128)(2,1)}, u32[]{:S(2)}) copy-start(bf16[1024,128]{1,0:T(8,128)(2,1)} %refs_6_.1) | copy-start | bytes 786436
  0.0 2.0 %copy-start.11 = (f32[1024]{0:T(1024)S(1)}, f32[1024]{0:T(1024)}, u32[]{:S(2)}) copy-start(f32[1024]{0:T(1024)} %param.24) | copy-start | bytes 12292
  0.1 2.0 %copy-start.16 = (f32[16,1]{0,1:T(1,128)S(1)}, f32[16,1]{0,1:T(1,128)}, u32[]{:S(2)}) copy-start(f32[16,1]{0,1:T(1,128)} %param.23) | copy-start | bytes 196
  0.1 2.1 %copy-start = (f32[16,1,128,256]{3,2,1,0:T(8,128)S(1)}, f32[16,1,128,256]{3,2,1,0:T(8,128)}, u32[]{:S(2)}) copy-start(f32[16,1,128,256]{3,2,1,0:T(8,128)} %refs_9_.1) | copy-start | bytes 6291460
  1.8 1.5 %copy-start.3 = (bf16[1,1024,256]{2,1,0:T(8,128)(2,1)S(1)}, bf16[1,1024,256]{2,1,0:T(8,128)(2,1)}, u32[]{:S(2)}) copy-start(bf16[1,1024,256]{2,1,0:T(8,128)(2,1)} %param.38) | copy-start | bytes 1572868
  1.9 2.1 %copy-start.4 = (bf16[1,1024,256]{2,1,0:T(8,128)(2,1)S(1)}, bf16[1,1024,256]{2,1,0:T(8,128)(2,1)}, u32[]{:S(2)}) copy-start(bf16[1,1024,256]{2,1,0:T(8,128)(2,1)} %param.39) | copy-start | bytes 1572868
  1.9 2.2 %copy-start.5 = (bf16[1,256,1024]{2,1,0:T(8,128)(2,1)S(1)}, bf16[1,256,1024]{2,1,0:T(8,128)(2,1)}, u32[]{:S(2)}) copy-start(bf16[1,256,1024]{2,1,0:T(8,128)(2,1)} %param.40) | copy-start | bytes 1572868
  1.9 8.0 %copy-start.17 = (f32[16,6]{0,1:T(8,128)S(1)}, f32[16,6]{0,1:T(8,128)}, u32[]{:S(2)}) copy-start(f32[16,6]{0,1:T(8,128)} %param.37) | copy-start | bytes 1156
  1.9 8.0 %copy-start.18 = (s32[16,6]{0,1:T(8,128)S(1)}, s32[16,6]{0,1:T(8,128)}, u32[]{:S(2)}) copy-start(s32[16,6]{0,1:T(8,128)} %param.36) | copy-start | bytes 1156
  1.9 9.7 %copy-start.9 = (f32[1024]{0:T(1024)S(1)}, f32[1024]{0:T(1024)}, u32[]{:S(2)}) copy-start(f32[1024]{0:T(1024)} %param.34) | copy-start | bytes 12292
  1.9 9.7 %copy-start.10 = (f32[1024]{0:T(1024)S(1)}, f32[1024]{0:T(1024)}, u32[]{:S(2)}) copy-start(f32[1024]{0:T(1024)} %param.35) | copy-start | bytes 12292
  3.4 21.9 %collective-permute-start.3 = (bf16[1024,256]{1,0:T(8,128)(2,1)S(1)}, bf16[1024,256]{1,0:T(8,128)(2,1)S(1)}, u32[]{:S(2)}, u32[]{:S(2)}) collective-permute-start(bf16[1024,256]{1,0:T(8,128)(2,1)S(1)} %bitcast.12), channel_id=1, source_target_pairs={{0,1},{1,0},{2,3},{3,2},{4,5},{5,4},{6,7},{7,6},{8,9},{9,8},{10,11... | collective-permute-start | bytes 1572872 | tf_op jit(solution)/shard_map/ppermute | solution.py:97
  3.9 21.3 %collective-permute-start.4 = (bf16[1024,256]{1,0:T(8,128)(2,1)S(1)}, bf16[1024,256]{1,0:T(8,128)(2,1)S(1)}, u32[]{:S(2)}, u32[]{:S(2)}) collective-permute-start(bf16[1024,256]{1,0:T(8,128)(2,1)S(1)} %bitcast.14), channel_id=1, source_target_pairs={{0,1},{1,0},{2,3},{3,2},{4,5},{5,4},{6,7},{7,6},{8,9},{9,8},{10,11... | collective-permute-start | bytes 1572872 | tf_op jit(solution)/shard_map/ppermute | solution.py:97
  4.0 21.2 %collective-permute-start.5 = (bf16[256,1024]{1,0:T(8,128)(2,1)S(1)}, bf16[256,1024]{1,0:T(8,128)(2,1)S(1)}, u32[]{:S(2)}, u32[]{:S(2)}) collective-permute-start(bf16[256,1024]{1,0:T(8,128)(2,1)S(1)} %bitcast.16), channel_id=1, source_target_pairs={{0,1},{1,0},{2,3},{3,2},{4,5},{5,4},{6,7},{7,6},{8,9},{9,8},{10,11... | collective-permute-start | bytes 1572872 | tf_op jit(solution)/shard_map/ppermute | solution.py:97
  4.5 2.7 %collective-permute-start.2 = (bf16[8,1024]{1,0:T(8,128)(2,1)S(1)}, bf16[8,1024]{1,0:T(8,128)(2,1)S(1)}, u32[]{:S(2)}, u32[]{:S(2)}) collective-permute-start(bf16[8,1024]{1,0:T(8,128)(2,1)S(1)} %get-tuple-element.22), channel_id=1, source_target_pairs={{0,1},{1,0},{2,3},{3,2},{4,5},{5,4},{6,7},{7,6},{8,9},{9,8},{10,11... | collective-permute-start | bytes 49160 | tf_op jit(solution)/shard_map/ppermute | solution.py:97
  4.5 5.4 %collective-permute-start.1 = (bf16[8,1024]{1,0:T(8,128)(2,1)S(1)}, bf16[8,1024]{1,0:T(8,128)(2,1)S(1)}, u32[]{:S(2)}, u32[]{:S(2)}) collective-permute-start(bf16[8,1024]{1,0:T(8,128)(2,1)S(1)} %get-tuple-element.22), channel_id=1, source_target_pairs={{0,3},{1,2},{2,1},{3,0},{4,7},{5,6},{6,5},{7,4},{8,11},{9,10},{10,... | collective-permute-start | bytes 49160 | tf_op jit(solution)/shard_map/ppermute | solution.py:97
  7.2 4.4 %collective-permute-start = (bf16[8,1024]{1,0:T(8,128)(2,1)S(1)}, bf16[8,1024]{1,0:T(8,128)(2,1)S(1)}, u32[]{:S(2)}, u32[]{:S(2)}) collective-permute-start(bf16[8,1024]{1,0:T(8,128)(2,1)S(1)} %get-tuple-element.21.refs_0_), channel_id=1, source_target_pairs={{0,2},{1,3},{2,0},{3,1},{4,6},{5,7},{6,4},{7,5},{8,10},{9,11},{10,... | collective-permute-start | bytes 49160 | tf_op jit(solution)/shard_map/ppermute | solution.py:97
  11.6 29.8 %copy-start.15 = (f32[256]{0:T(256)S(1)}, f32[256]{0:T(256)}, u32[]{:S(2)}) copy-start(f32[256]{0:T(256)} %param.41) | copy-start | bytes 3076
  35.9 5.4 %collective-permute-start.6 = (bf16[2,8,1024]{2,1,0:T(8,128)(2,1)S(1)}, bf16[2,8,1024]{2,1,0:T(8,128)(2,1)S(1)}, u32[]{:S(2)}, u32[]{:S(2)}) collective-permute-start(bf16[2,8,1024]{2,1,0:T(8,128)(2,1)S(1)} %get-tuple-element.35), channel_id=1, source_target_pairs={{0,1},{1,0},{2,3},{3,2},{4,5},{5,4},{6,7},{7,6},{8,9},{9,8},{10,11... | collective-permute-start | bytes 98312 | tf_op jit(solution)/shard_map/ppermute | solution.py:97
  36.0 3.2 %collective-permute-start.8 = (bf16[8,1024]{1,0:T(8,128)(2,1)S(1)}, bf16[8,1024]{1,0:T(8,128)(2,1)S(1)}, u32[]{:S(2)}, u32[]{:S(2)}) collective-permute-start(bf16[8,1024]{1,0:T(8,128)(2,1)S(1)} %get-tuple-element.34.share), channel_id=1, source_target_pairs={{0,3},{1,2},{2,1},{3,0},{4,7},{5,6},{6,5},{7,4},{8,11},{9,10},{10,... | collective-permute-start | bytes 49160 | tf_op jit(solution)/shard_map/ppermute | solution.py:97
  37.6 3.7 %collective-permute-start.7 = (bf16[8,1024]{1,0:T(8,128)(2,1)S(1)}, bf16[8,1024]{1,0:T(8,128)(2,1)S(1)}, u32[]{:S(2)}, u32[]{:S(2)}) collective-permute-start(bf16[8,1024]{1,0:T(8,128)(2,1)S(1)} %get-tuple-element.34.share), channel_id=1, source_target_pairs={{0,2},{1,3},{2,0},{3,1},{4,6},{5,7},{6,4},{7,5},{8,10},{9,11},{10,... | collective-permute-start | bytes 49160 | tf_op jit(solution)/shard_map/ppermute | solution.py:97

commit v10 on v9

--- a/solution.py
+++ b/solution.py
@@ -45,7 +45,8 @@
     experts_all = local_experts * groups
     top = routes.shape[1]
     cap = min(seqs, max(2, 3 * seqs * top // (2 * experts_all)))
-    dense = cap == seqs and local_experts == 1 and lanes == 4 and seqs % 16 == 0
+    paired = lanes % 2 == 0 and lanes & (lanes - 1) == 0 and seqs % 16 == 0
+    dense = cap == seqs and local_experts == 1 and paired
     partial_value = cell(
         tokens,
         memory,
@@ -312,11 +313,17 @@
     )(back, weights, resid)
 
 
-def last_body(share, both, other_y, other_far, resid, gain, out, picks):
-    f32 = jnp.float32
+def last_body(count, *refs):
+    f32 = jnp.float32
+    sames, others = refs[:count], refs[count : 2 * count - 1]
+    both, resid, gain, out, picks = refs[2 * count - 1 :]
     quarter = out.shape[1]
-    kept = share[...].astype(f32) + other_y[...].astype(f32)
-    other = both[0].astype(f32) + other_far[...].astype(f32)
+    kept = sames[0][...].astype(f32)
+    for part in sames[1:]:
+        kept = kept + part[...].astype(f32)
+    other = both[0].astype(f32)
+    for part in others:
+        other = other + part[...].astype(f32)
     picks[0] = kept * rms_scale(kept)
     picks[1] = other * rms_scale(other)
     picks[2] = resid[...].astype(f32)
@@ -330,18 +337,23 @@
     out[...] = jnp.concatenate([low, high], axis=0).astype(jnp.bfloat16)
 
 
-def last(share, both, other_y, other_far, resid, gain):
-    half, width = share.shape
+def last(same, both, other, resid, gain):
+    half, width = resid.shape
     quarter = gain.shape[0]
+    operands = [*same, *other, both, resid, gain.reshape(1, quarter)]
     return pl.pallas_call(
-        last_body,
+        lambda *refs: last_body(len(same), *refs),
         out_shape=jax.ShapeDtypeStruct((2 * half, quarter), jnp.bfloat16),
-        in_specs=[whole()] * 6,
+        in_specs=[whole()] * len(operands),
         out_specs=whole(),
         scratch_shapes=[pltpu.VMEM((4, half, width), jnp.float32)],
         compiler_params=pltpu.CompilerParams(vmem_limit_bytes=8 << 20),
         name="last",
-    )(share, both, other_y, other_far, resid, gain.reshape(1, quarter))
+    )(*operands)
+
+
+def odds_first(lanes):
+    return [*range(3, lanes, 2), *range(2, lanes, 2), 1]
 
 
 def every_token(
@@ -357,9 +369,10 @@
     ffn_gain_out,
 ):
     groups = lax.axis_size("ep")
+    lanes = lax.axis_size("tp")
     mine, theirs = halves
     parts = [mine]
-    for step in (2, 3, 1):
+    for step in odds_first(lanes):
         parts.append(exchange(theirs if step % 2 else mine, "tp", step))
     shards = (expert_gate[0], expert_up[0], expert_down[0])
     *waited, _ = lax.optimization_barrier((*shards, mine))
@@ -374,9 +387,11 @@
     back = lax.all_to_all(blocks, "ep", split_axis=0, concat_axis=0, tiled=True)
     share, both = combine(back, weights, resid)
     sums = {}
-    for step in (3, 2, 1):
+    for step in odds_first(lanes):
         sums[step] = exchange(both if step == 1 else share, "tp", step)
-    return last(share, sums[1], sums[2], sums[3], resid, gain_out)
+    same = [share] + [sums[step] for step in range(2, lanes, 2)]
+    other = [sums[step] for step in range(3, lanes, 2)]
+    return last(same, sums[1], other, resid, gain_out)
 
 
 def slotted(ffn_in, routes, route_weights, expert_gate, expert_up, expert_down, cap):

time: 42.3 us -> 42.3 us (level)
  no operation moved by 1% of the time
where the time goes in v10:
time: 42.3 us; the launch traced here: 42.1 us
  blocking collectives  23.2 us (55%)
  starting transfers between devices  8.68 us (21%)
  waiting for transfers between devices  4.94 us (12%)
  Pallas kernels  3.01 us (7%)
  between operations  2.02 us (5%)
    all_to_all x1, blocking collectives, every_token(): rows = lax.all_to_all(spread, 'ep', split_axis=0, concat_axis=0, tiled=True)  13.4 us
    all_to_all x1, blocking collectives, every_token(): back = lax.all_to_all(blocks, 'ep', split_axis=0, concat_axis=0, tiled=True)  9.74 us
    ppermute x9, starting transfers between devices, exchange(): return lax.ppermute(value, axis, pairs)  8.68 us
    ppermute x9, waiting for transfers between devices, exchange(): return lax.ppermute(value, axis, pairs)  4.94 us
    pallas_call x1, Pallas kernels, cell(): pl.pallas_call(body, out_shape=[shape] * (2 if halves else 1), in_specs=[...  1.19 us
  transfers between devices with their start and end apart: 9, of which 3 were waited for; matrix products, arithmetic and copies ran while one was open for 0% of the time, Pallas kernels for 0%

profile of v10, /device:TPU:0, one launch (start us, length us, event | category | flops | bytes accessed | tf_op | source)
XLA Modules:
  0.0 42.1 jit_solution(14456521094886859821)
XLA Ops:
  0.0 0.0 copy-start.1
  0.0 0.0 copy-start.7
  0.0 0.0 copy-start.6
  1.8 0.0 copy-start.3
  1.9 0.0 copy-start.4
  1.9 0.0 copy-start.5
  1.9 0.0 copy-start.17
  1.9 0.0 copy-start.18
  1.9 0.0 copy-start.9
  1.9 0.0 copy-start.10
  1.9 0.0 copy-done.8
  1.9 0.0 copy-done.2
  2.0 0.0 copy-done.14
  2.0 0.0 copy-done.13
  2.0 0.0 copy-done.12
  2.0 0.0 copy-done.1
  2.0 0.0 copy-done.7
  2.0 0.0 copy-done.6
  2.0 0.0 copy-done.11
  2.0 0.0 copy-done.16
  2.0 0.1 copy-done
  2.2 1.2 %cell.1 = (bf16[8,1024]{1,0:T(8,128)(2,1)S(1)}, bf16[8,1024]{1,0:T(8,128)(2,1)S(1)}) custom-call(bf16[16,1024]{1,0:T(8,128)(2,1)S(1)} %copy-done.8, f32[1,1024]{1,0:T(1,128)S(1)} %bitcast.21, bf16[1,1024]{1,0:T(2,128)(2,1)S(1)} %bitcast.22, bf16[1,1024]{1,0:T(2,128)(2,1)S(1)} %bitcast.23, f32[2,1]{1,0:T(2,128)S(1)} %biases.1.refs_4_, f32[1,16]{1,0:T(1,128)S(1)} %bitcast.26, ...), custom_call_target="tpu_custom_call" | custom-call | tf_op jit(solution)/shard_map/cell/pallas_call | solution.py:216
  3.4 0.6 %collective-permute-start.3 = (bf16[1024,256]{1,0:T(8,128)(2,1)S(1)}, bf16[1024,256]{1,0:T(8,128)(2,1)S(1)}, u32[]{:S(2)}, u32[]{:S(2)}) collective-permute-start(bf16[1024,256]{1,0:T(8,128)(2,1)S(1)} %bitcast.12), channel_id=1, source_target_pairs={{0,1},{1,0},{2,3},{3,2},{4,5},{5,4},{6,7},{7,6},{8,9},{9,8},{10,11... | collective-permute-start | bytes 1572872 | tf_op jit(solution)/shard_map/ppermute | solution.py:98
  3.9 0.1 collective-permute-start.4
  4.0 0.0 copy-done.5
  4.0 0.4 %collective-permute-start.5 = (bf16[256,1024]{1,0:T(8,128)(2,1)S(1)}, bf16[256,1024]{1,0:T(8,128)(2,1)S(1)}, u32[]{:S(2)}, u32[]{:S(2)}) collective-permute-start(bf16[256,1024]{1,0:T(8,128)(2,1)S(1)} %bitcast.16), channel_id=1, source_target_pairs={{0,1},{1,0},{2,3},{3,2},{4,5},{5,4},{6,7},{7,6},{8,9},{9,8},{10,11... | collective-permute-start | bytes 1572872 | tf_op jit(solution)/shard_map/ppermute | solution.py:98
  4.5 0.1 collective-permute-start.2
  4.5 2.6 %collective-permute-start = (bf16[8,1024]{1,0:T(8,128)(2,1)S(1)}, bf16[8,1024]{1,0:T(8,128)(2,1)S(1)}, u32[]{:S(2)}, u32[]{:S(2)}) collective-permute-start(bf16[8,1024]{1,0:T(8,128)(2,1)S(1)} %get-tuple-element.22), channel_id=1, source_target_pairs={{0,3},{1,2},{2,1},{3,0},{4,7},{5,6},{6,5},{7,4},{8,11},{9,10},{10,... | collective-permute-start | bytes 49160 | tf_op jit(solution)/shard_map/ppermute | solution.py:98
  7.2 0.0 collective-permute-done.2.refs_3_
  7.2 2.7 %collective-permute-start.1 = (bf16[8,1024]{1,0:T(8,128)(2,1)S(1)}, bf16[8,1024]{1,0:T(8,128)(2,1)S(1)}, u32[]{:S(2)}, u32[]{:S(2)}) collective-permute-start(bf16[8,1024]{1,0:T(8,128)(2,1)S(1)} %get-tuple-element.21.refs_0_), channel_id=1, source_target_pairs={{0,2},{1,3},{2,0},{3,1},{4,6},{5,7},{6,4},{7,5},{8,10},{9,11},{10,... | collective-permute-start | bytes 49160 | tf_op jit(solution)/shard_map/ppermute | solution.py:98
  9.9 0.0 collective-permute-done.refs_1_
  9.9 1.7 %collective-permute-done.1.refs_2_ = bf16[8,1024]{1,0:T(8,128)(2,1)S(1)} collective-permute-done((bf16[8,1024]{1,0:T(8,128)(2,1)S(1)}, bf16[8,1024]{1,0:T(8,128)(2,1)S(1)}, u32[]{:S(2)}, u32[]{:S(2)}) %collective-permute-start.1) | collective-permute-done | bytes 16416 | tf_op jit(solution)/shard_map/ppermute | solution.py:98
  11.6 0.0 copy-done.10
  11.6 0.2 after_mix.1
  11.8 13.4 %all_to_all.10.rows = bf16[8,8,1024]{2,1,0:T(8,128)(2,1)S(1)} all-to-all(bf16[8,8,1024]{2,1,0:T(8,128)(2,1)S(1)} %get-tuple-element.24), channel_id=1, replica_groups=mesh['ep'=8,'tp'=4] {'ep'}, dimensions={0} | all-to-all | bytes 262144 | tf_op jit(solution)/shard_map/all_to_all | solution.py:384
  25.3 0.0 collective-permute-done.3.gate_n
  25.3 0.0 collective-permute-done.4.up_n
  25.3 0.0 collective-permute-done.5.down_n
  25.3 0.7 %expert.1 = bf16[8,8,1024]{2,1,0:T(8,128)(2,1)S(1)} custom-call(bf16[8,8,1024]{2,1,0:T(8,128)(2,1)S(1)} %all_to_all.10.rows, bf16[1024,256]{1,0:T(8,128)(2,1)S(1)} %bitcast.13, bf16[1024,256]{1,0:T(8,128)(2,1)S(1)} %bitcast.15, bf16[256,1024]{1,0:T(8,128)(2,1)S(1)} %bitcast.17, bf16[1024,256]{1,0:T(8,128)(2,1)S(1)} %collective-permute-done.3.gate_n, ...), custom_call_target="tpu_custom_call" | custom-call | tf_op jit(solution)/shard_map/expert/pallas_call | solution.py:276
  26.0 9.7 %all_to_all.11.back = bf16[8,8,1024]{2,1,0:T(8,128)(2,1)S(1)} all-to-all(bf16[8,8,1024]{2,1,0:T(8,128)(2,1)S(1)} %expert.1), channel_id=1, replica_groups=mesh['ep'=8,'tp'=4] {'ep'}, dimensions={0} | all-to-all | bytes 262144 | tf_op jit(solution)/shard_map/all_to_all | solution.py:387
  35.8 0.2 share.1
  35.9 0.1 collective-permute-start.8
  36.0 1.6 %collective-permute-start.7 = (bf16[8,1024]{1,0:T(8,128)(2,1)S(1)}, bf16[8,1024]{1,0:T(8,128)(2,1)S(1)}, u32[]{:S(2)}, u32[]{:S(2)}) collective-permute-start(bf16[8,1024]{1,0:T(8,128)(2,1)S(1)} %get-tuple-element.34.refs_0_), channel_id=1, source_target_pairs={{0,3},{1,2},{2,1},{3,0},{4,7},{5,6},{6,5},{7,4},{8,11},{9,10},{10,... | collective-permute-start | bytes 49160 | tf_op jit(solution)/shard_map/ppermute | solution.py:98
  37.6 0.5 %collective-permute-start.6 = (bf16[8,1024]{1,0:T(8,128)(2,1)S(1)}, bf16[8,1024]{1,0:T(8,128)(2,1)S(1)}, u32[]{:S(2)}, u32[]{:S(2)}) collective-permute-start(bf16[8,1024]{1,0:T(8,128)(2,1)S(1)} %get-tuple-element.34.refs_0_), channel_id=1, source_target_pairs={{0,2},{1,3},{2,0},{3,1},{4,6},{5,7},{6,4},{7,5},{8,10},{9,11},{10,... | collective-permute-start | bytes 49160 | tf_op jit(solution)/shard_map/ppermute | solution.py:98
  38.1 1.1 %collective-permute-done.7.refs_2_ = bf16[8,1024]{1,0:T(8,128)(2,1)S(1)} collective-permute-done((bf16[8,1024]{1,0:T(8,128)(2,1)S(1)}, bf16[8,1024]{1,0:T(8,128)(2,1)S(1)}, u32[]{:S(2)}, u32[]{:S(2)}) %collective-permute-start.7) | collective-permute-done | bytes 16416 | tf_op jit(solution)/shard_map/ppermute | solution.py:98
  39.2 2.1 %collective-permute-done.6.refs_1_ = bf16[8,1024]{1,0:T(8,128)(2,1)S(1)} collective-permute-done((bf16[8,1024]{1,0:T(8,128)(2,1)S(1)}, bf16[8,1024]{1,0:T(8,128)(2,1)S(1)}, u32[]{:S(2)}, u32[]{:S(2)}) %collective-permute-start.6) | collective-permute-done | bytes 16416 | tf_op jit(solution)/shard_map/ppermute | solution.py:98
  41.4 0.0 collective-permute-done.8.refs_3_
  41.4 0.7 %last.1 = bf16[16,256]{1,0:T(8,128)(2,1)} custom-call(bf16[8,1024]{1,0:T(8,128)(2,1)S(1)} %get-tuple-element.34.refs_0_, bf16[8,1024]{1,0:T(8,128)(2,1)S(1)} %collective-permute-done.6.refs_1_, bf16[8,1024]{1,0:T(8,128)(2,1)S(1)} %collective-permute-done.7.refs_2_, bf16[2,8,1024]{2,1,0:T(8,128)(2,1)S(1)} %collective-permute-done.8.refs_3_, ...), custom_call_target="tpu_custom_call" | custom-call | tf_op jit(solution)/shard_map/last/pallas_call | solution.py:344
  (17 shorter events, 0.0 us)
Async XLA Ops:
  0.0 1.9 %copy-start.8 = (bf16[16,1024]{1,0:T(8,128)(2,1)S(1)}, bf16[16,1024]{1,0:T(8,128)(2,1)}, u32[]{:S(2)}) copy-start(bf16[16,1024]{1,0:T(8,128)(2,1)} %refs_4_.1) | copy-start | bytes 98308
  0.0 1.9 %copy-start.2 = (bf16[256,1024]{1,0:T(8,128)(2,1)S(1)}, bf16[256,1024]{1,0:T(8,128)(2,1)}, u32[]{:S(2)}) copy-start(bf16[256,1024]{1,0:T(8,128)(2,1)} %refs_11_.1) | copy-start | bytes 1572868
  0.0 2.0 %copy-start.14 = (f32[256]{0:T(256)S(1)}, f32[256]{0:T(256)}, u32[]{:S(2)}) copy-start(f32[256]{0:T(256)} %param.32) | copy-start | bytes 3076
  0.0 2.0 %copy-start.13 = (bf16[1024,1]{0,1:T(2,128)(2,1)S(1)}, bf16[1024,1]{0,1:T(2,128)(2,1)}, u32[]{:S(2)}) copy-start(bf16[1024,1]{0,1:T(2,128)(2,1)} %param.29) | copy-start | bytes 6148
  0.0 2.0 %copy-start.12 = (bf16[1024,1]{0,1:T(2,128)(2,1)S(1)}, bf16[1024,1]{0,1:T(2,128)(2,1)}, u32[]{:S(2)}) copy-start(bf16[1024,1]{0,1:T(2,128)(2,1)} %param.28) | copy-start | bytes 6148
  0.0 2.0 %copy-start.1 = (bf16[1024,256]{1,0:T(8,128)(2,1)S(1)}, bf16[1024,256]{1,0:T(8,128)(2,1)}, u32[]{:S(2)}) copy-start(bf16[1024,256]{1,0:T(8,128)(2,1)} %refs_8_.1) | copy-start | bytes 1572868
  0.0 2.0 %copy-start.7 = (bf16[1024,128]{1,0:T(8,128)(2,1)S(1)}, bf16[1024,128]{1,0:T(8,128)(2,1)}, u32[]{:S(2)}) copy-start(bf16[1024,128]{1,0:T(8,128)(2,1)} %refs_7_.1) | copy-start | bytes 786436
  0.0 2.0 %copy-start.6 = (bf16[1024,128]{1,0:T(8,128)(2,1)S(1)}, bf16[1024,128]{1,0:T(8,128)(2,1)}, u32[]{:S(2)}) copy-start(bf16[1024,128]{1,0:T(8,128)(2,1)} %refs_6_.1) | copy-start | bytes 786436
  0.0 2.0 %copy-start.11 = (f32[1024]{0:T(1024)S(1)}, f32[1024]{0:T(1024)}, u32[]{:S(2)}) copy-start(f32[1024]{0:T(1024)} %param.24) | copy-start | bytes 12292
  0.1 2.0 %copy-start.16 = (f32[16,1]{0,1:T(1,128)S(1)}, f32[16,1]{0,1:T(1,128)}, u32[]{:S(2)}) copy-start(f32[16,1]{0,1:T(1,128)} %param.23) | copy-start | bytes 196
  0.1 2.1 %copy-start = (f32[16,1,128,256]{3,2,1,0:T(8,128)S(1)}, f32[16,1,128,256]{3,2,1,0:T(8,128)}, u32[]{:S(2)}) copy-start(f32[16,1,128,256]{3,2,1,0:T(8,128)} %refs_9_.1) | copy-start | bytes 6291460
  1.8 1.5 %copy-start.3 = (bf16[1,1024,256]{2,1,0:T(8,128)(2,1)S(1)}, bf16[1,1024,256]{2,1,0:T(8,128)(2,1)}, u32[]{:S(2)}) copy-start(bf16[1,1024,256]{2,1,0:T(8,128)(2,1)} %param.38) | copy-start | bytes 1572868
  1.9 2.1 %copy-start.4 = (bf16[1,1024,256]{2,1,0:T(8,128)(2,1)S(1)}, bf16[1,1024,256]{2,1,0:T(8,128)(2,1)}, u32[]{:S(2)}) copy-start(bf16[1,1024,256]{2,1,0:T(8,128)(2,1)} %param.39) | copy-start | bytes 1572868
  1.9 2.2 %copy-start.5 = (bf16[1,256,1024]{2,1,0:T(8,128)(2,1)S(1)}, bf16[1,256,1024]{2,1,0:T(8,128)(2,1)}, u32[]{:S(2)}) copy-start(bf16[1,256,1024]{2,1,0:T(8,128)(2,1)} %param.40) | copy-start | bytes 1572868
  1.9 8.0 %copy-start.17 = (f32[16,6]{0,1:T(8,128)S(1)}, f32[16,6]{0,1:T(8,128)}, u32[]{:S(2)}) copy-start(f32[16,6]{0,1:T(8,128)} %param.37) | copy-start | bytes 1156
  1.9 8.0 %copy-start.18 = (s32[16,6]{0,1:T(8,128)S(1)}, s32[16,6]{0,1:T(8,128)}, u32[]{:S(2)}) copy-start(s32[16,6]{0,1:T(8,128)} %param.36) | copy-start | bytes 1156
  1.9 9.7 %copy-start.9 = (f32[1024]{0:T(1024)S(1)}, f32[1024]{0:T(1024)}, u32[]{:S(2)}) copy-start(f32[1024]{0:T(1024)} %param.34) | copy-start | bytes 12292
  1.9 9.7 %copy-start.10 = (f32[1024]{0:T(1024)S(1)}, f32[1024]{0:T(1024)}, u32[]{:S(2)}) copy-start(f32[1024]{0:T(1024)} %param.35) | copy-start | bytes 12292
  3.4 21.9 %collective-permute-start.3 = (bf16[1024,256]{1,0:T(8,128)(2,1)S(1)}, bf16[1024,256]{1,0:T(8,128)(2,1)S(1)}, u32[]{:S(2)}, u32[]{:S(2)}) collective-permute-start(bf16[1024,256]{1,0:T(8,128)(2,1)S(1)} %bitcast.12), channel_id=1, source_target_pairs={{0,1},{1,0},{2,3},{3,2},{4,5},{5,4},{6,7},{7,6},{8,9},{9,8},{10,11... | collective-permute-start | bytes 1572872 | tf_op jit(solution)/shard_map/ppermute | solution.py:98
  3.9 21.3 %collective-permute-start.4 = (bf16[1024,256]{1,0:T(8,128)(2,1)S(1)}, bf16[1024,256]{1,0:T(8,128)(2,1)S(1)}, u32[]{:S(2)}, u32[]{:S(2)}) collective-permute-start(bf16[1024,256]{1,0:T(8,128)(2,1)S(1)} %bitcast.14), channel_id=1, source_target_pairs={{0,1},{1,0},{2,3},{3,2},{4,5},{5,4},{6,7},{7,6},{8,9},{9,8},{10,11... | collective-permute-start | bytes 1572872 | tf_op jit(solution)/shard_map/ppermute | solution.py:98
  4.0 21.2 %collective-permute-start.5 = (bf16[256,1024]{1,0:T(8,128)(2,1)S(1)}, bf16[256,1024]{1,0:T(8,128)(2,1)S(1)}, u32[]{:S(2)}, u32[]{:S(2)}) collective-permute-start(bf16[256,1024]{1,0:T(8,128)(2,1)S(1)} %bitcast.16), channel_id=1, source_target_pairs={{0,1},{1,0},{2,3},{3,2},{4,5},{5,4},{6,7},{7,6},{8,9},{9,8},{10,11... | collective-permute-start | bytes 1572872 | tf_op jit(solution)/shard_map/ppermute | solution.py:98
  4.5 2.7 %collective-permute-start.2 = (bf16[8,1024]{1,0:T(8,128)(2,1)S(1)}, bf16[8,1024]{1,0:T(8,128)(2,1)S(1)}, u32[]{:S(2)}, u32[]{:S(2)}) collective-permute-start(bf16[8,1024]{1,0:T(8,128)(2,1)S(1)} %get-tuple-element.22), channel_id=1, source_target_pairs={{0,1},{1,0},{2,3},{3,2},{4,5},{5,4},{6,7},{7,6},{8,9},{9,8},{10,11... | collective-permute-start | bytes 49160 | tf_op jit(solution)/shard_map/ppermute | solution.py:98
  4.5 5.4 %collective-permute-start = (bf16[8,1024]{1,0:T(8,128)(2,1)S(1)}, bf16[8,1024]{1,0:T(8,128)(2,1)S(1)}, u32[]{:S(2)}, u32[]{:S(2)}) collective-permute-start(bf16[8,1024]{1,0:T(8,128)(2,1)S(1)} %get-tuple-element.22), channel_id=1, source_target_pairs={{0,3},{1,2},{2,1},{3,0},{4,7},{5,6},{6,5},{7,4},{8,11},{9,10},{10,... | collective-permute-start | bytes 49160 | tf_op jit(solution)/shard_map/ppermute | solution.py:98
  7.2 4.4 %collective-permute-start.1 = (bf16[8,1024]{1,0:T(8,128)(2,1)S(1)}, bf16[8,1024]{1,0:T(8,128)(2,1)S(1)}, u32[]{:S(2)}, u32[]{:S(2)}) collective-permute-start(bf16[8,1024]{1,0:T(8,128)(2,1)S(1)} %get-tuple-element.21.refs_0_), channel_id=1, source_target_pairs={{0,2},{1,3},{2,0},{3,1},{4,6},{5,7},{6,4},{7,5},{8,10},{9,11},{10,... | collective-permute-start | bytes 49160 | tf_op jit(solution)/shard_map/ppermute | solution.py:98
  11.6 29.8 %copy-start.15 = (f32[256]{0:T(256)S(1)}, f32[256]{0:T(256)}, u32[]{:S(2)}) copy-start(f32[256]{0:T(256)} %param.41) | copy-start | bytes 3076
  35.9 5.4 %collective-permute-start.8 = (bf16[2,8,1024]{2,1,0:T(8,128)(2,1)S(1)}, bf16[2,8,1024]{2,1,0:T(8,128)(2,1)S(1)}, u32[]{:S(2)}, u32[]{:S(2)}) collective-permute-start(bf16[2,8,1024]{2,1,0:T(8,128)(2,1)S(1)} %get-tuple-element.35), channel_id=1, source_target_pairs={{0,1},{1,0},{2,3},{3,2},{4,5},{5,4},{6,7},{7,6},{8,9},{9,8},{10,11... | collective-permute-start | bytes 98312 | tf_op jit(solution)/shard_map/ppermute | solution.py:98
  36.0 3.2 %collective-permute-start.7 = (bf16[8,1024]{1,0:T(8,128)(2,1)S(1)}, bf16[8,1024]{1,0:T(8,128)(2,1)S(1)}, u32[]{:S(2)}, u32[]{:S(2)}) collective-permute-start(bf16[8,1024]{1,0:T(8,128)(2,1)S(1)} %get-tuple-element.34.refs_0_), channel_id=1, source_target_pairs={{0,3},{1,2},{2,1},{3,0},{4,7},{5,6},{6,5},{7,4},{8,11},{9,10},{10,... | collective-permute-start | bytes 49160 | tf_op jit(solution)/shard_map/ppermute | solution.py:98
  37.6 3.7 %collective-permute-start.6 = (bf16[8,1024]{1,0:T(8,128)(2,1)S(1)}, bf16[8,1024]{1,0:T(8,128)(2,1)S(1)}, u32[]{:S(2)}, u32[]{:S(2)}) collective-permute-start(bf16[8,1024]{1,0:T(8,128)(2,1)S(1)} %get-tuple-element.34.refs_0_), channel_id=1, source_target_pairs={{0,2},{1,3},{2,0},{3,1},{4,6},{5,7},{6,4},{7,5},{8,10},{9,11},{10,... | collective-permute-start | bytes 49160 | tf_op jit(solution)/shard_map/ppermute | solution.py:98

commit v11 on v10

--- a/solution.py
+++ b/solution.py
@@ -123,7 +123,7 @@
         in_specs=[pl.BlockSpec(memory_space=pltpu.SMEM)] * 2,
         out_specs=whole(),
         compiler_params=pltpu.CompilerParams(vmem_limit_bytes=1 << 20),
-        cost_estimate=pl.CostEstimate(flops=11 * 10**8, transcendentals=0, bytes_accessed=4096),
+        cost_estimate=pl.CostEstimate(flops=8 * 10**8, transcendentals=0, bytes_accessed=4096),
         name="biases",
     )(igate_bias, fgate_bias)
 
@@ -131,8 +131,12 @@
 def cell_body(heads, key_dim, value_dim, halves, *refs):
     f32 = jnp.float32
     bf16 = jnp.bfloat16
-    (tokens, gain, wi, wf, bias, scale, wq, wk, wv, mem, hg, wo) = refs[:12]
-    outs, recall = refs[12:-1], refs[-1]
+    (tokens, gain, wi, wf, bias, scale, wq, wk, wv_h, mem, hg, wo_h) = refs[:12]
+    outs, (recall, wv, wo, sems) = refs[12:-4], refs[-4:]
+    value_copy = pltpu.make_async_copy(wv_h, wv, sems.at[0])
+    output_copy = pltpu.make_async_copy(wo_h, wo, sems.at[1])
+    value_copy.start()
+    output_copy.start()
     seqs = tokens.shape[0]
     xf = tokens[...].astype(f32)
     normed = (xf * rms_scale(xf) * gain[...]).astype(bf16)
@@ -157,6 +161,7 @@
         for h in range(heads):
             product = turned[h][:, b : b + 1] * mem[b, h]
             recall[h, b : b + 1, :] = jnp.sum(product, axis=0, keepdims=True)
+    value_copy.wait()
     values = jnp.dot(normed, wv[...], preferred_element_type=f32)
     parts = []
     for h in range(heads):
@@ -166,6 +171,7 @@
         read = carries[h] * recall[h] + (fresh[h] * match) * values[:, vs]
         inv = lax.rsqrt(jnp.mean(read * read, axis=1, keepdims=True) + EPS)
         parts.append((read * inv * hg[:, vs]).astype(bf16))
+    output_copy.wait()
     headout = parts[0] if heads == 1 else jnp.concatenate(parts, axis=1)
     product = jnp.dot(headout, wo[...], preferred_element_type=f32)
     if halves:
@@ -197,6 +203,7 @@
     bf16 = jnp.bfloat16
     seqs, width = tokens.shape
     heads, key_dim, value_dim = memory.shape[1:]
+    hbm = pl.BlockSpec(memory_space=pltpu.HBM)
     body = lambda *refs: cell_body(heads, key_dim, value_dim, halves, *refs)
     operands = [
         tokens,
@@ -213,12 +220,20 @@
         w_output,
     ]
     shape = jax.ShapeDtypeStruct((seqs // 2 if halves else seqs, w_output.shape[1]), bf16)
+    late = (8, 11)
+    for i in late:
+        operands[i] = pltpu.with_memory_space_constraint(operands[i], pltpu.HBM)
     result = pl.pallas_call(
         body,
         out_shape=[shape] * (2 if halves else 1),
-        in_specs=[whole()] * len(operands),
+        in_specs=[hbm if i in late else whole() for i in range(len(operands))],
         out_specs=[whole()] * (2 if halves else 1),
-        scratch_shapes=[pltpu.VMEM((heads, seqs, value_dim), f32)],
+        scratch_shapes=[
+            pltpu.VMEM((heads, seqs, value_dim), f32),
+            pltpu.VMEM(w_value.shape, w_value.dtype),
+            pltpu.VMEM(w_output.shape, w_output.dtype),
+            pltpu.SemaphoreType.DMA((2,)),
+        ],
         compiler_params=pltpu.CompilerParams(vmem_limit_bytes=12 << 20),
         name="cell",
     )(*operands)

time: 42.3 us -> 42.7 us (level)
  Pallas kernels: 3.01 us -> 3.65 us
    pallas_call x1, Pallas kernels: 1.19 us -> 1.84 us  [cell(): pl.pallas_call(body, out_shape=[shape] * (2 if halves else 1), in_specs=[...]
where the time goes in v11:
time: 42.7 us; the launch traced here: 42.5 us
  blocking collectives  23.2 us (54%)
  starting transfers between devices  8.72 us (20%)
  waiting for transfers between devices  4.94 us (12%)
  Pallas kernels  3.65 us (9%)
  between operations  1.74 us (4%)
    all_to_all x1, blocking collectives, every_token(): rows = lax.all_to_all(spread, 'ep', split_axis=0, concat_axis=0, tiled=True)  13.4 us
    all_to_all x1, blocking collectives, every_token(): back = lax.all_to_all(blocks, 'ep', split_axis=0, concat_axis=0, tiled=True)  9.74 us
    ppermute x9, starting transfers between devices, exchange(): return lax.ppermute(value, axis, pairs)  8.72 us
    ppermute x9, waiting for transfers between devices, exchange(): return lax.ppermute(value, axis, pairs)  4.94 us
    pallas_call x1, Pallas kernels, cell(): pl.pallas_call(body, out_shape=[shape] * (2 if halves else 1), in_specs=[...  1.84 us
  transfers between devices with their start and end apart: 9, of which 3 were waited for; matrix products, arithmetic and copies ran while one was open for 0% of the time, Pallas kernels for 0%

profile of v11, /device:TPU:0, one launch (start us, length us, event | category | flops | bytes accessed | tf_op | source)
XLA Modules:
  0.0 42.5 jit_solution(13589929361292962656)
XLA Ops:
  0.0 0.0 copy-start.4
  0.0 0.0 copy-start.9
  0.0 0.0 copy-start.14
  0.0 0.0 copy-start
  1.6 0.0 copy-start.1
  1.6 0.0 copy-start.2
  1.6 0.0 copy-start.3
  1.6 0.0 copy-start.15
  1.6 0.0 copy-start.16
  1.6 0.0 copy-start.7
  1.6 0.0 copy-start.8
  1.6 0.0 copy-done.6
  1.7 0.0 copy-done.12
  1.7 0.0 copy-done.11
  1.7 0.0 copy-done.10
  1.7 0.0 copy-done.5
  1.7 0.0 copy-done.4
  1.7 0.0 copy-done.9
  1.7 0.0 copy-done.14
  1.7 0.2 copy-done
  1.9 1.8 %cell.1 = (bf16[8,1024]{1,0:T(8,128)(2,1)S(1)}, bf16[8,1024]{1,0:T(8,128)(2,1)S(1)}) custom-call(bf16[16,1024]{1,0:T(8,128)(2,1)S(1)} %copy-done.6, f32[1,1024]{1,0:T(1,128)S(1)} %bitcast.21, bf16[1,1024]{1,0:T(2,128)(2,1)S(1)} %bitcast.22, bf16[1,1024]{1,0:T(2,128)(2,1)S(1)} %bitcast.23, f32[2,1]{1,0:T(2,128)S(1)} %biases.1.refs_4_, f32[1,16]{1,0:T(1,128)S(1)} %bitcast.26, ...), custom_call_target="tpu_custom_call" | custom-call | tf_op jit(solution)/shard_map/cell/pallas_call | solution.py:226
  3.7 0.0 copy-done.1
  3.7 0.6 %collective-permute-start.3 = (bf16[1024,256]{1,0:T(8,128)(2,1)S(1)}, bf16[1024,256]{1,0:T(8,128)(2,1)S(1)}, u32[]{:S(2)}, u32[]{:S(2)}) collective-permute-start(bf16[1024,256]{1,0:T(8,128)(2,1)S(1)} %bitcast.12), channel_id=1, source_target_pairs={{0,1},{1,0},{2,3},{3,2},{4,5},{5,4},{6,7},{7,6},{8,9},{9,8},{10,11... | collective-permute-start | bytes 1572872 | tf_op jit(solution)/shard_map/ppermute | solution.py:98
  4.3 0.1 collective-permute-start.4
  4.4 0.0 copy-done.3
  4.4 0.4 collective-permute-start.5
  4.9 0.1 collective-permute-start.2
  4.9 2.6 %collective-permute-start = (bf16[8,1024]{1,0:T(8,128)(2,1)S(1)}, bf16[8,1024]{1,0:T(8,128)(2,1)S(1)}, u32[]{:S(2)}, u32[]{:S(2)}) collective-permute-start(bf16[8,1024]{1,0:T(8,128)(2,1)S(1)} %get-tuple-element.22), channel_id=1, source_target_pairs={{0,3},{1,2},{2,1},{3,0},{4,7},{5,6},{6,5},{7,4},{8,11},{9,10},{10,... | collective-permute-start | bytes 49160 | tf_op jit(solution)/shard_map/ppermute | solution.py:98
  7.6 0.0 collective-permute-done.2.refs_3_
  7.6 2.7 %collective-permute-start.1 = (bf16[8,1024]{1,0:T(8,128)(2,1)S(1)}, bf16[8,1024]{1,0:T(8,128)(2,1)S(1)}, u32[]{:S(2)}, u32[]{:S(2)}) collective-permute-start(bf16[8,1024]{1,0:T(8,128)(2,1)S(1)} %get-tuple-element.21.refs_0_), channel_id=1, source_target_pairs={{0,2},{1,3},{2,0},{3,1},{4,6},{5,7},{6,4},{7,5},{8,10},{9,11},{10,... | collective-permute-start | bytes 49160 | tf_op jit(solution)/shard_map/ppermute | solution.py:98
  10.3 0.0 collective-permute-done.refs_1_
  10.3 1.7 %collective-permute-done.1.refs_2_ = bf16[8,1024]{1,0:T(8,128)(2,1)S(1)} collective-permute-done((bf16[8,1024]{1,0:T(8,128)(2,1)S(1)}, bf16[8,1024]{1,0:T(8,128)(2,1)S(1)}, u32[]{:S(2)}, u32[]{:S(2)}) %collective-permute-start.1) | collective-permute-done | bytes 16416 | tf_op jit(solution)/shard_map/ppermute | solution.py:98
  12.0 0.0 copy-done.8
  12.0 0.2 after_mix.1
  12.2 13.4 %all_to_all.10.rows = bf16[8,8,1024]{2,1,0:T(8,128)(2,1)S(1)} all-to-all(bf16[8,8,1024]{2,1,0:T(8,128)(2,1)S(1)} %get-tuple-element.24), channel_id=1, replica_groups=mesh['ep'=8,'tp'=4] {'ep'}, dimensions={0} | all-to-all | bytes 262144 | tf_op jit(solution)/shard_map/all_to_all | solution.py:399
  25.7 0.0 collective-permute-done.3.gate_n
  25.7 0.0 collective-permute-done.4.up_n
  25.7 0.0 collective-permute-done.5.down_n
  25.7 0.7 %expert.1 = bf16[8,8,1024]{2,1,0:T(8,128)(2,1)S(1)} custom-call(bf16[8,8,1024]{2,1,0:T(8,128)(2,1)S(1)} %all_to_all.10.rows, bf16[1024,256]{1,0:T(8,128)(2,1)S(1)} %bitcast.13, bf16[1024,256]{1,0:T(8,128)(2,1)S(1)} %bitcast.15, bf16[256,1024]{1,0:T(8,128)(2,1)S(1)} %bitcast.17, bf16[1024,256]{1,0:T(8,128)(2,1)S(1)} %collective-permute-done.3.gate_n, ...), custom_call_target="tpu_custom_call" | custom-call | tf_op jit(solution)/shard_map/expert/pallas_call | solution.py:291
  26.4 9.7 %all_to_all.11.back = bf16[8,8,1024]{2,1,0:T(8,128)(2,1)S(1)} all-to-all(bf16[8,8,1024]{2,1,0:T(8,128)(2,1)S(1)} %expert.1), channel_id=1, replica_groups=mesh['ep'=8,'tp'=4] {'ep'}, dimensions={0} | all-to-all | bytes 262144 | tf_op jit(solution)/shard_map/all_to_all | solution.py:402
  36.2 0.2 share.1
  36.3 0.1 collective-permute-start.8
  36.4 1.6 %collective-permute-start.7 = (bf16[8,1024]{1,0:T(8,128)(2,1)S(1)}, bf16[8,1024]{1,0:T(8,128)(2,1)S(1)}, u32[]{:S(2)}, u32[]{:S(2)}) collective-permute-start(bf16[8,1024]{1,0:T(8,128)(2,1)S(1)} %get-tuple-element.34.refs_0_), channel_id=1, source_target_pairs={{0,3},{1,2},{2,1},{3,0},{4,7},{5,6},{6,5},{7,4},{8,11},{9,10},{10,... | collective-permute-start | bytes 49160 | tf_op jit(solution)/shard_map/ppermute | solution.py:98
  38.0 0.5 %collective-permute-start.6 = (bf16[8,1024]{1,0:T(8,128)(2,1)S(1)}, bf16[8,1024]{1,0:T(8,128)(2,1)S(1)}, u32[]{:S(2)}, u32[]{:S(2)}) collective-permute-start(bf16[8,1024]{1,0:T(8,128)(2,1)S(1)} %get-tuple-element.34.refs_0_), channel_id=1, source_target_pairs={{0,2},{1,3},{2,0},{3,1},{4,6},{5,7},{6,4},{7,5},{8,10},{9,11},{10,... | collective-permute-start | bytes 49160 | tf_op jit(solution)/shard_map/ppermute | solution.py:98
  38.5 1.1 %collective-permute-done.7.refs_2_ = bf16[8,1024]{1,0:T(8,128)(2,1)S(1)} collective-permute-done((bf16[8,1024]{1,0:T(8,128)(2,1)S(1)}, bf16[8,1024]{1,0:T(8,128)(2,1)S(1)}, u32[]{:S(2)}, u32[]{:S(2)}) %collective-permute-start.7) | collective-permute-done | bytes 16416 | tf_op jit(solution)/shard_map/ppermute | solution.py:98
  39.6 2.1 %collective-permute-done.6.refs_1_ = bf16[8,1024]{1,0:T(8,128)(2,1)S(1)} collective-permute-done((bf16[8,1024]{1,0:T(8,128)(2,1)S(1)}, bf16[8,1024]{1,0:T(8,128)(2,1)S(1)}, u32[]{:S(2)}, u32[]{:S(2)}) %collective-permute-start.6) | collective-permute-done | bytes 16416 | tf_op jit(solution)/shard_map/ppermute | solution.py:98
  41.8 0.0 collective-permute-done.8.refs_3_
  41.8 0.7 %last.1 = bf16[16,256]{1,0:T(8,128)(2,1)} custom-call(bf16[8,1024]{1,0:T(8,128)(2,1)S(1)} %get-tuple-element.34.refs_0_, bf16[8,1024]{1,0:T(8,128)(2,1)S(1)} %collective-permute-done.6.refs_1_, bf16[8,1024]{1,0:T(8,128)(2,1)S(1)} %collective-permute-done.7.refs_2_, bf16[2,8,1024]{2,1,0:T(8,128)(2,1)S(1)} %collective-permute-done.8.refs_3_, ...), custom_call_target="tpu_custom_call" | custom-call | tf_op jit(solution)/shard_map/last/pallas_call | solution.py:359
  (13 shorter events, 0.0 us)
Async XLA Ops:
  0.0 1.6 %copy-start.6 = (bf16[16,1024]{1,0:T(8,128)(2,1)S(1)}, bf16[16,1024]{1,0:T(8,128)(2,1)}, u32[]{:S(2)}) copy-start(bf16[16,1024]{1,0:T(8,128)(2,1)} %refs_4_.1) | copy-start | bytes 98308
  0.0 1.7 %copy-start.12 = (f32[256]{0:T(256)S(1)}, f32[256]{0:T(256)}, u32[]{:S(2)}) copy-start(f32[256]{0:T(256)} %param.32) | copy-start | bytes 3076
  0.0 1.7 %copy-start.11 = (bf16[1024,1]{0,1:T(2,128)(2,1)S(1)}, bf16[1024,1]{0,1:T(2,128)(2,1)}, u32[]{:S(2)}) copy-start(bf16[1024,1]{0,1:T(2,128)(2,1)} %param.29) | copy-start | bytes 6148
  0.0 1.7 %copy-start.10 = (bf16[1024,1]{0,1:T(2,128)(2,1)S(1)}, bf16[1024,1]{0,1:T(2,128)(2,1)}, u32[]{:S(2)}) copy-start(bf16[1024,1]{0,1:T(2,128)(2,1)} %param.28) | copy-start | bytes 6148
  0.0 1.7 %copy-start.5 = (bf16[1024,128]{1,0:T(8,128)(2,1)S(1)}, bf16[1024,128]{1,0:T(8,128)(2,1)}, u32[]{:S(2)}) copy-start(bf16[1024,128]{1,0:T(8,128)(2,1)} %refs_7_.1) | copy-start | bytes 786436
  0.0 1.7 %copy-start.4 = (bf16[1024,128]{1,0:T(8,128)(2,1)S(1)}, bf16[1024,128]{1,0:T(8,128)(2,1)}, u32[]{:S(2)}) copy-start(bf16[1024,128]{1,0:T(8,128)(2,1)} %refs_6_.1) | copy-start | bytes 786436
  0.0 1.7 %copy-start.9 = (f32[1024]{0:T(1024)S(1)}, f32[1024]{0:T(1024)}, u32[]{:S(2)}) copy-start(f32[1024]{0:T(1024)} %param.24) | copy-start | bytes 12292
  0.0 1.7 %copy-start.14 = (f32[16,1]{0,1:T(1,128)S(1)}, f32[16,1]{0,1:T(1,128)}, u32[]{:S(2)}) copy-start(f32[16,1]{0,1:T(1,128)} %param.23) | copy-start | bytes 196
  0.0 1.8 %copy-start = (f32[16,1,128,256]{3,2,1,0:T(8,128)S(1)}, f32[16,1,128,256]{3,2,1,0:T(8,128)}, u32[]{:S(2)}) copy-start(f32[16,1,128,256]{3,2,1,0:T(8,128)} %refs_9_.1) | copy-start | bytes 6291460
  1.6 2.2 %copy-start.1 = (bf16[1,1024,256]{2,1,0:T(8,128)(2,1)S(1)}, bf16[1,1024,256]{2,1,0:T(8,128)(2,1)}, u32[]{:S(2)}) copy-start(bf16[1,1024,256]{2,1,0:T(8,128)(2,1)} %param.38) | copy-start | bytes 1572868
  1.6 2.8 %copy-start.2 = (bf16[1,1024,256]{2,1,0:T(8,128)(2,1)S(1)}, bf16[1,1024,256]{2,1,0:T(8,128)(2,1)}, u32[]{:S(2)}) copy-start(bf16[1,1024,256]{2,1,0:T(8,128)(2,1)} %param.39) | copy-start | bytes 1572868
  1.6 2.8 %copy-start.3 = (bf16[1,256,1024]{2,1,0:T(8,128)(2,1)S(1)}, bf16[1,256,1024]{2,1,0:T(8,128)(2,1)}, u32[]{:S(2)}) copy-start(bf16[1,256,1024]{2,1,0:T(8,128)(2,1)} %param.40) | copy-start | bytes 1572868
  1.6 8.7 %copy-start.15 = (f32[16,6]{0,1:T(8,128)S(1)}, f32[16,6]{0,1:T(8,128)}, u32[]{:S(2)}) copy-start(f32[16,6]{0,1:T(8,128)} %param.37) | copy-start | bytes 1156
  1.6 8.7 %copy-start.16 = (s32[16,6]{0,1:T(8,128)S(1)}, s32[16,6]{0,1:T(8,128)}, u32[]{:S(2)}) copy-start(s32[16,6]{0,1:T(8,128)} %param.36) | copy-start | bytes 1156
  1.6 10.4 %copy-start.7 = (f32[1024]{0:T(1024)S(1)}, f32[1024]{0:T(1024)}, u32[]{:S(2)}) copy-start(f32[1024]{0:T(1024)} %param.34) | copy-start | bytes 12292
  1.6 10.4 %copy-start.8 = (f32[1024]{0:T(1024)S(1)}, f32[1024]{0:T(1024)}, u32[]{:S(2)}) copy-start(f32[1024]{0:T(1024)} %param.35) | copy-start | bytes 12292
  3.7 21.9 %collective-permute-start.3 = (bf16[1024,256]{1,0:T(8,128)(2,1)S(1)}, bf16[1024,256]{1,0:T(8,128)(2,1)S(1)}, u32[]{:S(2)}, u32[]{:S(2)}) collective-permute-start(bf16[1024,256]{1,0:T(8,128)(2,1)S(1)} %bitcast.12), channel_id=1, source_target_pairs={{0,1},{1,0},{2,3},{3,2},{4,5},{5,4},{6,7},{7,6},{8,9},{9,8},{10,11... | collective-permute-start | bytes 1572872 | tf_op jit(solution)/shard_map/ppermute | solution.py:98
  4.3 21.3 %collective-permute-start.4 = (bf16[1024,256]{1,0:T(8,128)(2,1)S(1)}, bf16[1024,256]{1,0:T(8,128)(2,1)S(1)}, u32[]{:S(2)}, u32[]{:S(2)}) collective-permute-start(bf16[1024,256]{1,0:T(8,128)(2,1)S(1)} %bitcast.14), channel_id=1, source_target_pairs={{0,1},{1,0},{2,3},{3,2},{4,5},{5,4},{6,7},{7,6},{8,9},{9,8},{10,11... | collective-permute-start | bytes 1572872 | tf_op jit(solution)/shard_map/ppermute | solution.py:98
  4.4 21.2 %collective-permute-start.5 = (bf16[256,1024]{1,0:T(8,128)(2,1)S(1)}, bf16[256,1024]{1,0:T(8,128)(2,1)S(1)}, u32[]{:S(2)}, u32[]{:S(2)}) collective-permute-start(bf16[256,1024]{1,0:T(8,128)(2,1)S(1)} %bitcast.16), channel_id=1, source_target_pairs={{0,1},{1,0},{2,3},{3,2},{4,5},{5,4},{6,7},{7,6},{8,9},{9,8},{10,11... | collective-permute-start | bytes 1572872 | tf_op jit(solution)/shard_map/ppermute | solution.py:98
  4.9 2.7 %collective-permute-start.2 = (bf16[8,1024]{1,0:T(8,128)(2,1)S(1)}, bf16[8,1024]{1,0:T(8,128)(2,1)S(1)}, u32[]{:S(2)}, u32[]{:S(2)}) collective-permute-start(bf16[8,1024]{1,0:T(8,128)(2,1)S(1)} %get-tuple-element.22), channel_id=1, source_target_pairs={{0,1},{1,0},{2,3},{3,2},{4,5},{5,4},{6,7},{7,6},{8,9},{9,8},{10,11... | collective-permute-start | bytes 49160 | tf_op jit(solution)/shard_map/ppermute | solution.py:98
  4.9 5.4 %collective-permute-start = (bf16[8,1024]{1,0:T(8,128)(2,1)S(1)}, bf16[8,1024]{1,0:T(8,128)(2,1)S(1)}, u32[]{:S(2)}, u32[]{:S(2)}) collective-permute-start(bf16[8,1024]{1,0:T(8,128)(2,1)S(1)} %get-tuple-element.22), channel_id=1, source_target_pairs={{0,3},{1,2},{2,1},{3,0},{4,7},{5,6},{6,5},{7,4},{8,11},{9,10},{10,... | collective-permute-start | bytes 49160 | tf_op jit(solution)/shard_map/ppermute | solution.py:98
  7.6 4.4 %collective-permute-start.1 = (bf16[8,1024]{1,0:T(8,128)(2,1)S(1)}, bf16[8,1024]{1,0:T(8,128)(2,1)S(1)}, u32[]{:S(2)}, u32[]{:S(2)}) collective-permute-start(bf16[8,1024]{1,0:T(8,128)(2,1)S(1)} %get-tuple-element.21.refs_0_), channel_id=1, source_target_pairs={{0,2},{1,3},{2,0},{3,1},{4,6},{5,7},{6,4},{7,5},{8,10},{9,11},{10,... | collective-permute-start | bytes 49160 | tf_op jit(solution)/shard_map/ppermute | solution.py:98
  12.0 29.8 %copy-start.13 = (f32[256]{0:T(256)S(1)}, f32[256]{0:T(256)}, u32[]{:S(2)}) copy-start(f32[256]{0:T(256)} %param.41) | copy-start | bytes 3076
  36.3 5.4 %collective-permute-start.8 = (bf16[2,8,1024]{2,1,0:T(8,128)(2,1)S(1)}, bf16[2,8,1024]{2,1,0:T(8,128)(2,1)S(1)}, u32[]{:S(2)}, u32[]{:S(2)}) collective-permute-start(bf16[2,8,1024]{2,1,0:T(8,128)(2,1)S(1)} %get-tuple-element.35), channel_id=1, source_target_pairs={{0,1},{1,0},{2,3},{3,2},{4,5},{5,4},{6,7},{7,6},{8,9},{9,8},{10,11... | collective-permute-start | bytes 98312 | tf_op jit(solution)/shard_map/ppermute | solution.py:98
  36.4 3.2 %collective-permute-start.7 = (bf16[8,1024]{1,0:T(8,128)(2,1)S(1)}, bf16[8,1024]{1,0:T(8,128)(2,1)S(1)}, u32[]{:S(2)}, u32[]{:S(2)}) collective-permute-start(bf16[8,1024]{1,0:T(8,128)(2,1)S(1)} %get-tuple-element.34.refs_0_), channel_id=1, source_target_pairs={{0,3},{1,2},{2,1},{3,0},{4,7},{5,6},{6,5},{7,4},{8,11},{9,10},{10,... | collective-permute-start | bytes 49160 | tf_op jit(solution)/shard_map/ppermute | solution.py:98
  38.0 3.7 %collective-permute-start.6 = (bf16[8,1024]{1,0:T(8,128)(2,1)S(1)}, bf16[8,1024]{1,0:T(8,128)(2,1)S(1)}, u32[]{:S(2)}, u32[]{:S(2)}) collective-permute-start(bf16[8,1024]{1,0:T(8,128)(2,1)S(1)} %get-tuple-element.34.refs_0_), channel_id=1, source_target_pairs={{0,2},{1,3},{2,0},{3,1},{4,6},{5,7},{6,4},{7,5},{8,10},{9,11},{10,... | collective-permute-start | bytes 49160 | tf_op jit(solution)/shard_map/ppermute | solution.py:98

commit v12 on v10

--- a/solution.py
+++ b/solution.py
@@ -262,13 +262,13 @@
     f32 = jnp.float32
     groups, half, width = rows.shape
     ffn_in = rows[...].reshape(groups * half, width)
-    total = None
-    for gates, ups, downs in ((gate_w, up_w, down_w), (gate_n, up_n, down_n)):
+    pairs = []
+    for gates, ups in ((gate_w, up_w), (gate_n, up_n)):
         gate = jnp.dot(ffn_in, gates[...], preferred_element_type=f32)
-        up = jnp.dot(ffn_in, ups[...], preferred_element_type=f32)
-        act = (gate * jax.nn.sigmoid(gate) * up).astype(jnp.bfloat16)
-        part = jnp.dot(act, downs[...], preferred_element_type=f32)
-        total = part if total is None else total + part
+        pairs.append((gate, jnp.dot(ffn_in, ups[...], preferred_element_type=f32)))
+    acts = [(gate * jax.nn.sigmoid(gate) * up).astype(jnp.bfloat16) for gate, up in pairs]
+    total = jnp.dot(acts[0], down_w[...], preferred_element_type=f32)
+    total = total + jnp.dot(acts[1], down_n[...], preferred_element_type=f32)
     out[...] = total.astype(jnp.bfloat16).reshape(groups, half, width)
 
 

time: 42.3 us -> 42.3 us (level)
  no operation moved by 1% of the time
where the time goes in v12:
time: 42.3 us; the launch traced here: 42.1 us
  blocking collectives  23.2 us (55%)
  starting transfers between devices  8.68 us (21%)
  waiting for transfers between devices  4.94 us (12%)
  Pallas kernels  3.01 us (7%)
  between operations  2.02 us (5%)
    all_to_all x1, blocking collectives, every_token(): rows = lax.all_to_all(spread, 'ep', split_axis=0, concat_axis=0, tiled=True)  13.4 us
    all_to_all x1, blocking collectives, every_token(): back = lax.all_to_all(blocks, 'ep', split_axis=0, concat_axis=0, tiled=True)  9.74 us
    ppermute x9, starting transfers between devices, exchange(): return lax.ppermute(value, axis, pairs)  8.68 us
    ppermute x9, waiting for transfers between devices, exchange(): return lax.ppermute(value, axis, pairs)  4.94 us
    pallas_call x1, Pallas kernels, cell(): pl.pallas_call(body, out_shape=[shape] * (2 if halves else 1), in_specs=[...  1.19 us
  transfers between devices with their start and end apart: 9, of which 3 were waited for; matrix products, arithmetic and copies ran while one was open for 0% of the time, Pallas kernels for 0%

profile of v12, /device:TPU:0, one launch (start us, length us, event | category | flops | bytes accessed | tf_op | source)
XLA Modules:
  0.0 42.1 jit_solution(14456521094886859821)
XLA Ops:
  0.0 0.0 copy-start.1
  0.0 0.0 copy-start.7
  0.0 0.0 copy-start.6
  1.8 0.0 copy-start.3
  1.9 0.0 copy-start.4
  1.9 0.0 copy-start.5
  1.9 0.0 copy-start.17
  1.9 0.0 copy-start.18
  1.9 0.0 copy-start.9
  1.9 0.0 copy-start.10
  1.9 0.0 copy-done.8
  1.9 0.0 copy-done.2
  2.0 0.0 copy-done.14
  2.0 0.0 copy-done.13
  2.0 0.0 copy-done.12
  2.0 0.0 copy-done.1
  2.0 0.0 copy-done.7
  2.0 0.0 copy-done.6
  2.0 0.0 copy-done.11
  2.0 0.0 copy-done.16
  2.0 0.1 copy-done
  2.2 1.2 %cell.1 = (bf16[8,1024]{1,0:T(8,128)(2,1)S(1)}, bf16[8,1024]{1,0:T(8,128)(2,1)S(1)}) custom-call(bf16[16,1024]{1,0:T(8,128)(2,1)S(1)} %copy-done.8, f32[1,1024]{1,0:T(1,128)S(1)} %bitcast.21, bf16[1,1024]{1,0:T(2,128)(2,1)S(1)} %bitcast.22, bf16[1,1024]{1,0:T(2,128)(2,1)S(1)} %bitcast.23, f32[2,1]{1,0:T(2,128)S(1)} %biases.1.refs_4_, f32[1,16]{1,0:T(1,128)S(1)} %bitcast.26, ...), custom_call_target="tpu_custom_call" | custom-call | tf_op jit(solution)/shard_map/cell/pallas_call | solution.py:216
  3.4 0.6 %collective-permute-start.3 = (bf16[1024,256]{1,0:T(8,128)(2,1)S(1)}, bf16[1024,256]{1,0:T(8,128)(2,1)S(1)}, u32[]{:S(2)}, u32[]{:S(2)}) collective-permute-start(bf16[1024,256]{1,0:T(8,128)(2,1)S(1)} %bitcast.12), channel_id=1, source_target_pairs={{0,1},{1,0},{2,3},{3,2},{4,5},{5,4},{6,7},{7,6},{8,9},{9,8},{10,11... | collective-permute-start | bytes 1572872 | tf_op jit(solution)/shard_map/ppermute | solution.py:98
  3.9 0.1 collective-permute-start.4
  4.0 0.0 copy-done.5
  4.0 0.4 %collective-permute-start.5 = (bf16[256,1024]{1,0:T(8,128)(2,1)S(1)}, bf16[256,1024]{1,0:T(8,128)(2,1)S(1)}, u32[]{:S(2)}, u32[]{:S(2)}) collective-permute-start(bf16[256,1024]{1,0:T(8,128)(2,1)S(1)} %bitcast.16), channel_id=1, source_target_pairs={{0,1},{1,0},{2,3},{3,2},{4,5},{5,4},{6,7},{7,6},{8,9},{9,8},{10,11... | collective-permute-start | bytes 1572872 | tf_op jit(solution)/shard_map/ppermute | solution.py:98
  4.5 0.1 collective-permute-start.2
  4.5 2.6 %collective-permute-start = (bf16[8,1024]{1,0:T(8,128)(2,1)S(1)}, bf16[8,1024]{1,0:T(8,128)(2,1)S(1)}, u32[]{:S(2)}, u32[]{:S(2)}) collective-permute-start(bf16[8,1024]{1,0:T(8,128)(2,1)S(1)} %get-tuple-element.22), channel_id=1, source_target_pairs={{0,3},{1,2},{2,1},{3,0},{4,7},{5,6},{6,5},{7,4},{8,11},{9,10},{10,... | collective-permute-start | bytes 49160 | tf_op jit(solution)/shard_map/ppermute | solution.py:98
  7.2 0.0 collective-permute-done.2.refs_3_
  7.2 2.7 %collective-permute-start.1 = (bf16[8,1024]{1,0:T(8,128)(2,1)S(1)}, bf16[8,1024]{1,0:T(8,128)(2,1)S(1)}, u32[]{:S(2)}, u32[]{:S(2)}) collective-permute-start(bf16[8,1024]{1,0:T(8,128)(2,1)S(1)} %get-tuple-element.21.refs_0_), channel_id=1, source_target_pairs={{0,2},{1,3},{2,0},{3,1},{4,6},{5,7},{6,4},{7,5},{8,10},{9,11},{10,... | collective-permute-start | bytes 49160 | tf_op jit(solution)/shard_map/ppermute | solution.py:98
  9.9 0.0 collective-permute-done.refs_1_
  9.9 1.7 %collective-permute-done.1.refs_2_ = bf16[8,1024]{1,0:T(8,128)(2,1)S(1)} collective-permute-done((bf16[8,1024]{1,0:T(8,128)(2,1)S(1)}, bf16[8,1024]{1,0:T(8,128)(2,1)S(1)}, u32[]{:S(2)}, u32[]{:S(2)}) %collective-permute-start.1) | collective-permute-done | bytes 16416 | tf_op jit(solution)/shard_map/ppermute | solution.py:98
  11.6 0.0 copy-done.10
  11.6 0.2 after_mix.1
  11.8 13.4 %all_to_all.10.rows = bf16[8,8,1024]{2,1,0:T(8,128)(2,1)S(1)} all-to-all(bf16[8,8,1024]{2,1,0:T(8,128)(2,1)S(1)} %get-tuple-element.24), channel_id=1, replica_groups=mesh['ep'=8,'tp'=4] {'ep'}, dimensions={0} | all-to-all | bytes 262144 | tf_op jit(solution)/shard_map/all_to_all | solution.py:384
  25.3 0.0 collective-permute-done.3.gate_n
  25.3 0.0 collective-permute-done.4.up_n
  25.3 0.0 collective-permute-done.5.down_n
  25.3 0.7 %expert.1 = bf16[8,8,1024]{2,1,0:T(8,128)(2,1)S(1)} custom-call(bf16[8,8,1024]{2,1,0:T(8,128)(2,1)S(1)} %all_to_all.10.rows, bf16[1024,256]{1,0:T(8,128)(2,1)S(1)} %bitcast.13, bf16[1024,256]{1,0:T(8,128)(2,1)S(1)} %bitcast.15, bf16[256,1024]{1,0:T(8,128)(2,1)S(1)} %bitcast.17, bf16[1024,256]{1,0:T(8,128)(2,1)S(1)} %collective-permute-done.3.gate_n, ...), custom_call_target="tpu_custom_call" | custom-call | tf_op jit(solution)/shard_map/expert/pallas_call | solution.py:276
  26.0 9.7 %all_to_all.11.back = bf16[8,8,1024]{2,1,0:T(8,128)(2,1)S(1)} all-to-all(bf16[8,8,1024]{2,1,0:T(8,128)(2,1)S(1)} %expert.1), channel_id=1, replica_groups=mesh['ep'=8,'tp'=4] {'ep'}, dimensions={0} | all-to-all | bytes 262144 | tf_op jit(solution)/shard_map/all_to_all | solution.py:387
  35.8 0.2 share.1
  35.9 0.1 collective-permute-start.8
  36.0 1.6 %collective-permute-start.7 = (bf16[8,1024]{1,0:T(8,128)(2,1)S(1)}, bf16[8,1024]{1,0:T(8,128)(2,1)S(1)}, u32[]{:S(2)}, u32[]{:S(2)}) collective-permute-start(bf16[8,1024]{1,0:T(8,128)(2,1)S(1)} %get-tuple-element.34.refs_0_), channel_id=1, source_target_pairs={{0,3},{1,2},{2,1},{3,0},{4,7},{5,6},{6,5},{7,4},{8,11},{9,10},{10,... | collective-permute-start | bytes 49160 | tf_op jit(solution)/shard_map/ppermute | solution.py:98
  37.6 0.5 %collective-permute-start.6 = (bf16[8,1024]{1,0:T(8,128)(2,1)S(1)}, bf16[8,1024]{1,0:T(8,128)(2,1)S(1)}, u32[]{:S(2)}, u32[]{:S(2)}) collective-permute-start(bf16[8,1024]{1,0:T(8,128)(2,1)S(1)} %get-tuple-element.34.refs_0_), channel_id=1, source_target_pairs={{0,2},{1,3},{2,0},{3,1},{4,6},{5,7},{6,4},{7,5},{8,10},{9,11},{10,... | collective-permute-start | bytes 49160 | tf_op jit(solution)/shard_map/ppermute | solution.py:98
  38.1 1.1 %collective-permute-done.7.refs_2_ = bf16[8,1024]{1,0:T(8,128)(2,1)S(1)} collective-permute-done((bf16[8,1024]{1,0:T(8,128)(2,1)S(1)}, bf16[8,1024]{1,0:T(8,128)(2,1)S(1)}, u32[]{:S(2)}, u32[]{:S(2)}) %collective-permute-start.7) | collective-permute-done | bytes 16416 | tf_op jit(solution)/shard_map/ppermute | solution.py:98
  39.2 2.1 %collective-permute-done.6.refs_1_ = bf16[8,1024]{1,0:T(8,128)(2,1)S(1)} collective-permute-done((bf16[8,1024]{1,0:T(8,128)(2,1)S(1)}, bf16[8,1024]{1,0:T(8,128)(2,1)S(1)}, u32[]{:S(2)}, u32[]{:S(2)}) %collective-permute-start.6) | collective-permute-done | bytes 16416 | tf_op jit(solution)/shard_map/ppermute | solution.py:98
  41.4 0.0 collective-permute-done.8.refs_3_
  41.4 0.7 %last.1 = bf16[16,256]{1,0:T(8,128)(2,1)} custom-call(bf16[8,1024]{1,0:T(8,128)(2,1)S(1)} %get-tuple-element.34.refs_0_, bf16[8,1024]{1,0:T(8,128)(2,1)S(1)} %collective-permute-done.6.refs_1_, bf16[8,1024]{1,0:T(8,128)(2,1)S(1)} %collective-permute-done.7.refs_2_, bf16[2,8,1024]{2,1,0:T(8,128)(2,1)S(1)} %collective-permute-done.8.refs_3_, ...), custom_call_target="tpu_custom_call" | custom-call | tf_op jit(solution)/shard_map/last/pallas_call | solution.py:344
  (17 shorter events, 0.0 us)
Async XLA Ops:
  0.0 1.9 %copy-start.8 = (bf16[16,1024]{1,0:T(8,128)(2,1)S(1)}, bf16[16,1024]{1,0:T(8,128)(2,1)}, u32[]{:S(2)}) copy-start(bf16[16,1024]{1,0:T(8,128)(2,1)} %refs_4_.1) | copy-start | bytes 98308
  0.0 1.9 %copy-start.2 = (bf16[256,1024]{1,0:T(8,128)(2,1)S(1)}, bf16[256,1024]{1,0:T(8,128)(2,1)}, u32[]{:S(2)}) copy-start(bf16[256,1024]{1,0:T(8,128)(2,1)} %refs_11_.1) | copy-start | bytes 1572868
  0.0 2.0 %copy-start.14 = (f32[256]{0:T(256)S(1)}, f32[256]{0:T(256)}, u32[]{:S(2)}) copy-start(f32[256]{0:T(256)} %param.32) | copy-start | bytes 3076
  0.0 2.0 %copy-start.13 = (bf16[1024,1]{0,1:T(2,128)(2,1)S(1)}, bf16[1024,1]{0,1:T(2,128)(2,1)}, u32[]{:S(2)}) copy-start(bf16[1024,1]{0,1:T(2,128)(2,1)} %param.29) | copy-start | bytes 6148
  0.0 2.0 %copy-start.12 = (bf16[1024,1]{0,1:T(2,128)(2,1)S(1)}, bf16[1024,1]{0,1:T(2,128)(2,1)}, u32[]{:S(2)}) copy-start(bf16[1024,1]{0,1:T(2,128)(2,1)} %param.28) | copy-start | bytes 6148
  0.0 2.0 %copy-start.1 = (bf16[1024,256]{1,0:T(8,128)(2,1)S(1)}, bf16[1024,256]{1,0:T(8,128)(2,1)}, u32[]{:S(2)}) copy-start(bf16[1024,256]{1,0:T(8,128)(2,1)} %refs_8_.1) | copy-start | bytes 1572868
  0.0 2.0 %copy-start.7 = (bf16[1024,128]{1,0:T(8,128)(2,1)S(1)}, bf16[1024,128]{1,0:T(8,128)(2,1)}, u32[]{:S(2)}) copy-start(bf16[1024,128]{1,0:T(8,128)(2,1)} %refs_7_.1) | copy-start | bytes 786436
  0.0 2.0 %copy-start.6 = (bf16[1024,128]{1,0:T(8,128)(2,1)S(1)}, bf16[1024,128]{1,0:T(8,128)(2,1)}, u32[]{:S(2)}) copy-start(bf16[1024,128]{1,0:T(8,128)(2,1)} %refs_6_.1) | copy-start | bytes 786436
  0.0 2.0 %copy-start.11 = (f32[1024]{0:T(1024)S(1)}, f32[1024]{0:T(1024)}, u32[]{:S(2)}) copy-start(f32[1024]{0:T(1024)} %param.24) | copy-start | bytes 12292
  0.1 2.0 %copy-start.16 = (f32[16,1]{0,1:T(1,128)S(1)}, f32[16,1]{0,1:T(1,128)}, u32[]{:S(2)}) copy-start(f32[16,1]{0,1:T(1,128)} %param.23) | copy-start | bytes 196
  0.1 2.1 %copy-start = (f32[16,1,128,256]{3,2,1,0:T(8,128)S(1)}, f32[16,1,128,256]{3,2,1,0:T(8,128)}, u32[]{:S(2)}) copy-start(f32[16,1,128,256]{3,2,1,0:T(8,128)} %refs_9_.1) | copy-start | bytes 6291460
  1.8 1.5 %copy-start.3 = (bf16[1,1024,256]{2,1,0:T(8,128)(2,1)S(1)}, bf16[1,1024,256]{2,1,0:T(8,128)(2,1)}, u32[]{:S(2)}) copy-start(bf16[1,1024,256]{2,1,0:T(8,128)(2,1)} %param.38) | copy-start | bytes 1572868
  1.9 2.1 %copy-start.4 = (bf16[1,1024,256]{2,1,0:T(8,128)(2,1)S(1)}, bf16[1,1024,256]{2,1,0:T(8,128)(2,1)}, u32[]{:S(2)}) copy-start(bf16[1,1024,256]{2,1,0:T(8,128)(2,1)} %param.39) | copy-start | bytes 1572868
  1.9 2.2 %copy-start.5 = (bf16[1,256,1024]{2,1,0:T(8,128)(2,1)S(1)}, bf16[1,256,1024]{2,1,0:T(8,128)(2,1)}, u32[]{:S(2)}) copy-start(bf16[1,256,1024]{2,1,0:T(8,128)(2,1)} %param.40) | copy-start | bytes 1572868
  1.9 8.0 %copy-start.17 = (f32[16,6]{0,1:T(8,128)S(1)}, f32[16,6]{0,1:T(8,128)}, u32[]{:S(2)}) copy-start(f32[16,6]{0,1:T(8,128)} %param.37) | copy-start | bytes 1156
  1.9 8.0 %copy-start.18 = (s32[16,6]{0,1:T(8,128)S(1)}, s32[16,6]{0,1:T(8,128)}, u32[]{:S(2)}) copy-start(s32[16,6]{0,1:T(8,128)} %param.36) | copy-start | bytes 1156
  1.9 9.7 %copy-start.9 = (f32[1024]{0:T(1024)S(1)}, f32[1024]{0:T(1024)}, u32[]{:S(2)}) copy-start(f32[1024]{0:T(1024)} %param.34) | copy-start | bytes 12292
  1.9 9.7 %copy-start.10 = (f32[1024]{0:T(1024)S(1)}, f32[1024]{0:T(1024)}, u32[]{:S(2)}) copy-start(f32[1024]{0:T(1024)} %param.35) | copy-start | bytes 12292
  3.4 21.9 %collective-permute-start.3 = (bf16[1024,256]{1,0:T(8,128)(2,1)S(1)}, bf16[1024,256]{1,0:T(8,128)(2,1)S(1)}, u32[]{:S(2)}, u32[]{:S(2)}) collective-permute-start(bf16[1024,256]{1,0:T(8,128)(2,1)S(1)} %bitcast.12), channel_id=1, source_target_pairs={{0,1},{1,0},{2,3},{3,2},{4,5},{5,4},{6,7},{7,6},{8,9},{9,8},{10,11... | collective-permute-start | bytes 1572872 | tf_op jit(solution)/shard_map/ppermute | solution.py:98
  3.9 21.3 %collective-permute-start.4 = (bf16[1024,256]{1,0:T(8,128)(2,1)S(1)}, bf16[1024,256]{1,0:T(8,128)(2,1)S(1)}, u32[]{:S(2)}, u32[]{:S(2)}) collective-permute-start(bf16[1024,256]{1,0:T(8,128)(2,1)S(1)} %bitcast.14), channel_id=1, source_target_pairs={{0,1},{1,0},{2,3},{3,2},{4,5},{5,4},{6,7},{7,6},{8,9},{9,8},{10,11... | collective-permute-start | bytes 1572872 | tf_op jit(solution)/shard_map/ppermute | solution.py:98
  4.0 21.2 %collective-permute-start.5 = (bf16[256,1024]{1,0:T(8,128)(2,1)S(1)}, bf16[256,1024]{1,0:T(8,128)(2,1)S(1)}, u32[]{:S(2)}, u32[]{:S(2)}) collective-permute-start(bf16[256,1024]{1,0:T(8,128)(2,1)S(1)} %bitcast.16), channel_id=1, source_target_pairs={{0,1},{1,0},{2,3},{3,2},{4,5},{5,4},{6,7},{7,6},{8,9},{9,8},{10,11... | collective-permute-start | bytes 1572872 | tf_op jit(solution)/shard_map/ppermute | solution.py:98
  4.5 2.7 %collective-permute-start.2 = (bf16[8,1024]{1,0:T(8,128)(2,1)S(1)}, bf16[8,1024]{1,0:T(8,128)(2,1)S(1)}, u32[]{:S(2)}, u32[]{:S(2)}) collective-permute-start(bf16[8,1024]{1,0:T(8,128)(2,1)S(1)} %get-tuple-element.22), channel_id=1, source_target_pairs={{0,1},{1,0},{2,3},{3,2},{4,5},{5,4},{6,7},{7,6},{8,9},{9,8},{10,11... | collective-permute-start | bytes 49160 | tf_op jit(solution)/shard_map/ppermute | solution.py:98
  4.5 5.4 %collective-permute-start = (bf16[8,1024]{1,0:T(8,128)(2,1)S(1)}, bf16[8,1024]{1,0:T(8,128)(2,1)S(1)}, u32[]{:S(2)}, u32[]{:S(2)}) collective-permute-start(bf16[8,1024]{1,0:T(8,128)(2,1)S(1)} %get-tuple-element.22), channel_id=1, source_target_pairs={{0,3},{1,2},{2,1},{3,0},{4,7},{5,6},{6,5},{7,4},{8,11},{9,10},{10,... | collective-permute-start | bytes 49160 | tf_op jit(solution)/shard_map/ppermute | solution.py:98
  7.2 4.4 %collective-permute-start.1 = (bf16[8,1024]{1,0:T(8,128)(2,1)S(1)}, bf16[8,1024]{1,0:T(8,128)(2,1)S(1)}, u32[]{:S(2)}, u32[]{:S(2)}) collective-permute-start(bf16[8,1024]{1,0:T(8,128)(2,1)S(1)} %get-tuple-element.21.refs_0_), channel_id=1, source_target_pairs={{0,2},{1,3},{2,0},{3,1},{4,6},{5,7},{6,4},{7,5},{8,10},{9,11},{10,... | collective-permute-start | bytes 49160 | tf_op jit(solution)/shard_map/ppermute | solution.py:98
  11.6 29.8 %copy-start.15 = (f32[256]{0:T(256)S(1)}, f32[256]{0:T(256)}, u32[]{:S(2)}) copy-start(f32[256]{0:T(256)} %param.41) | copy-start | bytes 3076
  35.9 5.4 %collective-permute-start.8 = (bf16[2,8,1024]{2,1,0:T(8,128)(2,1)S(1)}, bf16[2,8,1024]{2,1,0:T(8,128)(2,1)S(1)}, u32[]{:S(2)}, u32[]{:S(2)}) collective-permute-start(bf16[2,8,1024]{2,1,0:T(8,128)(2,1)S(1)} %get-tuple-element.35), channel_id=1, source_target_pairs={{0,1},{1,0},{2,3},{3,2},{4,5},{5,4},{6,7},{7,6},{8,9},{9,8},{10,11... | collective-permute-start | bytes 98312 | tf_op jit(solution)/shard_map/ppermute | solution.py:98
  36.0 3.2 %collective-permute-start.7 = (bf16[8,1024]{1,0:T(8,128)(2,1)S(1)}, bf16[8,1024]{1,0:T(8,128)(2,1)S(1)}, u32[]{:S(2)}, u32[]{:S(2)}) collective-permute-start(bf16[8,1024]{1,0:T(8,128)(2,1)S(1)} %get-tuple-element.34.refs_0_), channel_id=1, source_target_pairs={{0,3},{1,2},{2,1},{3,0},{4,7},{5,6},{6,5},{7,4},{8,11},{9,10},{10,... | collective-permute-start | bytes 49160 | tf_op jit(solution)/shard_map/ppermute | solution.py:98
  37.6 3.7 %collective-permute-start.6 = (bf16[8,1024]{1,0:T(8,128)(2,1)S(1)}, bf16[8,1024]{1,0:T(8,128)(2,1)S(1)}, u32[]{:S(2)}, u32[]{:S(2)}) collective-permute-start(bf16[8,1024]{1,0:T(8,128)(2,1)S(1)} %get-tuple-element.34.refs_0_), channel_id=1, source_target_pairs={{0,2},{1,3},{2,0},{3,1},{4,6},{5,7},{6,4},{7,5},{8,10},{9,11},{10,... | collective-permute-start | bytes 49160 | tf_op jit(solution)/shard_map/ppermute | solution.py:98
